TPU v7x, 256 devices: a whole 4x4x8 slice. The times are simulated.
256 devices in a mesh: kv: 16 (over y, x), tp: 16 (over z, core).
Axes of the slice: x: 4, y: 4, z: 8, core: 2. Of those that a mesh axis runs over, the one named last changes fastest.
Arguments:
- tokens: bfloat16 [1536, 4096], P('kv', 'tp'), may hold values from -20 to 20
- state: float32 [1536, 32, 4096], P('kv', 'tp'), may hold values from -4 to 4
- w_query: bfloat16 [4096, 2048], P(None, 'tp'), may hold values from -0.09375 to 0.09375
- w_key: bfloat16 [4096, 2048], P(None, 'tp'), may hold values from -0.09375 to 0.09375
- w_value: bfloat16 [4096, 2048], P(None, 'tp'), may hold values from -0.09375 to 0.09375
- w_gate: bfloat16 [4096, 2048], P(None, 'tp'), may hold values from -0.09375 to 0.09375
- w_decay: bfloat16 [4096, 32], replicated, may hold values from -0.09375 to 0.09375
- w_beta: bfloat16 [4096, 32], replicated, may hold values from -0.09375 to 0.09375
- decay_rate: float32 [32], P('tp'), may hold values from 0.03 to 3
- decay_bias: float32 [32], P('tp'), may hold values from -1 to 1
- mix_gain: float32 [4096], replicated, may hold values from 0.1 to 1.9
- out_gain: float32 [64], replicated, may hold values from 0.1 to 1.9
- w_out: bfloat16 [2048, 4096], P('tp'), may hold values from -0.125 to 0.125
- ffn_gain: float32 [4096], replicated, may hold values from 0.1 to 1.9
- w_up: bfloat16 [4096, 16384], P('tp', 'kv'), may hold values from -0.09375 to 0.09375
- w_down: bfloat16 [16384, 4096], P('kv', 'tp'), may hold values from -0.046875 to 0.046875
Outputs:
- mixed: bfloat16 [1536, 4096], P('kv', 'tp')
- new_state: float32 [1536, 32, 4096], P('kv', 'tp')
All inputs are finite; a program needn't handle non-finite values.
Results may differ from a plain program's by a relative error of at most 0.024.
Values may be sent and summed in bfloat16 or wider, within the bound.
No kernel may reach another device: no remote copies, remote signals or barrier semaphores. Data moves between devices by JAX's collectives and lax.ppermute only.
A program may use at most 64 MiB of HBM per device.

v0:
```python
import jax
import jax.numpy as jnp
from jax import lax
from jax.sharding import Mesh
from jax.sharding import PartitionSpec as P

D = 4096
HEAD_DIM = 64
TP = ("tp_0", "tp_1")


EPS = 1e-06


def sent_to_all(array, axis):
    length = lax.axis_size(axis)
    return lax.all_to_all(
        jnp.broadcast_to(array[None], (length, *array.shape)), axis, 0, 0, tiled=True
    )


def joined_along(parts, dim):
    dims = list(parts.shape[1:])
    dims[dim] *= parts.shape[0]
    return jnp.moveaxis(parts, 0, dim).reshape(dims)


def gathered_copies(array, axis, dim):
    parts = sent_to_all(array, axis)
    return joined_along(parts, dim)


def in_blocks(array, dim, length):
    before, after = (array.shape[:dim], array.shape[dim + 1 :])
    return jnp.moveaxis(array.reshape(*before, length, -1, *after), dim, 0)


def sum_at_owner(array, axis, dim):
    parts = in_blocks(array, dim, lax.axis_size(axis))
    arrived = lax.all_to_all(parts, axis, split_axis=0, concat_axis=0, tiled=True)
    return arrived.astype(jnp.float32).sum(axis=0)


def over_copies(array, axis):
    everything = sent_to_all(array, axis)
    return jnp.sum(everything, axis=0)


def scatter_pairs(array, chips, core, dim):
    sizes = (lax.axis_size(chips), lax.axis_size(core))
    parts = in_blocks(array, dim, sizes[0] * sizes[1])
    inside = parts.shape[1:]
    parts = parts.reshape(*sizes, *inside).swapaxes(0, 1).reshape(-1, *inside)
    parts = lax.psum_scatter(parts, core, scatter_dimension=0, tiled=True)
    return lax.psum_scatter(parts, chips, scatter_dimension=0, tiled=True)[0]


def unit_norm(vector):
    return vector * lax.rsqrt(jnp.sum(vector * vector, axis=-1, keepdims=True) + EPS)


def local(
    tokens,
    state,
    w_query,
    w_key,
    w_value,
    w_gate,
    w_decay,
    w_beta,
    decay_rate,
    decay_bias,
    mix_gain,
    out_gain,
    w_out,
    ffn_gain,
    w_up,
    w_down,
):
    rows = tokens.shape[0]
    width_share = tokens.shape[1]
    head_count = w_query.shape[1] // HEAD_DIM
    full_rows = gathered_copies(tokens, TP, 1)
    full_f = full_rows.astype(jnp.float32)
    normed = (
        full_f * lax.rsqrt(jnp.mean(full_f * full_f, axis=-1, keepdims=True) + EPS) * mix_gain
    ).astype(jnp.bfloat16)
    query = jnp.dot(normed, w_query, preferred_element_type=jnp.float32).reshape(
        rows, head_count, HEAD_DIM
    )
    key_proj = jnp.dot(normed, w_key, preferred_element_type=jnp.float32).reshape(
        rows, head_count, HEAD_DIM
    )
    value = jnp.dot(normed, w_value, preferred_element_type=jnp.float32).reshape(
        rows, head_count, HEAD_DIM
    )
    gate = jnp.dot(normed, w_gate, preferred_element_type=jnp.float32).reshape(
        rows, head_count, HEAD_DIM
    )
    query = unit_norm(query) * HEAD_DIM ** (-0.5)
    key_proj = unit_norm(key_proj)
    head_start = lax.axis_index(TP) * head_count
    decay_cols = lax.dynamic_slice_in_dim(w_decay, head_start, head_count, 1)
    beta_cols = lax.dynamic_slice_in_dim(w_beta, head_start, head_count, 1)
    pre_decay = jnp.dot(normed, decay_cols, preferred_element_type=jnp.float32)
    decay = jnp.exp(-decay_rate * jax.nn.softplus(pre_decay + decay_bias))
    strength = jax.nn.sigmoid(jnp.dot(normed, beta_cols, preferred_element_type=jnp.float32))
    matrix = state.reshape(rows, head_count, HEAD_DIM, HEAD_DIM) * decay[:, :, None, None]
    recalled = jnp.einsum("bhk,bhkv->bhv", key_proj, matrix, precision=lax.Precision.HIGHEST)
    delta = (value - recalled) * strength[:, :, None]
    matrix = matrix + key_proj[:, :, :, None] * delta[:, :, None, :]
    head_out = jnp.einsum("bhk,bhkv->bhv", query, matrix, precision=lax.Precision.HIGHEST)
    head_out = (
        head_out
        * lax.rsqrt(jnp.mean(head_out * head_out, axis=-1, keepdims=True) + EPS)
        * out_gain
        * jax.nn.silu(gate)
    )
    head_out = head_out.reshape(rows, head_count * HEAD_DIM).astype(jnp.bfloat16)
    partial_value = jnp.dot(head_out, w_out, preferred_element_type=jnp.float32)
    feature_start = lax.axis_index(TP) * width_share
    gain_share = lax.dynamic_slice_in_dim(ffn_gain, feature_start, width_share, 0)
    resid = tokens.astype(jnp.float32) + sum_at_owner(partial_value.astype(jnp.bfloat16), TP, 1)
    squares = over_copies(jnp.sum(resid * resid, axis=-1), TP)
    scale = lax.rsqrt(squares[:, None] / D + EPS)
    ffn_in = (resid * scale * gain_share).astype(jnp.bfloat16)
    up_part = jnp.dot(gathered_copies(ffn_in, "kv", 0), w_up, preferred_element_type=jnp.float32)
    up_share = scatter_pairs(up_part.astype(jnp.bfloat16), "tp_0", "tp_1", 0).astype(jnp.float32)
    hidden_share = jnp.square(jax.nn.relu(up_share)).astype(jnp.bfloat16)
    hidden = lax.all_gather(hidden_share, TP, axis=0, tiled=True)
    down = sum_at_owner(
        jnp.dot(hidden, w_down, preferred_element_type=jnp.float32).astype(jnp.bfloat16), "kv", 0
    )
    mixed = (resid + down).astype(jnp.bfloat16)
    return (mixed, matrix.reshape(rows, head_count, HEAD_DIM * HEAD_DIM))


def solution(mesh):
    split = Mesh(mesh.devices.reshape(mesh.shape["kv"], 8, 2), ("kv", "tp_0", "tp_1"))
    placed = (
        P("kv", TP),
        P("kv", TP, None),
        P(None, TP),
        P(None, TP),
        P(None, TP),
        P(None, TP),
        P(),
        P(),
        P(TP),
        P(TP),
        P(),
        P(),
        P(TP, None),
        P(),
        P(TP, "kv"),
        P("kv", TP),
    )
    return jax.shard_map(
        local,
        mesh=split,
        in_specs=placed,
        out_specs=(P("kv", TP), P("kv", TP, None)),
        check_vma=False,
    )
```

profile of v0, /device:TPU:1, one launch (start us, length us, event | category | flops | bytes accessed | tf_op | source)
XLA Modules:
  0.0 243.3 jit_solution(4121412433545076519)
XLA Ops:
  7.2 1.9 broadcast_in_dim.6
  9.1 10.0 %all-to-all-start = ((bf16[16,96,256]{2,1,0:T(8,128)(2,1)}), bf16[16,96,256]{2,1,0:T(8,128)(2,1)S(1)}, u32[]{:S(2)}, u32[]{:S(2)}) async-start(bf16[16,96,256]{2,1,0:T(8,128)(2,1)} %broadcast_in_dim.6), calls=%async_computation | async-start | bytes 1572864 | tf_op jit(solution)/shard_map/all_to_all | solution.py:17
  19.1 0.7 mul.175
  19.8 1.3 copy.69
  21.1 2.3 copy.66
  23.4 6.1 %copy.67 = f32[96,2,4096]{0,2,1:T(8,128)} copy(f32[96,2,4096]{2,1,0:T(2,128)} %param.17) | data formatting | bytes 6291456 | tf_op args[1]
  29.5 1.3 copy.70
  30.8 2.3 copy.71
  33.1 8.7 %all-to-all-done = bf16[16,96,256]{2,1,0:T(8,128)(2,1)S(1)} async-done(((bf16[16,96,256]{2,1,0:T(8,128)(2,1)}), bf16[16,96,256]{2,1,0:T(8,128)(2,1)S(1)}, u32[]{:S(2)}, u32[]{:S(2)}) %all-to-all-start) | async-done | bytes 786464 | tf_op jit(solution)/shard_map/all_to_all | solution.py:17
  43.1 1.7 multiply_reduce_fusion.4
  44.8 1.7 multiply_reduce_fusion.5
  47.2 1.5 fusion.11
  48.7 1.3 fusion.16
  51.2 3.0 %broadcast_multiply_fusion = (f32[96,2,64,64]{0,3,2,1:T(8,128)}, f32[96,2,64]{0,2,1:T(8,128)S(1)}) fusion(f32[96,2,64]{0,2,1:T(8,128)S(1)} %fusion.8, f32[96,2,64]{0,2,1:T(8,128)S(1)} %get-tuple-element.19, f32[96,2,64,64]{0,3,2,1:T(8,128)S(1)} %bitcast.55, f32[96,2]{0,1:T(2,128)S(1)} %fusion.16, f32[96,2,64]{0,2,1:T(8,128)S(1)} %get-tuple-element.18), kind=kLoop, calls=%fused_computation.11 | loop fusion | flops 3919872 | bytes 6488832 | tf_op jit(solution)/shard_map/mul | solution.py:111
  55.3 25.8 %all_to_all.26 = bf16[16,96,256]{2,1,0:T(8,128)(2,1)S(1)} all-to-all(bf16[16,96,256]{2,1,0:T(8,128)(2,1)S(1)} %bitcast.66), channel_id=1, replica_groups=mesh['kv'=16,'tp_0'=8,'tp_1'=2] {'tp_0','tp_1'}, dimensions={0} | all-to-all | bytes 1572864 | tf_op jit(solution)/shard_map/all_to_all | solution.py:40
  81.3 0.6 broadcast_in_dim.7
  82.0 3.4 %all-to-all-start.2 = ((f32[16,1,96]{2,1,0:T(1,128)}), f32[16,1,96]{2,1,0:T(1,128)S(1)}, u32[]{:S(2)}, u32[]{:S(2)}) async-start(f32[16,1,96]{2,1,0:T(1,128)} %broadcast_in_dim.7), calls=%async_computation.2 | async-start | bytes 16384 | tf_op jit(solution)/shard_map/all_to_all | solution.py:17
  85.4 0.8 dynamic_slice.11
  86.2 5.8 %all-to-all-done.2 = f32[16,1,96]{2,1,0:T(1,128)S(1)} async-done(((f32[16,1,96]{2,1,0:T(1,128)}), f32[16,1,96]{2,1,0:T(1,128)S(1)}, u32[]{:S(2)}, u32[]{:S(2)}) %all-to-all-start.2) | async-done | bytes 6176 | tf_op jit(solution)/shard_map/all_to_all | solution.py:17
  92.1 20.1 %all_to_all.27 = bf16[16,96,256]{2,1,0:T(8,128)(2,1)S(1)} all-to-all(bf16[16,96,256]{2,1,0:T(8,128)(2,1)S(1)} %broadcast_in_dim.8), channel_id=1, replica_groups=mesh['kv'=16,'tp_0'=8,'tp_1'=2] {'kv'}, dimensions={0} | all-to-all | bytes 1572864 | tf_op jit(solution)/shard_map/all_to_all | solution.py:17
  112.2 1.0 convolution_convert_fusion.1
  113.2 2.1 copy.74
  115.4 10.4 %reduce-scatter.3.cloned.1.call-done = bf16[8,96,1024]{2,1,0:T(8,128)(2,1)} async-done(((bf16[16,96,1024]{2,1,0:T(8,128)(2,1)}), bf16[8,96,1024]{2,1,0:T(8,128)(2,1)}) %reduce-scatter.3.cloned.1.call-update) | async-done | bytes 1572880 | tf_op jit(solution)/shard_map/reduce_scatter | solution.py:54
  125.8 40.4 %reduce-scatter.5.cloned.1.call-done = bf16[1,96,1024]{2,1,0:T(8,128)(2,1)} async-done(((bf16[8,96,1024]{2,1,0:T(8,128)(2,1)}), bf16[1,96,1024]{2,1,0:T(8,128)(2,1)}) %reduce-scatter.5.cloned.1.call-update) | async-done | bytes 196624 | tf_op jit(solution)/shard_map/reduce_scatter | solution.py:55
  166.2 1.6 multiply_convert_fusion.1
  167.9 44.2 %all-gather.3.cloned.1.call-done = bf16[1,1536,1024]{2,1,0:T(8,128)(2,1)} async-done(((bf16[1,96,1024]{2,1,0:T(8,128)(2,1)}), bf16[1,1536,1024]{2,1,0:T(8,128)(2,1)}) %all-gather.3.cloned.1.call-update) | async-done | bytes 3145744 | tf_op jit(solution)/shard_map/all_gather | solution.py:130
  212.1 3.8 %fusion.2 = bf16[1536,256]{1,0:T(8,128)(2,1)} fusion(bf16[1024,256]{1,0:T(8,128)(2,1)S(1)} %copy-done.11, bf16[1,1536,1024]{2,1,0:T(8,128)(2,1)} %all-gather.3.cloned.1.call-done), kind=kOutput, calls=%fused_computation.7 | convolution fusion | flops 805699584 | bytes 4456448 | tf_op jit(solution)/shard_map/dot_general | solution.py:132
  215.9 6.5 %all-to-all-start.4 = ((bf16[16,96,256]{2,1,0:T(8,128)(2,1)}), bf16[16,96,256]{2,1,0:T(8,128)(2,1)S(1)}, u32[]{:S(2)}, u32[]{:S(2)}) async-start(bf16[16,96,256]{2,1,0:T(8,128)(2,1)} %bitcast.19), calls=%async_computation.6 | async-start | bytes 1572864 | tf_op jit(solution)/shard_map/all_to_all | solution.py:40
  222.4 5.8 %bitcast_add_fusion = f32[96,2,4096]{0,2,1:T(8,128)} fusion(f32[96,2,64,64]{0,3,2,1:T(8,128)} %get-tuple-element.12, f32[96,2,4096]{0,2,1:T(8,128)} %copy.67, f32[96,2]{0,1:T(2,128)S(1)} %fusion.16), kind=kLoop, calls=%fused_computation.1 | loop fusion | flops 1572864 | bytes 9437952 | tf_op jit(solution)/shard_map/add | solution.py:111
  228.2 6.0 %copy.76 = f32[96,2,4096]{2,1,0:T(2,128)} copy(f32[96,2,4096]{0,2,1:T(8,128)} %bitcast_add_fusion) | data formatting | bytes 6291456
  234.2 1.8 all-to-all-done.4
  236.2 0.6 add_convert_fusion
  (57 shorter events, 4.8 us)
Async XLA Ops:
  7.2 47.6 %copy-start = (bf16[128,4096]{1,0:T(8,128)(2,1)S(1)}, bf16[128,4096]{1,0:T(8,128)(2,1)}, u32[]{:S(2)}) copy-start(bf16[128,4096]{1,0:T(8,128)(2,1)} %param.28) | copy-start | bytes 3145732
  7.2 12.6 %copy-start.4 = (bf16[4096,128]{1,0:T(8,128)(2,1)S(1)}, bf16[4096,128]{1,0:T(8,128)(2,1)}, u32[]{:S(2)}) copy-start(bf16[4096,128]{1,0:T(8,128)(2,1)} %param.19) | copy-start | bytes 3145732
  7.2 16.2 %copy-start.12 = (f32[2]{0:T(128)S(1)}, f32[2]{0:T(128)}, u32[]{:S(2)}) copy-start(f32[2]{0:T(128)} %param.24) | copy-start | bytes 28
  9.1 32.7 %all-to-all-start = ((bf16[16,96,256]{2,1,0:T(8,128)(2,1)}), bf16[16,96,256]{2,1,0:T(8,128)(2,1)S(1)}, u32[]{:S(2)}, u32[]{:S(2)}) async-start(bf16[16,96,256]{2,1,0:T(8,128)(2,1)} %broadcast_in_dim.6), calls=%async_computation | async-start | bytes 1572864 | tf_op jit(solution)/shard_map/all_to_all | solution.py:17
  23.4 6.1 %copy-start.5 = (bf16[4096,128]{1,0:T(8,128)(2,1)S(1)}, bf16[4096,128]{1,0:T(8,128)(2,1)}, u32[]{:S(2)}) copy-start(bf16[4096,128]{1,0:T(8,128)(2,1)} %param.20) | copy-start | bytes 3145732
  46.5 0.7 copy-start.8
  46.5 2.2 copy-start.9
  46.7 3.4 %copy-start.1 = (f32[96,2,4096]{0,2,1:T(8,128)S(1)}, f32[96,2,4096]{0,2,1:T(8,128)}, u32[]{:S(2)}) copy-start(f32[96,2,4096]{0,2,1:T(8,128)} %copy.67) | copy-start | bytes 9437188
  48.7 2.0 copy-start.2
  51.2 3.1 %copy-start.3 = (bf16[4096,128]{0,1:T(8,128)(2,1)S(1)}, bf16[4096,128]{0,1:T(8,128)(2,1)}, u32[]{:S(2)}) copy-start(bf16[4096,128]{0,1:T(8,128)(2,1)} %copy.71) | copy-start | bytes 3145732
  51.2 3.1 %copy-start.10 = (f32[64]{0:T(128)S(1)}, f32[64]{0:T(128)}, u32[]{:S(2)}) copy-start(f32[64]{0:T(128)} %param.27) | copy-start | bytes 772
  54.8 26.5 %copy-start.6 = (bf16[96,256]{1,0:T(8,128)(2,1)S(1)}, bf16[96,256]{1,0:T(8,128)(2,1)}, u32[]{:S(2)}) copy-start(bf16[96,256]{1,0:T(8,128)(2,1)} %param.16) | copy-start | bytes 147460
  55.2 57.0 %copy-start.7 = (bf16[256,1024]{1,0:T(8,128)(2,1)S(1)}, bf16[256,1024]{1,0:T(8,128)(2,1)}, u32[]{:S(2)}) copy-start(bf16[256,1024]{1,0:T(8,128)(2,1)} %param.30) | copy-start | bytes 1572868
  82.0 10.0 %all-to-all-start.2 = ((f32[16,1,96]{2,1,0:T(1,128)}), f32[16,1,96]{2,1,0:T(1,128)S(1)}, u32[]{:S(2)}, u32[]{:S(2)}) async-start(f32[16,1,96]{2,1,0:T(1,128)} %broadcast_in_dim.7), calls=%async_computation.2 | async-start | bytes 16384 | tf_op jit(solution)/shard_map/all_to_all | solution.py:17
  85.3 40.4 %reduce-scatter.3.cloned.1.call-start = ((), (), s32[]{:S(2)}) async-start(), calls=%async_computation.7 | async-start | bytes 4718592 | tf_op jit(solution)/shard_map/reduce_scatter | solution.py:54
  115.3 96.8 %copy-start.11 = (bf16[1024,256]{1,0:T(8,128)(2,1)S(1)}, bf16[1024,256]{1,0:T(8,128)(2,1)}, u32[]{:S(2)}) copy-start(bf16[1024,256]{1,0:T(8,128)(2,1)} %param.31) | copy-start | bytes 1572868
  115.3 50.9 %reduce-scatter.5.cloned.1.call-start = ((), (), s32[]{:S(2)}) async-start(), calls=%async_computation.8 | async-start | bytes 1769472 | tf_op jit(solution)/shard_map/reduce_scatter | solution.py:55
  125.8 86.4 %all-gather.3.cloned.1.call-start = ((), (), s32[]{:S(2)}) async-start(), calls=%async_computation.9 | async-start | bytes 3342336 | tf_op jit(solution)/shard_map/all_gather | solution.py:130
  215.9 20.2 %all-to-all-start.4 = ((bf16[16,96,256]{2,1,0:T(8,128)(2,1)}), bf16[16,96,256]{2,1,0:T(8,128)(2,1)S(1)}, u32[]{:S(2)}, u32[]{:S(2)}) async-start(bf16[16,96,256]{2,1,0:T(8,128)(2,1)} %bitcast.19), calls=%async_computation.6 | async-start | bytes 1572864 | tf_op jit(solution)/shard_map/all_to_all | solution.py:40
Sparse Core Ops, SparseCore 0:
  115.5 10.2 reduce-scatter.2
  128.3 37.8 reduce-scatter.4
  168.6 43.4 all-gather.2
where the time goes:
time: 244 us; the launch traced here: 243 us
  waiting for transfers between devices  111 us (45%)
  blocking collectives  45.9 us (19%)
  local copies, waits for them, and re-layouts  26.8 us (11%)
  starting transfers between devices  20 us (8%)
  between operations  14 us (6%)
  other arithmetic  12.9 us (5%)
  matrix products  12.2 us (5%)
    all_gather x1, waiting for transfers between devices, local(): hidden = lax.all_gather(hidden_share, TP, axis=0, tiled=True)  44.2 us
    reduce_scatter x1, waiting for transfers between devices, scatter_pairs(): return lax.psum_scatter(parts, chips, scatter_dimension=0, tiled=True)[0]  40.4 us
    all_to_all x1, blocking collectives, sum_at_owner(): lax.all_to_all(parts, axis, split_axis=0, concat_axis=0, tiled=True)  25.8 us
    all_to_all x1, blocking collectives, sent_to_all(): lax.all_to_all(jnp.broadcast_to(array[None], (length, *array.shape)), axi...  20.1 us
    unnamed x32, local copies, waits for them, and re-layouts  19.7 us
    all_to_all x2, waiting for transfers between devices, sent_to_all(): lax.all_to_all(jnp.broadcast_to(array[None], (length, *array.shape)), axi...  14.5 us
    all_to_all x2, starting transfers between devices, sent_to_all(): lax.all_to_all(jnp.broadcast_to(array[None], (length, *array.shape)), axi...  13.3 us
    reduce_scatter x1, waiting for transfers between devices, scatter_pairs(): parts = lax.psum_scatter(parts, core, scatter_dimension=0, tiled=True)  10.4 us
  transfers between devices with their start and end apart: 6, of which 6 were waited for; matrix products, arithmetic and copies ran while one was open for 11% of the time, Pallas kernels for 0%

commit v1 on v0

v1 whole, which is shorter than its diff:
```python
import jax
import jax.numpy as jnp
from jax import lax
from jax.experimental import pallas as pl
from jax.experimental.pallas import tpu as pltpu
from jax.sharding import Mesh
from jax.sharding import PartitionSpec as P

D = 4096
HEAD_DIM = 64
EPS = 1e-06
F32 = jnp.float32
BF16 = jnp.bfloat16
TP = ("z", "c")


def attn_kernel(h0_ref, rate_ref, bias_ref, tok_ref, mg_ref, wq_ref, wk_ref, wv_ref, wg_ref, wd_ref, wb_ref, og_ref, st_hbm,
                ns_hbm, ho_ref, st, xn, kn, qn, vv, od, sem_in, sem_out):
    rows=tok_ref.shape[1]; width=tok_ref.shape[2]; parts=tok_ref.shape[0]
    nt=rows//8
    cin=pltpu.make_async_copy(st_hbm, st, sem_in); cin.start()
    ss=jnp.zeros((rows,1),F32)
    for t in range(parts):
        x=tok_ref[t].astype(F32); ss=ss+jnp.sum(x*x,axis=-1,keepdims=True)
    r=lax.rsqrt(ss/(parts*width)+EPS)
    for t in range(parts):
        xn[:,t*width:(t+1)*width]=(tok_ref[t].astype(F32)*r*mg_ref[t]).astype(BF16)
    x=xn[...]
    q=jnp.dot(x,wq_ref[...],preferred_element_type=F32)
    k=jnp.dot(x,wk_ref[...],preferred_element_type=F32)
    v=jnp.dot(x,wv_ref[...],preferred_element_type=F32)
    g=jnp.dot(x,wg_ref[...],preferred_element_type=F32)
    nt_dims=(((1,),(1,)),((),()))
    pd=lax.dot_general(x,wd_ref[...],nt_dims,preferred_element_type=F32)
    pb=lax.dot_general(x,wb_ref[...],nt_dims,preferred_element_type=F32)
    lane=lax.broadcasted_iota(jnp.int32,(rows,128),1)
    lo=lane<64
    def halves(a):
        s0=jnp.sum(jnp.where(lo,a,0.0),axis=-1,keepdims=True)
        s1=jnp.sum(jnp.where(lo,0.0,a),axis=-1,keepdims=True)
        return s0,s1
    def spread(s): return jnp.where(lo,s[0],s[1])
    qs=q*lax.rsqrt(spread(halves(q*q))+EPS)*(64**-0.5)
    ks=k*lax.rsqrt(spread(halves(k*k))+EPS)
    qn[...]=qs; kn[...]=ks; vv[...]=v
    kq=halves(qs*ks)
    hl=lax.broadcasted_iota(jnp.int32,pd.shape,1)
    h0=h0_ref[0]
    for h in range(2):
        sel=hl==h0+h
        d=jnp.sum(jnp.where(sel,pd,0.0),axis=-1,keepdims=True)+bias_ref[h]
        sp=jnp.maximum(d,0.0)+jnp.log1p(jnp.exp(-jnp.abs(d)))
        dec=jnp.exp(-rate_ref[h]*sp)
        b=jnp.sum(jnp.where(sel,pb,0.0),axis=-1,keepdims=True)
        stren=1.0/(1.0+jnp.exp(-b))
        od[h,0]=jnp.broadcast_to(dec,(rows,128))
        od[h,1]=jnp.broadcast_to(stren,(rows,128))
        od[h,2]=jnp.broadcast_to(kq[h],(rows,128))
    cin.wait()
    lane8=lax.broadcasted_iota(jnp.int32,(8,128),1)
    half8=lane8//64
    def pick(a,idx): return jnp.take_along_axis(a,idx,axis=1)
    def out_copy(bt): return pltpu.make_async_copy(st.at[pl.ds(bt*512,512),:],ns_hbm.at[pl.ds(bt*512,512),:],sem_out)
    def body(bt,_):
        r0=pl.multiple_of(bt*8,8)
        k8=kn[pl.ds(r0,8),:]; q8=qn[pl.ds(r0,8),:]; v8=vv[pl.ds(r0,8),:]
        for h in range(2):
            rec=jnp.zeros((8,128),F32); out=jnp.zeros((8,128),F32)
            S=[];K=[]
            for j in range(32):
                s=st[pl.ds(bt*512+2*j+h,8,stride=64),:]
                idx=half8+(h*64+2*j)
                ke=pick(k8,idx); qe=pick(q8,idx)
                rec=rec+s*ke; out=out+s*qe
                S.append(s);K.append(ke)
            rec=rec+pltpu.roll(rec,64,1); out=out+pltpu.roll(out,64,1)
            dec=od[h,0,pl.ds(r0,8),:]; stren=od[h,1,pl.ds(r0,8),:]; kq8=od[h,2,pl.ds(r0,8),:]
            vh=pick(v8,lane8-64*half8+h*64)
            delta=stren*(vh-dec*rec)
            od[h,3,pl.ds(r0,8),:]=dec*out+kq8*delta
            for j in range(32):
                st[pl.ds(bt*512+2*j+h,8,stride=64),:]=dec*S[j]+K[j]*delta
        @pl.when(bt>0)
        def _(): out_copy(bt-1).start()
        return 0
    lax.fori_loop(0,nt,body,0)
    o=jnp.where(lo,od[0,3],od[1,3])
    ms=spread(halves(o*o))*(1.0/64)
    ho=o*lax.rsqrt(ms+EPS)*og_ref[...]*(g/(1.0+jnp.exp(-g)))
    ho_ref[...]=ho.astype(BF16)
    out_copy(nt-1).start()
    def w(bt,_):
        out_copy(bt).wait(); return 0
    lax.fori_loop(0,nt,w,0)

def attn(tok,h0,wq,wk,wv,wg,wd,wb,rate,bias,mix_gain,out_gain,state):
    parts,rows,width=tok.shape
    mg=mix_gain.reshape(parts,1,width)
    og=jnp.tile(out_gain,2).reshape(1,128)
    heads=state.shape[1]
    st=state.reshape(rows,heads,32,128).transpose(0,2,1,3).reshape(rows*64,128)
    vm=pl.BlockSpec(memory_space=pltpu.VMEM); sm=pl.BlockSpec(memory_space=pltpu.SMEM); an=pl.BlockSpec(memory_space=pl.ANY)
    ns,ho=pl.pallas_call(attn_kernel,
        out_shape=(jax.ShapeDtypeStruct((rows*64,128),F32),jax.ShapeDtypeStruct((rows,128),BF16)),
        in_specs=[sm,sm,sm]+[vm]*9+[an],
        out_specs=(an,vm),
        scratch_shapes=[pltpu.VMEM((rows*64,128),F32),pltpu.VMEM((rows,parts*width),BF16)]+[pltpu.VMEM((rows,128),F32)]*3+[pltpu.VMEM((2,4,rows,128),F32),pltpu.SemaphoreType.DMA,pltpu.SemaphoreType.DMA],
        cost_estimate=pl.CostEstimate(flops=2*96*4096*600,bytes_accessed=12_000_000,transcendentals=50000),
        name="attn",
    )(h0,rate,bias,tok,mg,wq,wk,wv,wg,wd.T,wb.T,og,st)
    ns=ns.reshape(rows,32,heads,128).transpose(0,2,1,3).reshape(rows,heads,4096)
    return ns,ho


def shifted(array, by):
    length = lax.axis_size("z")
    return lax.ppermute(array, "z", [(i, (i + by) % length) for i in range(length)])


def other_core(array):
    return lax.ppermute(array, "c", [(0, 1), (1, 0)])


def add(*terms):
    total = terms[0].astype(F32)
    for term in terms[1:]:
        total = total + term.astype(F32)
    return total


def ring_sum(block):
    far = block(4)
    half = far.shape[0] // 2
    up = shifted(far[:half], 1)
    down = shifted(far[half:], -1)
    near, back = block(3), block(5)
    up = jnp.concatenate([add(near[:half], up).astype(BF16), near[half:]], 0)
    down = jnp.concatenate([back[:half], add(back[half:], down).astype(BF16)], 0)
    for step in (2, 1):
        up = add(block(step), shifted(up, 1)).astype(BF16)
        down = add(block(8 - step), shifted(down, -1)).astype(BF16)
    return add(block(0), shifted(up, 1), shifted(down, -1))


def ring_gather(block):
    parts = [None] * 8
    parts[0] = block
    rows = block.shape[0] // 2
    ahead = [block[:rows], block[rows:]]
    behind = [block[:rows], block[rows:]]
    for step in range(1, 4):
        behind = [shifted(piece, 1) for piece in behind]
        ahead = [shifted(piece, -1) for piece in ahead]
        parts[8 - step] = jnp.concatenate(behind, 0)
        parts[step] = jnp.concatenate(ahead, 0)
    parts[4] = jnp.concatenate([shifted(ahead[0], -1), shifted(behind[1], 1)], 0)
    return jnp.concatenate(parts, 0)


def local(
    tokens,
    state,
    w_query,
    w_key,
    w_value,
    w_gate,
    w_decay,
    w_beta,
    decay_rate,
    decay_bias,
    mix_gain,
    out_gain,
    w_out,
    ffn_gain,
    w_up,
    w_down,
):
    rows, width = tokens.shape
    z = lax.axis_index("z")
    c = lax.axis_index("c")
    tp = z * 2 + c
    hidden_half = w_up.shape[1] // 2
    up_mine = lax.dynamic_slice_in_dim(w_up, c * hidden_half, hidden_half, 1)
    up_other = other_core(lax.dynamic_slice_in_dim(w_up, (1 - c) * hidden_half, hidden_half, 1))
    down_mine = lax.dynamic_slice_in_dim(w_down, c * hidden_half, hidden_half, 0)
    down_other = other_core(lax.dynamic_slice_in_dim(w_down, (1 - c) * hidden_half, hidden_half, 0))

    everything = lax.all_gather(tokens, TP, axis=0, tiled=False)
    new_state, head_out = attn(
        everything, (tp * 2).reshape(1).astype(jnp.int32), w_query, w_key, w_value, w_gate, w_decay, w_beta,
        decay_rate, decay_bias, mix_gain, out_gain, state,
    )
    partial = jnp.dot(head_out, w_out, preferred_element_type=F32).astype(BF16)
    parts = jnp.moveaxis(partial.reshape(rows, -1, width), 1, 0)
    arrived = lax.all_to_all(parts, TP, 0, 0, tiled=True)
    resid = tokens.astype(F32) + arrived.astype(F32).sum(axis=0)
    gain = lax.dynamic_slice_in_dim(ffn_gain, tp * width, width, 0)
    squares = jnp.sum(resid * resid, axis=-1)
    all_squares = lax.all_to_all(jnp.broadcast_to(squares[None, None], (16, 1, rows)), TP, 0, 0, tiled=True)
    scaled = (resid * gain).astype(BF16)
    mine = lax.all_to_all(jnp.broadcast_to(scaled[None], (16, rows, width)), "kv", 0, 0, tiled=True)
    mine = mine.reshape(16 * rows, width)
    theirs = other_core(mine)
    up_part = (
        jnp.dot(mine, up_mine, preferred_element_type=F32) + jnp.dot(theirs, up_other, preferred_element_type=F32)
    ).astype(BF16)
    up_part = up_part.reshape(8, 2 * rows, hidden_half)

    def up_block(offset):
        return lax.dynamic_index_in_dim(up_part, lax.rem(z + offset, 8), 0, keepdims=False)

    hidden = jnp.square(jax.nn.relu(ring_sum(up_block))).astype(BF16)
    hidden = ring_gather(hidden)
    give = jnp.dot(hidden, down_other, preferred_element_type=F32).astype(BF16)
    took = other_core(give)
    down = (jnp.dot(hidden, down_mine, preferred_element_type=F32) + took.astype(F32)).astype(BF16)
    down = down.reshape(8, 2 * rows, width)
    down = lax.dynamic_slice_in_dim(jnp.concatenate([down, down], 0), lax.rem(8 - z, 8), 8, 0)
    down = lax.all_to_all(down.reshape(16, rows, width), "kv", 0, 0, tiled=True)
    down = down.astype(F32).sum(axis=0)
    square_scale = 1.0 / (jnp.sum(all_squares, axis=(0, 1)) / D + EPS)
    mixed = (resid + down * square_scale[:, None]).astype(BF16)
    return (mixed, new_state)


def solution(mesh):
    split = Mesh(mesh.devices.reshape(mesh.shape["kv"], 8, 2), ("kv", "z", "c"))
    placed = (
        P("kv", TP),
        P("kv", TP, None),
        P(None, TP),
        P(None, TP),
        P(None, TP),
        P(None, TP),
        P(),
        P(),
        P(TP),
        P(TP),
        P(),
        P(),
        P(TP, None),
        P(),
        P(TP, "kv"),
        P("kv", TP),
    )
    return jax.shard_map(
        local,
        mesh=split,
        in_specs=placed,
        out_specs=(P("kv", TP), P("kv", TP, None)),
        check_vma=False,
    )
```

time: 244 us -> 198 us (0.81)
  waiting for transfers between devices: 111 us -> 67.3 us
  starting transfers between devices: 20 us -> 48.5 us
  local copies, waits for them, and re-layouts: 26.8 us -> 5.93 us
  Pallas kernels: 0 us -> 13.7 us
  between operations: 14 us -> 0.92 us
  matrix products: 12.2 us -> 6.19 us
  other arithmetic: 12.9 us -> 9.91 us
    reduce_scatter x2 -> x0, waiting for transfers between devices: 50.8 us -> none  [the longest x1 40.4 us: scatter_pairs(): return lax.psum_scatter(parts, chips, scatter_dimension=0, tiled=True)[0]]
    all_gather x1 -> x0, waiting for transfers between devices: 44.2 us -> none  [local(): hidden = lax.all_gather(hidden_share, TP, axis=0, tiled=True)]
    ppermute x0 -> x26, starting transfers between devices: none -> 36.3 us  [the longest x22 24.5 us: shifted(): lax.ppermute(array, 'z', [(i, (i + by) % length) for i in range(length)])]
    ppermute x0 -> x26, waiting for transfers between devices: none -> 28.5 us  [the longest x22 27.6 us: shifted(): lax.ppermute(array, 'z', [(i, (i + by) % length) for i in range(length)])]
    all_to_all x2 -> x1, blocking collectives: 45.9 us -> 19.9 us  [local(): lax.all_to_all(jnp.broadcast_to(scaled[None], (16, rows, width)), 'kv', 0...]
    all_gather x0 -> x1, blocking collectives: none -> 25.2 us  [local(): everything = lax.all_gather(tokens, TP, axis=0, tiled=False)]
    all_to_all x3, waiting for transfers between devices: 16.3 us -> 38.8 us  [the longest x1 22 us: local(): arrived = lax.all_to_all(parts, TP, 0, 0, tiled=True)]
    unnamed x32 -> x25, local copies, waits for them, and re-layouts: 19.7 us -> 0.82 us
  transfers between devices with their start and end apart: 6 -> 29, of which waited for: 6 -> 14; matrix products, arithmetic and copies ran while one was open for 11% -> 5% of each run, Pallas kernels for 0% -> 0%
where the time goes in v1:
time: 198 us
  waiting for transfers between devices  67.3 us (34%)
  starting transfers between devices  48.5 us (24%)
  blocking collectives  45.1 us (23%)
  Pallas kernels  13.7 us (7%)
  other arithmetic  9.91 us (5%)
  matrix products  6.19 us (3%)
  local copies, waits for them, and re-layouts  5.93 us (3%)
    ppermute x22, waiting for transfers between devices, shifted(): lax.ppermute(array, 'z', [(i, (i + by) % length) for i in range(length)])  27.6 us
    all_gather x1, blocking collectives, local(): everything = lax.all_gather(tokens, TP, axis=0, tiled=False)  25.2 us
    ppermute x22, starting transfers between devices, shifted(): lax.ppermute(array, 'z', [(i, (i + by) % length) for i in range(length)])  24.5 us
    all_to_all x1, waiting for transfers between devices, local(): arrived = lax.all_to_all(parts, TP, 0, 0, tiled=True)  22 us
    all_to_all x1, blocking collectives, local(): lax.all_to_all(jnp.broadcast_to(scaled[None], (16, rows, width)), 'kv', 0...  19.9 us
    pallas_call x1, Pallas kernels, attn(): pl.pallas_call(attn_kernel, out_shape=(jax.ShapeDtypeStruct((rows * 64, 1...  13.7 us
    all_to_all x1, waiting for transfers between devices, local(): down = lax.all_to_all(down.reshape(16, rows, width), 'kv', 0, 0, tiled=True)  12.6 us
    ppermute x4, starting transfers between devices, other_core(): return lax.ppermute(array, 'c', [(0, 1), (1, 0)])  11.7 us
  transfers between devices with their start and end apart: 29, of which 14 were waited for; matrix products, arithmetic and copies ran while one was open for 5% of the time, Pallas kernels for 0%

profile of v1, /device:TPU:1, one launch (start us, length us, event | category | flops | bytes accessed | tf_op | source)
XLA Modules:
  0.0 197.6 jit_solution(5433445552732214819)
XLA Ops:
  0.7 25.2 %all-gather = bf16[1536,256]{1,0:T(8,128)(2,1)} all-gather(bf16[96,256]{1,0:T(8,128)(2,1)} %param.16), channel_id=2, replica_groups=mesh['kv'=16,'z'=8,'c'=2] {'z','c'}, dimensions={0}, use_global_device_ids=true | all-gather | bytes 835584 | tf_op jit(solution)/shard_map/all_gather | solution.py:188
  27.1 13.7 %attn.1 = (f32[6144,128]{1,0:T(8,128)}, bf16[96,128]{1,0:T(8,128)(2,1)}) custom-call(s32[1]{0:T(128)} %bitcast.h0_ref, f32[2]{0:T(128)} %rate_ref.1, f32[2]{0:T(128)} %bias_ref.1, bf16[16,96,256]{2,1,0:T(8,128)(2,1)} %bitcast.77, f32[16,1,256]{2,1,0:T(1,128)} %bitcast.83, bf16[4096,128]{1,0:T(8,128)(2,1)} %wq_ref.1, bf16[4096,128]{1,0:T(8,128)(2,1)} %wk_ref.1, ...), custom_call_target="tpu_custom_call" | custom-call | flops 471859200 | bytes 12000000 | tf_op jit(solution)/shard_map/attn/pallas_call | solution.py:103
  43.0 3.9 %all-to-all-start = ((bf16[16,96,256]{2,1,0:T(8,128)(2,1)}), bf16[16,96,256]{2,1,0:T(8,128)(2,1)S(1)}, u32[]{:S(2)}, u32[]{:S(2)}) async-start(bf16[16,96,256]{2,1,0:T(8,128)(2,1)} %bitcast.68), calls=%async_computation | async-start | bytes 1572864 | tf_op jit(solution)/shard_map/all_to_all | solution.py:195
  47.7 22.0 %all-to-all-done = bf16[16,96,256]{2,1,0:T(8,128)(2,1)S(1)} async-done(((bf16[16,96,256]{2,1,0:T(8,128)(2,1)}), bf16[16,96,256]{2,1,0:T(8,128)(2,1)S(1)}, u32[]{:S(2)}, u32[]{:S(2)}) %all-to-all-start) | async-done | bytes 786464 | tf_op jit(solution)/shard_map/all_to_all | solution.py:195
  70.5 19.9 %all_to_all.20 = bf16[16,96,256]{2,1,0:T(8,128)(2,1)S(1)} all-to-all(bf16[16,96,256]{2,1,0:T(8,128)(2,1)S(1)} %broadcast_in_dim.4), channel_id=1, replica_groups=mesh['kv'=16,'z'=8,'c'=2] {'kv'}, dimensions={0} | all-to-all | bytes 1572864 | tf_op jit(solution)/shard_map/all_to_all | solution.py:201
  93.7 1.5 fusion
  95.4 2.7 %collective-permute-start.6 = (bf16[96,512]{1,0:T(8,128)(2,1)S(1)}, bf16[96,512]{1,0:T(8,128)(2,1)S(1)}, u32[]{:S(2)}, u32[]{:S(2)}) collective-permute-start(bf16[96,512]{1,0:T(8,128)(2,1)S(1)} %get-tuple-element.14), channel_id=1, source_target_pairs={{0,14},{2,0},{4,2},{6,4},{8,6},{10,8},{12,10},{14,12},{1,15},{3,1}... | collective-permute-start | bytes 294920 | tf_op jit(solution)/shard_map/ppermute | solution.py:117
  98.1 2.6 %collective-permute-done.2 = bf16[96,512]{1,0:T(8,128)(2,1)S(1)} collective-permute-done((bf16[96,512]{1,0:T(8,128)(2,1)S(1)}, bf16[96,512]{1,0:T(8,128)(2,1)S(1)}, u32[]{:S(2)}, u32[]{:S(2)}) %collective-permute-start.2) | collective-permute-done | bytes 98336 | tf_op jit(solution)/shard_map/ppermute | solution.py:117
  101.5 2.1 %collective-permute-start.7 = (bf16[192,512]{1,0:T(8,128)(2,1)S(1)}, bf16[192,512]{1,0:T(8,128)(2,1)}, u32[]{:S(2)}, u32[]{:S(2)}) collective-permute-start(bf16[192,512]{1,0:T(8,128)(2,1)S(1)} %pad_maximum_fusion.1), channel_id=1, source_target_pairs={{0,14},{2,0},{4,2},{6,4},{8,6},{10,8},{12,10},{14,12},{1,15},{3,1}... | collective-permute-start | bytes 589832 | tf_op jit(solution)/shard_map/ppermute | solution.py:117
  103.6 3.8 %collective-permute-done.3 = bf16[192,512]{1,0:T(8,128)(2,1)} collective-permute-done((bf16[192,512]{1,0:T(8,128)(2,1)S(1)}, bf16[192,512]{1,0:T(8,128)(2,1)}, u32[]{:S(2)}, u32[]{:S(2)}) %collective-permute-start.3) | collective-permute-done | bytes 196640 | tf_op jit(solution)/shard_map/ppermute | solution.py:117
  107.4 1.7 fusion.5
  109.1 6.0 %collective-permute-done.4 = bf16[192,512]{1,0:T(8,128)(2,1)} collective-permute-done((bf16[192,512]{1,0:T(8,128)(2,1)}, bf16[192,512]{1,0:T(8,128)(2,1)}, u32[]{:S(2)}, u32[]{:S(2)}) %collective-permute-start.4) | collective-permute-done | bytes 196640 | tf_op jit(solution)/shard_map/ppermute | solution.py:117
  115.2 1.9 fusion.6
  117.0 1.5 collective-permute-start.5
  118.5 3.4 %collective-permute-done.8 = bf16[192,512]{1,0:T(8,128)(2,1)} collective-permute-done((bf16[192,512]{1,0:T(8,128)(2,1)}, bf16[192,512]{1,0:T(8,128)(2,1)}, u32[]{:S(2)}, u32[]{:S(2)}) %collective-permute-start.8) | collective-permute-done | bytes 196640 | tf_op jit(solution)/shard_map/ppermute | solution.py:117
  121.9 1.6 fusion.4
  124.7 3.6 %collective-permute-done.9 = bf16[192,512]{1,0:T(8,128)(2,1)} collective-permute-done((bf16[192,512]{1,0:T(8,128)(2,1)}, bf16[192,512]{1,0:T(8,128)(2,1)}, u32[]{:S(2)}, u32[]{:S(2)}) %collective-permute-start.9) | collective-permute-done | bytes 196640 | tf_op jit(solution)/shard_map/ppermute | solution.py:117
  129.5 2.5 %collective-permute-start.11 = (bf16[96,512]{1,0:T(8,128)(2,1)S(1)}, bf16[96,512]{1,0:T(8,128)(2,1)S(1)}, u32[]{:S(2)}, u32[]{:S(2)}) collective-permute-start(bf16[96,512]{1,0:T(8,128)(2,1)S(1)} %get-tuple-element.16), channel_id=1, source_target_pairs={{0,14},{2,0},{4,2},{6,4},{8,6},{10,8},{12,10},{14,12},{1,15},{3,1}... | collective-permute-start | bytes 294920 | tf_op jit(solution)/shard_map/ppermute | solution.py:117
  132.0 2.7 %collective-permute-start.10 = (bf16[96,512]{1,0:T(8,128)(2,1)S(1)}, bf16[96,512]{1,0:T(8,128)(2,1)S(1)}, u32[]{:S(2)}, u32[]{:S(2)}) collective-permute-start(bf16[96,512]{1,0:T(8,128)(2,1)S(1)} %get-tuple-element.17), channel_id=1, source_target_pairs={{0,14},{2,0},{4,2},{6,4},{8,6},{10,8},{12,10},{14,12},{1,15},{3,1}... | collective-permute-start | bytes 294920 | tf_op jit(solution)/shard_map/ppermute | solution.py:117
  134.7 6.4 %collective-permute-start.24 = (bf16[512,256]{1,0:T(8,128)(2,1)S(1)}, bf16[512,256]{1,0:T(8,128)(2,1)S(1)}, u32[]{:S(2)}, u32[]{:S(2)}) collective-permute-start(bf16[512,256]{1,0:T(8,128)(2,1)S(1)} %constant_dynamic-slice_fusion), channel_id=1, source_target_pairs={{0,1},{1,0},{2,3},{3,2},{4,5},{5,4},{6,7},{7,6},{8,9},{9,8},{10,11... | collective-permute-start | bytes 786440 | tf_op jit(solution)/shard_map/ppermute | solution.py:121
  141.1 2.7 %collective-permute-start.12 = (bf16[96,512]{1,0:T(8,128)(2,1)S(1)}, bf16[96,512]{1,0:T(8,128)(2,1)S(1)}, u32[]{:S(2)}, u32[]{:S(2)}) collective-permute-start(bf16[96,512]{1,0:T(8,128)(2,1)S(1)} %collective-permute-done.10), channel_id=1, source_target_pairs={{0,14},{2,0},{4,2},{6,4},{8,6},{10,8},{12,10},{14,12},{1,15},{3,1}... | collective-permute-start | bytes 294920 | tf_op jit(solution)/shard_map/ppermute | solution.py:117
  143.8 1.4 collective-permute-start.18
  146.5 2.7 %collective-permute-start.14 = (bf16[96,512]{1,0:T(8,128)(2,1)S(1)}, bf16[96,512]{1,0:T(8,128)(2,1)S(1)}, u32[]{:S(2)}, u32[]{:S(2)}) collective-permute-start(bf16[96,512]{1,0:T(8,128)(2,1)S(1)} %collective-permute-done.12), channel_id=1, source_target_pairs={{0,14},{2,0},{4,2},{6,4},{8,6},{10,8},{12,10},{14,12},{1,15},{3,1}... | collective-permute-start | bytes 294920 | tf_op jit(solution)/shard_map/ppermute | solution.py:117
  151.8 2.7 %collective-permute-start.16 = (bf16[96,512]{1,0:T(8,128)(2,1)S(1)}, bf16[96,512]{1,0:T(8,128)(2,1)S(1)}, u32[]{:S(2)}, u32[]{:S(2)}) collective-permute-start(bf16[96,512]{1,0:T(8,128)(2,1)S(1)} %collective-permute-done.14), channel_id=1, source_target_pairs={{0,14},{2,0},{4,2},{6,4},{8,6},{10,8},{12,10},{14,12},{1,15},{3,1}... | collective-permute-start | bytes 294920 | tf_op jit(solution)/shard_map/ppermute | solution.py:117
  156.5 4.0 %collective-permute-done.20 = bf16[96,512]{1,0:T(8,128)(2,1)S(1)} collective-permute-done((bf16[96,512]{1,0:T(8,128)(2,1)S(1)}, bf16[96,512]{1,0:T(8,128)(2,1)S(1)}, u32[]{:S(2)}, u32[]{:S(2)}) %collective-permute-start.20) | collective-permute-done | bytes 98336 | tf_op jit(solution)/shard_map/ppermute | solution.py:117
  160.6 1.5 convolution_convert_fusion.1
  162.0 4.9 %collective-permute-start.25 = (bf16[1536,256]{1,0:T(8,128)(2,1)}, bf16[1536,256]{1,0:T(8,128)(2,1)S(1)}, u32[]{:S(2)}, u32[]{:S(2)}) collective-permute-start(bf16[1536,256]{1,0:T(8,128)(2,1)} %convolution_convert_fusion.1), channel_id=1, source_target_pairs={{0,1},{1,0},{2,3},{3,2},{4,5},{5,4},{6,7},{7,6},{8,9},{9,8},{10,11... | collective-permute-start | bytes 2359304 | tf_op jit(solution)/shard_map/ppermute | solution.py:121
  168.2 4.7 %all-to-all-start.3 = ((f32[16,1,96]{2,1,0:T(1,128)}), f32[16,1,96]{2,1,0:T(1,128)}, u32[]{:S(2)}, u32[]{:S(2)}) async-start(f32[16,1,96]{2,1,0:T(1,128)} %broadcast_in_dim.5), calls=%async_computation.3 | async-start | bytes 16384 | tf_op jit(solution)/shard_map/all_to_all | solution.py:199
  172.9 1.5 fusion.1
  175.6 4.2 %all-to-all-done.3 = f32[16,1,96]{2,1,0:T(1,128)} async-done(((f32[16,1,96]{2,1,0:T(1,128)}), f32[16,1,96]{2,1,0:T(1,128)}, u32[]{:S(2)}, u32[]{:S(2)}) %all-to-all-start.3) | async-done | bytes 6176 | tf_op jit(solution)/shard_map/all_to_all | solution.py:199
  179.8 3.6 %all-to-all-start.2 = ((bf16[16,96,256]{2,1,0:T(8,128)(2,1)}), bf16[16,96,256]{2,1,0:T(8,128)(2,1)S(1)}, u32[]{:S(2)}, u32[]{:S(2)}) async-start(bf16[16,96,256]{2,1,0:T(8,128)(2,1)} %bitcast.23), calls=%async_computation.2 | async-start | bytes 1572864 | tf_op jit(solution)/shard_map/all_to_all | solution.py:219
  184.1 12.6 %all-to-all-done.2 = bf16[16,96,256]{2,1,0:T(8,128)(2,1)S(1)} async-done(((bf16[16,96,256]{2,1,0:T(8,128)(2,1)}), bf16[16,96,256]{2,1,0:T(8,128)(2,1)S(1)}, u32[]{:S(2)}, u32[]{:S(2)}) %all-to-all-start.2) | async-done | bytes 786464 | tf_op jit(solution)/shard_map/all_to_all | solution.py:219
  (84 shorter events, 21.6 us)
Async XLA Ops:
  0.6 40.3 %copy-start = (bf16[128,4096]{1,0:T(8,128)(2,1)S(1)}, bf16[128,4096]{1,0:T(8,128)(2,1)}, u32[]{:S(2)}) copy-start(bf16[128,4096]{1,0:T(8,128)(2,1)} %param.28) | copy-start | bytes 3145732
  43.0 26.8 %copy-start.4 = (bf16[96,256]{1,0:T(8,128)(2,1)S(1)}, bf16[96,256]{1,0:T(8,128)(2,1)}, u32[]{:S(2)}) copy-start(bf16[96,256]{1,0:T(8,128)(2,1)} %param.16) | copy-start | bytes 147460
  43.0 26.7 %all-to-all-start = ((bf16[16,96,256]{2,1,0:T(8,128)(2,1)}), bf16[16,96,256]{2,1,0:T(8,128)(2,1)S(1)}, u32[]{:S(2)}, u32[]{:S(2)}) async-start(bf16[16,96,256]{2,1,0:T(8,128)(2,1)} %bitcast.68), calls=%async_computation | async-start | bytes 1572864 | tf_op jit(solution)/shard_map/all_to_all | solution.py:195
  47.7 42.7 %copy-start.2 = (bf16[256,1024]{1,0:T(8,128)(2,1)S(1)}, bf16[256,1024]{1,0:T(8,128)(2,1)}, u32[]{:S(2)}) copy-start(bf16[256,1024]{1,0:T(8,128)(2,1)} %param.30) | copy-start | bytes 1572868
  90.4 3.4 %collective-permute-start = (bf16[1536,256]{1,0:T(8,128)(2,1)S(1)}, bf16[1536,256]{1,0:T(8,128)(2,1)S(1)}, u32[]{:S(2)}, u32[]{:S(2)}) collective-permute-start(bf16[1536,256]{1,0:T(8,128)(2,1)S(1)} %bitcast.75), channel_id=1, source_target_pairs={{0,1},{1,0},{2,3},{3,2},{4,5},{5,4},{6,7},{7,6},{8,9},{9,8},{10,11... | collective-permute-start | bytes 2359304 | tf_op jit(solution)/shard_map/ppermute | solution.py:121
  91.1 1.9 collective-permute-start.1
  95.3 5.3 %collective-permute-start.2 = (bf16[96,512]{1,0:T(8,128)(2,1)S(1)}, bf16[96,512]{1,0:T(8,128)(2,1)S(1)}, u32[]{:S(2)}, u32[]{:S(2)}) collective-permute-start(bf16[96,512]{1,0:T(8,128)(2,1)S(1)} %get-tuple-element.12), channel_id=1, source_target_pairs={{0,2},{2,4},{4,6},{6,8},{8,10},{10,12},{12,14},{14,0},{1,3},{3,5},... | collective-permute-start | bytes 294920 | tf_op jit(solution)/shard_map/ppermute | solution.py:117
  95.4 5.3 %collective-permute-start.6 = (bf16[96,512]{1,0:T(8,128)(2,1)S(1)}, bf16[96,512]{1,0:T(8,128)(2,1)S(1)}, u32[]{:S(2)}, u32[]{:S(2)}) collective-permute-start(bf16[96,512]{1,0:T(8,128)(2,1)S(1)} %get-tuple-element.14), channel_id=1, source_target_pairs={{0,14},{2,0},{4,2},{6,4},{8,6},{10,8},{12,10},{14,12},{1,15},{3,1}... | collective-permute-start | bytes 294920 | tf_op jit(solution)/shard_map/ppermute | solution.py:117
  100.7 6.7 %collective-permute-start.3 = (bf16[192,512]{1,0:T(8,128)(2,1)S(1)}, bf16[192,512]{1,0:T(8,128)(2,1)}, u32[]{:S(2)}, u32[]{:S(2)}) collective-permute-start(bf16[192,512]{1,0:T(8,128)(2,1)S(1)} %pad_maximum_fusion), channel_id=1, source_target_pairs={{0,2},{2,4},{4,6},{6,8},{8,10},{10,12},{12,14},{14,0},{1,3},{3,5},... | collective-permute-start | bytes 589832 | tf_op jit(solution)/shard_map/ppermute | solution.py:117
  101.5 7.6 %collective-permute-start.7 = (bf16[192,512]{1,0:T(8,128)(2,1)S(1)}, bf16[192,512]{1,0:T(8,128)(2,1)}, u32[]{:S(2)}, u32[]{:S(2)}) collective-permute-start(bf16[192,512]{1,0:T(8,128)(2,1)S(1)} %pad_maximum_fusion.1), channel_id=1, source_target_pairs={{0,14},{2,0},{4,2},{6,4},{8,6},{10,8},{12,10},{14,12},{1,15},{3,1}... | collective-permute-start | bytes 589832 | tf_op jit(solution)/shard_map/ppermute | solution.py:117
  109.1 6.0 %collective-permute-start.4 = (bf16[192,512]{1,0:T(8,128)(2,1)}, bf16[192,512]{1,0:T(8,128)(2,1)}, u32[]{:S(2)}, u32[]{:S(2)}) collective-permute-start(bf16[192,512]{1,0:T(8,128)(2,1)} %fusion.5), channel_id=1, source_target_pairs={{0,2},{2,4},{4,6},{6,8},{8,10},{10,12},{12,14},{14,0},{1,3},{3,5},... | collective-permute-start | bytes 589832 | tf_op jit(solution)/shard_map/ppermute | solution.py:117
  117.0 4.8 %collective-permute-start.8 = (bf16[192,512]{1,0:T(8,128)(2,1)}, bf16[192,512]{1,0:T(8,128)(2,1)}, u32[]{:S(2)}, u32[]{:S(2)}) collective-permute-start(bf16[192,512]{1,0:T(8,128)(2,1)} %get-tuple-element.9), channel_id=1, source_target_pairs={{0,14},{2,0},{4,2},{6,4},{8,6},{10,8},{12,10},{14,12},{1,15},{3,1}... | collective-permute-start | bytes 589832 | tf_op jit(solution)/shard_map/ppermute | solution.py:117
  117.0 7.7 %collective-permute-start.5 = (bf16[192,512]{1,0:T(8,128)(2,1)}, bf16[192,512]{1,0:T(8,128)(2,1)S(1)}, u32[]{:S(2)}, u32[]{:S(2)}) collective-permute-start(bf16[192,512]{1,0:T(8,128)(2,1)} %get-tuple-element.8), channel_id=1, source_target_pairs={{0,2},{2,4},{4,6},{6,8},{8,10},{10,12},{12,14},{14,0},{1,3},{3,5},... | collective-permute-start | bytes 589832 | tf_op jit(solution)/shard_map/ppermute | solution.py:117
  123.5 4.8 %collective-permute-start.9 = (bf16[192,512]{1,0:T(8,128)(2,1)}, bf16[192,512]{1,0:T(8,128)(2,1)}, u32[]{:S(2)}, u32[]{:S(2)}) collective-permute-start(bf16[192,512]{1,0:T(8,128)(2,1)} %fusion.4), channel_id=1, source_target_pairs={{0,14},{2,0},{4,2},{6,4},{8,6},{10,8},{12,10},{14,12},{1,15},{3,1}... | collective-permute-start | bytes 589832 | tf_op jit(solution)/shard_map/ppermute | solution.py:117
  129.5 14.2 %collective-permute-start.11 = (bf16[96,512]{1,0:T(8,128)(2,1)S(1)}, bf16[96,512]{1,0:T(8,128)(2,1)S(1)}, u32[]{:S(2)}, u32[]{:S(2)}) collective-permute-start(bf16[96,512]{1,0:T(8,128)(2,1)S(1)} %get-tuple-element.16), channel_id=1, source_target_pairs={{0,14},{2,0},{4,2},{6,4},{8,6},{10,8},{12,10},{14,12},{1,15},{3,1}... | collective-permute-start | bytes 294920 | tf_op jit(solution)/shard_map/ppermute | solution.py:117
  132.0 11.8 %collective-permute-start.17 = (bf16[96,512]{1,0:T(8,128)(2,1)S(1)}, bf16[96,512]{1,0:T(8,128)(2,1)S(1)}, u32[]{:S(2)}, u32[]{:S(2)}) collective-permute-start(bf16[96,512]{1,0:T(8,128)(2,1)S(1)} %get-tuple-element.16), channel_id=1, source_target_pairs={{0,2},{2,4},{4,6},{6,8},{8,10},{10,12},{12,14},{14,0},{1,3},{3,5},... | collective-permute-start | bytes 294920 | tf_op jit(solution)/shard_map/ppermute | solution.py:117
  132.0 9.1 %collective-permute-start.10 = (bf16[96,512]{1,0:T(8,128)(2,1)S(1)}, bf16[96,512]{1,0:T(8,128)(2,1)S(1)}, u32[]{:S(2)}, u32[]{:S(2)}) collective-permute-start(bf16[96,512]{1,0:T(8,128)(2,1)S(1)} %get-tuple-element.17), channel_id=1, source_target_pairs={{0,14},{2,0},{4,2},{6,4},{8,6},{10,8},{12,10},{14,12},{1,15},{3,1}... | collective-permute-start | bytes 294920 | tf_op jit(solution)/shard_map/ppermute | solution.py:117
  134.7 25.9 %collective-permute-start.24 = (bf16[512,256]{1,0:T(8,128)(2,1)S(1)}, bf16[512,256]{1,0:T(8,128)(2,1)S(1)}, u32[]{:S(2)}, u32[]{:S(2)}) collective-permute-start(bf16[512,256]{1,0:T(8,128)(2,1)S(1)} %constant_dynamic-slice_fusion), channel_id=1, source_target_pairs={{0,1},{1,0},{2,3},{3,2},{4,5},{5,4},{6,7},{7,6},{8,9},{9,8},{10,11... | collective-permute-start | bytes 786440 | tf_op jit(solution)/shard_map/ppermute | solution.py:121
  141.1 5.5 %collective-permute-start.21 = (bf16[96,512]{1,0:T(8,128)(2,1)S(1)}, bf16[96,512]{1,0:T(8,128)(2,1)S(1)}, u32[]{:S(2)}, u32[]{:S(2)}) collective-permute-start(bf16[96,512]{1,0:T(8,128)(2,1)S(1)} %get-tuple-element.17), channel_id=1, source_target_pairs={{0,2},{2,4},{4,6},{6,8},{8,10},{10,12},{12,14},{14,0},{1,3},{3,5},... | collective-permute-start | bytes 294920 | tf_op jit(solution)/shard_map/ppermute | solution.py:117
  141.1 5.5 %collective-permute-start.12 = (bf16[96,512]{1,0:T(8,128)(2,1)S(1)}, bf16[96,512]{1,0:T(8,128)(2,1)S(1)}, u32[]{:S(2)}, u32[]{:S(2)}) collective-permute-start(bf16[96,512]{1,0:T(8,128)(2,1)S(1)} %collective-permute-done.10), channel_id=1, source_target_pairs={{0,14},{2,0},{4,2},{6,4},{8,6},{10,8},{12,10},{14,12},{1,15},{3,1}... | collective-permute-start | bytes 294920 | tf_op jit(solution)/shard_map/ppermute | solution.py:117
  143.7 5.6 %collective-permute-start.13 = (bf16[96,512]{1,0:T(8,128)(2,1)S(1)}, bf16[96,512]{1,0:T(8,128)(2,1)S(1)}, u32[]{:S(2)}, u32[]{:S(2)}) collective-permute-start(bf16[96,512]{1,0:T(8,128)(2,1)S(1)} %collective-permute-done.11), channel_id=1, source_target_pairs={{0,14},{2,0},{4,2},{6,4},{8,6},{10,8},{12,10},{14,12},{1,15},{3,1}... | collective-permute-start | bytes 294920 | tf_op jit(solution)/shard_map/ppermute | solution.py:117
  143.8 5.6 %collective-permute-start.18 = (bf16[96,512]{1,0:T(8,128)(2,1)S(1)}, bf16[96,512]{1,0:T(8,128)(2,1)S(1)}, u32[]{:S(2)}, u32[]{:S(2)}) collective-permute-start(bf16[96,512]{1,0:T(8,128)(2,1)S(1)} %collective-permute-done.17), channel_id=1, source_target_pairs={{0,2},{2,4},{4,6},{6,8},{8,10},{10,12},{12,14},{14,0},{1,3},{3,5},... | collective-permute-start | bytes 294920 | tf_op jit(solution)/shard_map/ppermute | solution.py:117
  146.5 5.2 %collective-permute-start.22 = (bf16[96,512]{1,0:T(8,128)(2,1)S(1)}, bf16[96,512]{1,0:T(8,128)(2,1)S(1)}, u32[]{:S(2)}, u32[]{:S(2)}) collective-permute-start(bf16[96,512]{1,0:T(8,128)(2,1)S(1)} %collective-permute-done.21), channel_id=1, source_target_pairs={{0,2},{2,4},{4,6},{6,8},{8,10},{10,12},{12,14},{14,0},{1,3},{3,5},... | collective-permute-start | bytes 294920 | tf_op jit(solution)/shard_map/ppermute | solution.py:117
  146.5 5.2 %collective-permute-start.14 = (bf16[96,512]{1,0:T(8,128)(2,1)S(1)}, bf16[96,512]{1,0:T(8,128)(2,1)S(1)}, u32[]{:S(2)}, u32[]{:S(2)}) collective-permute-start(bf16[96,512]{1,0:T(8,128)(2,1)S(1)} %collective-permute-done.12), channel_id=1, source_target_pairs={{0,14},{2,0},{4,2},{6,4},{8,6},{10,8},{12,10},{14,12},{1,15},{3,1}... | collective-permute-start | bytes 294920 | tf_op jit(solution)/shard_map/ppermute | solution.py:117
  149.3 6.0 %collective-permute-start.15 = (bf16[96,512]{1,0:T(8,128)(2,1)S(1)}, bf16[96,512]{1,0:T(8,128)(2,1)S(1)}, u32[]{:S(2)}, u32[]{:S(2)}) collective-permute-start(bf16[96,512]{1,0:T(8,128)(2,1)S(1)} %collective-permute-done.13), channel_id=1, source_target_pairs={{0,14},{2,0},{4,2},{6,4},{8,6},{10,8},{12,10},{14,12},{1,15},{3,1}... | collective-permute-start | bytes 294920 | tf_op jit(solution)/shard_map/ppermute | solution.py:117
  149.5 5.8 %collective-permute-start.19 = (bf16[96,512]{1,0:T(8,128)(2,1)S(1)}, bf16[96,512]{1,0:T(8,128)(2,1)S(1)}, u32[]{:S(2)}, u32[]{:S(2)}) collective-permute-start(bf16[96,512]{1,0:T(8,128)(2,1)S(1)} %collective-permute-done.18), channel_id=1, source_target_pairs={{0,2},{2,4},{4,6},{6,8},{8,10},{10,12},{12,14},{14,0},{1,3},{3,5},... | collective-permute-start | bytes 294920 | tf_op jit(solution)/shard_map/ppermute | solution.py:117
  151.8 8.7 %collective-permute-start.23 = (bf16[96,512]{1,0:T(8,128)(2,1)S(1)}, bf16[96,512]{1,0:T(8,128)(2,1)S(1)}, u32[]{:S(2)}, u32[]{:S(2)}) collective-permute-start(bf16[96,512]{1,0:T(8,128)(2,1)S(1)} %collective-permute-done.22), channel_id=1, source_target_pairs={{0,2},{2,4},{4,6},{6,8},{8,10},{10,12},{12,14},{14,0},{1,3},{3,5},... | collective-permute-start | bytes 294920 | tf_op jit(solution)/shard_map/ppermute | solution.py:117
  151.8 4.7 %collective-permute-start.16 = (bf16[96,512]{1,0:T(8,128)(2,1)S(1)}, bf16[96,512]{1,0:T(8,128)(2,1)S(1)}, u32[]{:S(2)}, u32[]{:S(2)}) collective-permute-start(bf16[96,512]{1,0:T(8,128)(2,1)S(1)} %collective-permute-done.14), channel_id=1, source_target_pairs={{0,14},{2,0},{4,2},{6,4},{8,6},{10,8},{12,10},{14,12},{1,15},{3,1}... | collective-permute-start | bytes 294920 | tf_op jit(solution)/shard_map/ppermute | solution.py:117
  155.3 5.2 %collective-permute-start.20 = (bf16[96,512]{1,0:T(8,128)(2,1)S(1)}, bf16[96,512]{1,0:T(8,128)(2,1)S(1)}, u32[]{:S(2)}, u32[]{:S(2)}) collective-permute-start(bf16[96,512]{1,0:T(8,128)(2,1)S(1)} %collective-permute-done.19), channel_id=1, source_target_pairs={{0,2},{2,4},{4,6},{6,8},{8,10},{10,12},{12,14},{14,0},{1,3},{3,5},... | collective-permute-start | bytes 294920 | tf_op jit(solution)/shard_map/ppermute | solution.py:117
  162.0 10.8 %collective-permute-start.25 = (bf16[1536,256]{1,0:T(8,128)(2,1)}, bf16[1536,256]{1,0:T(8,128)(2,1)S(1)}, u32[]{:S(2)}, u32[]{:S(2)}) collective-permute-start(bf16[1536,256]{1,0:T(8,128)(2,1)} %convolution_convert_fusion.1), channel_id=1, source_target_pairs={{0,1},{1,0},{2,3},{3,2},{4,5},{5,4},{6,7},{7,6},{8,9},{9,8},{10,11... | collective-permute-start | bytes 2359304 | tf_op jit(solution)/shard_map/ppermute | solution.py:121
  168.2 11.6 %all-to-all-start.3 = ((f32[16,1,96]{2,1,0:T(1,128)}), f32[16,1,96]{2,1,0:T(1,128)}, u32[]{:S(2)}, u32[]{:S(2)}) async-start(f32[16,1,96]{2,1,0:T(1,128)} %broadcast_in_dim.5), calls=%async_computation.3 | async-start | bytes 16384 | tf_op jit(solution)/shard_map/all_to_all | solution.py:199
  179.8 17.0 %all-to-all-start.2 = ((bf16[16,96,256]{2,1,0:T(8,128)(2,1)}), bf16[16,96,256]{2,1,0:T(8,128)(2,1)S(1)}, u32[]{:S(2)}, u32[]{:S(2)}) async-start(bf16[16,96,256]{2,1,0:T(8,128)(2,1)} %bitcast.23), calls=%async_computation.2 | async-start | bytes 1572864 | tf_op jit(solution)/shard_map/all_to_all | solution.py:219
  (3 other events, 52.8 us)

commit v2 on v0

v2 whole, which is shorter than its diff:
```python
import jax
import jax.numpy as jnp
from jax import lax
from jax.experimental import pallas as pl
from jax.experimental.pallas import tpu as pltpu
from jax.sharding import Mesh
from jax.sharding import PartitionSpec as P

D = 4096
EPS = 1e-06
F32 = jnp.float32
BF16 = jnp.bfloat16
TP = ("z", "c")
KV = ("y", "x")
EVERYWHERE = ("y", "x", "z", "c")
PAD = 8


def attn_kernel(h0_ref, rate_ref, bias_ref, tok_ref, mg_ref, wq_hbm, wk_hbm, wv_hbm, wg_hbm, wd_hbm, wb_hbm, wo_hbm, og_ref, st_hbm,
                ns_hbm, keep_ref, give_ref, wo, w4, w2, st, xn, vv, od, ex, e2, sem_w, sem_in, sem_out):
    rows = tok_ref.shape[1]
    width = tok_ref.shape[2]
    parts = tok_ref.shape[0]
    nt = rows // 8
    loads = [pltpu.make_async_copy(src, w4.at[i], sem_w.at[i]) for i, src in enumerate((wq_hbm, wk_hbm, wv_hbm, wg_hbm))]
    loads += [pltpu.make_async_copy(src, w2.at[i], sem_w.at[4 + i]) for i, src in enumerate((wd_hbm, wb_hbm))]
    loads += [pltpu.make_async_copy(wo_hbm, wo, sem_w.at[6])]
    cin = pltpu.make_async_copy(st_hbm, st, sem_in)
    for i in (1, 0, 4, 5, 2):
        loads[i].start()
    cin.start()
    loads[3].start()
    loads[6].start()
    ei = lax.broadcasted_iota(jnp.int32, e2.shape, 0)
    ec = lax.broadcasted_iota(jnp.int32, e2.shape, 1)
    e2[...] = jnp.where((ei & 63) == (ec >> 6), 1.0, 0.0).astype(BF16)
    ss = jnp.zeros((rows, width), F32)
    for t in range(parts):
        x = tok_ref[t].astype(F32)
        ss = ss + x * x
    r = lax.rsqrt(jnp.sum(ss, axis=-1, keepdims=True) / (parts * width) + EPS)
    for t in range(parts):
        xn[:, t * width:(t + 1) * width] = (tok_ref[t].astype(F32) * r * mg_ref[t]).astype(BF16)
    x = xn[...]

    def proj(i):
        loads[i].wait()
        return jnp.dot(x, w4[i], preferred_element_type=F32)

    lane = lax.broadcasted_iota(jnp.int32, (rows, 128), 1)
    lo = lane < 64

    def halves(a):
        s0 = jnp.sum(jnp.where(lo, a, 0.0), axis=-1, keepdims=True)
        s1 = jnp.sum(jnp.where(lo, 0.0, a), axis=-1, keepdims=True)
        return s0, s1

    def spread(s):
        return jnp.where(lo, s[0], s[1])

    def expand(a, slot):
        hi = a.astype(BF16).astype(F32)
        low = a - hi
        for h in range(2):
            if h == 0:
                both = jnp.where(lo, hi, pltpu.roll(low, 64, 1))
            else:
                both = jnp.where(lo, pltpu.roll(hi, 64, 1), low)
            ex[slot + h] = jnp.dot(both.astype(BF16), e2[...], preferred_element_type=F32)

    k = proj(1)
    ks = k * lax.rsqrt(spread(halves(k * k)) + EPS)
    expand(ks, 0)
    q = proj(0)
    qs = q * lax.rsqrt(spread(halves(q * q)) + EPS) * (64 ** -0.5)
    expand(qs, 2)
    nt_dims = (((1,), (1,)), ((), ()))
    loads[4].wait()
    loads[5].wait()
    pd = lax.dot_general(x, w2[0], nt_dims, preferred_element_type=F32)
    pb = lax.dot_general(x, w2[1], nt_dims, preferred_element_type=F32)
    v = proj(2)
    vr = pltpu.roll(v, 64, 1)
    vv[0] = jnp.where(lo, v, vr)
    vv[1] = jnp.where(lo, vr, v)
    kq = halves(qs * ks)
    hl = lax.broadcasted_iota(jnp.int32, pd.shape, 1)
    h0 = h0_ref[0]
    for h in range(2):
        sel = hl == h0 + h
        d = jnp.sum(jnp.where(sel, pd, 0.0), axis=-1, keepdims=True) + bias_ref[h]
        sp = jnp.maximum(d, 0.0) + jnp.log1p(jnp.exp(-jnp.abs(d)))
        dec = jnp.exp(-rate_ref[h] * sp)
        b = jnp.sum(jnp.where(sel, pb, 0.0), axis=-1, keepdims=True)
        stren = 1.0 / (1.0 + jnp.exp(-b))
        od[h, 0] = jnp.broadcast_to(dec, (rows, 128))
        od[h, 1] = jnp.broadcast_to(stren, (rows, 128))
        od[h, 2] = jnp.broadcast_to(kq[h], (rows, 128))
    cin.wait()

    def out_copy(bt):
        return pltpu.make_async_copy(st.at[pl.ds(bt * 512, 512), :], ns_hbm.at[pl.ds(bt * 512, 512), :], sem_out)

    def body(bt, _):
        r0 = pl.multiple_of(bt * 8, 8)
        for h in range(2):
            rec = jnp.zeros((8, 128), F32)
            out = jnp.zeros((8, 128), F32)
            terms = []
            for j in range(32):
                s = st[pl.ds(bt * 512 + 2 * j + h, 8, stride=64), :]
                ke = ex[h, pl.ds(r0, 8), j * 128:(j + 1) * 128]
                qe = ex[2 + h, pl.ds(r0, 8), j * 128:(j + 1) * 128]
                rec = rec + s * ke
                out = out + s * qe
                terms.append(s)
            rec = rec + pltpu.roll(rec, 64, 1)
            out = out + pltpu.roll(out, 64, 1)
            dec = od[h, 0, pl.ds(r0, 8), :]
            stren = od[h, 1, pl.ds(r0, 8), :]
            kq8 = od[h, 2, pl.ds(r0, 8), :]
            delta = stren * (vv[h, pl.ds(r0, 8), :] - dec * rec)
            od[h, 3, pl.ds(r0, 8), :] = dec * out + kq8 * delta
            for j in range(32):
                ke = ex[h, pl.ds(r0, 8), j * 128:(j + 1) * 128]
                st[pl.ds(bt * 512 + 2 * j + h, 8, stride=64), :] = dec * terms[j] + ke * delta

        @pl.when(bt > 0)
        def _():
            out_copy(bt - 1).start()

        return 0

    lax.fori_loop(0, nt, body, 0)
    g = proj(3)
    o = jnp.where(lo, od[0, 3], od[1, 3])
    ms = spread(halves(o * o)) * (1.0 / 64)
    gain = jnp.concatenate([og_ref[...], og_ref[...]], axis=1)
    ho = o * lax.rsqrt(ms + EPS) * gain * (g / (1.0 + jnp.exp(-g)))
    head_out = ho.astype(BF16)
    loads[6].wait()
    core = h0_ref[1]
    for i in range(keep_ref.shape[0]):
        for ref, side in ((give_ref, 1 - core), (keep_ref, core)):
            cols = wo[:, pl.ds(pl.multiple_of((2 * i + side) * width, width), width)]
            ref[i] = jnp.dot(head_out, cols, preferred_element_type=F32).astype(BF16)
    out_copy(nt - 1).start()

    def finish(bt, _):
        out_copy(bt).wait()
        return 0

    lax.fori_loop(0, nt, finish, 0)


def attn(tok, h0, wq, wk, wv, wg, wd, wb, wo, rate, bias, mix_gain, out_gain, state):
    parts, rows, width = tok.shape
    mg = mix_gain.reshape(parts, 1, width)
    heads = state.shape[1]
    st = state.reshape(rows, heads, 32, 128).transpose(0, 2, 1, 3).reshape(rows * 64, 128)
    vm = pl.BlockSpec(memory_space=pltpu.VMEM)
    sm = pl.BlockSpec(memory_space=pltpu.SMEM)
    an = pl.BlockSpec(memory_space=pl.ANY)
    ns, keep, give = pl.pallas_call(
        attn_kernel,
        out_shape=(jax.ShapeDtypeStruct((rows * 64, 128), F32), jax.ShapeDtypeStruct((8, rows, width), BF16), jax.ShapeDtypeStruct((8, rows, width), BF16)),
        in_specs=[sm, sm, sm, vm, vm] + [an] * 7 + [vm, an],
        out_specs=(an, vm, vm),
        scratch_shapes=[
            pltpu.VMEM(wo.shape, BF16),
            pltpu.VMEM((4,) + wq.shape, BF16),
            pltpu.VMEM((2,) + wd.shape[::-1], BF16),
            pltpu.VMEM((rows * 64, 128), F32),
            pltpu.VMEM((rows, parts * width), BF16),
            pltpu.VMEM((2, rows, 128), F32),
            pltpu.VMEM((2, 4, rows, 128), F32),
            pltpu.VMEM((4, rows, 4096), F32),
            pltpu.VMEM((128, 4096), BF16),
            pltpu.SemaphoreType.DMA((7,)),
            pltpu.SemaphoreType.DMA,
            pltpu.SemaphoreType.DMA,
        ],
        compiler_params=pltpu.CompilerParams(vmem_limit_bytes=56 * 1024 * 1024),
        cost_estimate=pl.CostEstimate(flops=2 * 96 * 4096 * 600, bytes_accessed=12_000_000, transcendentals=50000),
        name="attn",
    )(h0, rate, bias, tok, mg, wq, wk, wv, wg, wd.T, wb.T, wo, out_gain.reshape(1, 64), st)
    ns = ns.reshape(rows, 32, heads, 128).transpose(0, 2, 1, 3).reshape(rows, heads, 4096)
    return ns, keep, give


VM = pl.BlockSpec(memory_space=pltpu.VMEM)
SM = pl.BlockSpec(memory_space=pltpu.SMEM)


def shifted(array, by, axis="z"):
    length = lax.axis_size(axis)
    return lax.ppermute(array, axis, [(i, (i + by) % length) for i in range(length)])


def other_core(array):
    return lax.ppermute(array, "c", [(0, 1), (1, 0)])


def out_kernel(tok_ref, gain_ref, parts_ref, resid_ref, send_ref):
    rows, width = tok_ref.shape
    acc = tok_ref[...].astype(F32)
    for i in range(parts_ref.shape[0]):
        acc = acc + parts_ref[i].astype(F32)
    resid_ref[...] = acc
    squares = jnp.sum(acc * acc, axis=-1, keepdims=True)
    eye = lax.broadcasted_iota(jnp.int32, (rows, 128), 0) == lax.broadcasted_iota(jnp.int32, (rows, 128), 1)
    flat = jnp.sum(jnp.where(eye, squares, 0.0), axis=0, keepdims=True)
    scaled = (acc * gain_ref[...]).astype(BF16)
    extra = jnp.broadcast_to(flat, (PAD, 128)).astype(BF16)
    blank = jnp.zeros((PAD, width - 128), BF16)
    for i in range(send_ref.shape[0]):
        send_ref[i, :rows, :] = scaled
        send_ref[i, rows:, :128] = extra
        send_ref[i, rows:, 128:] = blank


def residual(tokens, gain, parts):
    rows, width = tokens.shape
    return pl.pallas_call(
        out_kernel,
        out_shape=(jax.ShapeDtypeStruct((rows, width), F32), jax.ShapeDtypeStruct((16, rows + PAD, width), BF16)),
        in_specs=[VM] * 3,
        out_specs=(VM, VM),
        compiler_params=pltpu.CompilerParams(vmem_limit_bytes=16 * 1024 * 1024),
        cost_estimate=pl.CostEstimate(flops=1_000_000, bytes_accessed=2_000_000, transcendentals=0),
        name="out",
    )(tokens, gain, parts)


def up_kernel(z_ref, mine_ref, other_ref, wm_ref, wo_ref, *outs):
    rows = mine_ref.shape[1] - PAD
    width = mine_ref.shape[2]
    for o in (4, 3, 5, 2, 6, 1, 7, 0):
        at = (z_ref[0] + o) & 7
        own = mine_ref[pl.ds(2 * at, 2)]
        his = other_ref[pl.ds(2 * at, 2)]
        outs[o][: 2 * rows, :] = (
            jnp.dot(own[:, :rows].reshape(2 * rows, width), wm_ref[...], preferred_element_type=F32)
            + jnp.dot(his[:, :rows].reshape(2 * rows, width), wo_ref[...], preferred_element_type=F32)
        ).astype(BF16)
        squares = own[:, rows:, :128].astype(F32) + his[:, rows:, :128].astype(F32)
        outs[o][2 * rows :, :128] = squares[0].astype(BF16)
        outs[o][2 * rows :, 128:256] = squares[1].astype(BF16)
        outs[o][2 * rows :, 256:] = jnp.zeros((PAD, outs[o].shape[1] - 256), BF16)


def up_product(z, mine, other, w_mine, w_other):
    rows = mine.shape[1] - PAD
    return pl.pallas_call(
        up_kernel,
        out_shape=tuple(jax.ShapeDtypeStruct((2 * rows + PAD, w_mine.shape[1]), BF16) for _ in range(8)),
        in_specs=[SM] + [VM] * 4,
        out_specs=tuple([VM] * 8),
        compiler_params=pltpu.CompilerParams(vmem_limit_bytes=24 * 1024 * 1024),
        cost_estimate=pl.CostEstimate(flops=2 * 1536 * 512 * 512, bytes_accessed=4_000_000, transcendentals=0),
        name="up",
    )(z.reshape(1), mine, other, w_mine, w_other)


def hidden_kernel(a_ref, b_ref, c_ref, out_ref):
    total = a_ref[...].astype(F32) + b_ref[...].astype(F32) + c_ref[...].astype(F32)
    both = out_ref.shape[0]
    rows = both // 2
    eye = lax.broadcasted_iota(jnp.int32, (rows, 128), 0) == lax.broadcasted_iota(jnp.int32, (rows, 128), 1)
    for b in range(2):
        flat = total[both : both + 1, b * 128 : (b + 1) * 128]
        squares = jnp.sum(jnp.where(eye, flat, 0.0), axis=1, keepdims=True)
        up = jnp.maximum(total[b * rows : (b + 1) * rows], 0.0)
        out_ref[b * rows : (b + 1) * rows, :] = (up * up / (squares / D + EPS)).astype(BF16)


def finish_hidden(first, second, third):
    return pl.pallas_call(
        hidden_kernel,
        out_shape=jax.ShapeDtypeStruct((first.shape[0] - PAD, first.shape[1]), BF16),
        in_specs=[VM] * 3,
        out_specs=VM,
        compiler_params=pltpu.CompilerParams(vmem_limit_bytes=16 * 1024 * 1024),
        cost_estimate=pl.CostEstimate(flops=1_000_000, bytes_accessed=800_000, transcendentals=0),
        name="hidden",
    )(first, second, third)


def add(one, two):
    return (one.astype(F32) + two.astype(F32)).astype(BF16)


def ring_sum(blocks):
    ahead = blocks[4]
    back = blocks[5]
    ahead = add(blocks[3], shifted(ahead, 1))
    for step in (2, 1):
        ahead = add(blocks[step], shifted(ahead, 1))
        back = add(blocks[8 - step], shifted(back, -1))
    return blocks[0], shifted(ahead, 1), shifted(back, -1)


def ring_gather(block, *after):
    parts = [None] * 8
    parts[0] = block
    half = block.shape[0] // 2
    ahead = behind = block
    for step in range(1, 4):
        if after[step - 1] is not None:
            ahead, behind, _ = lax.optimization_barrier((ahead, behind, after[step - 1]))
        behind = shifted(behind, 1)
        ahead = shifted(ahead, -1)
        parts[8 - step] = behind
        parts[step] = ahead
    ahead, behind, _ = lax.optimization_barrier((ahead, behind, after[3]))
    low = shifted(ahead[:half], -1)
    high = shifted(behind[half:], 1)
    parts[4:5] = [low, high]
    return parts


def down_kernel(c_ref, mine_ref, other_ref, *refs):
    weights, out_ref = refs[:-1], refs[-1]
    rows = out_ref.shape[1]
    half = mine_ref.shape[1]
    flip = jnp.broadcast_to(c_ref[0], mine_ref.shape) > 0
    mine = mine_ref[...].astype(F32)
    other = other_ref[...].astype(F32)
    low = jnp.where(flip, other, mine).astype(BF16)
    high = jnp.where(flip, mine, other).astype(BF16)
    for o in range(8):
        if o == 4:
            top, bottom = weights[4][...], weights[5][...]
        else:
            ref = weights[o] if o < 4 else weights[o + 1]
            top, bottom = ref[:half, :], ref[half:, :]
        out = jnp.dot(low, top, preferred_element_type=F32) + jnp.dot(high, bottom, preferred_element_type=F32)
        out_ref[2 * o] = out[:rows].astype(BF16)
        out_ref[2 * o + 1] = out[rows:].astype(BF16)


def down_product(c, mine, other, weights):
    rows = mine.shape[0] // 2
    width = weights[0].shape[1]
    return pl.pallas_call(
        down_kernel,
        out_shape=jax.ShapeDtypeStruct((16, rows, width), BF16),
        in_specs=[SM] + [VM] * 11,
        out_specs=VM,
        compiler_params=pltpu.CompilerParams(vmem_limit_bytes=24 * 1024 * 1024),
        cost_estimate=pl.CostEstimate(flops=2 * 192 * 1024 * 2048, bytes_accessed=6_000_000, transcendentals=0),
        name="down",
    )(c.reshape(1), mine, other, *weights)


def layer(
    tokens,
    state,
    w_query,
    w_key,
    w_value,
    w_gate,
    w_decay,
    w_beta,
    decay_rate,
    decay_bias,
    mix_gain,
    out_gain,
    w_out,
    ffn_gain,
    w_up,
    w_down,
):
    _, width = tokens.shape
    _, _, z, c = (lax.axis_index(axis).astype(jnp.int32) for axis in EVERYWHERE)
    tp = z * 2 + c
    half = w_up.shape[1] // 2
    everything = lax.all_gather(tokens, TP, axis=0, tiled=False)
    up_mine = lax.dynamic_slice_in_dim(w_up, c * half, half, 1)
    up_other = other_core(lax.dynamic_slice_in_dim(w_up, (1 - c) * half, half, 1))
    gain = lax.dynamic_slice_in_dim(ffn_gain, tp * width, width, 0).reshape(1, width)
    everything, up_other = lax.optimization_barrier((everything, up_other))
    new_state, keep, give = attn(
        everything, jnp.stack([tp * 2, c]), w_query, w_key, w_value, w_gate, w_decay, w_beta, w_out,
        decay_rate, decay_bias, mix_gain, out_gain, state,
    )
    took = other_core(give)
    parts = lax.all_to_all(add(keep, took), "z", 0, 0, tiled=True)
    resid, send = residual(tokens, gain, parts)
    mine = lax.all_to_all(send, KV, 0, 0, tiled=True)
    theirs = other_core(mine)
    blocks = up_product(z, mine, theirs, up_mine, up_other)
    down_weights = ring_gather(w_down, None, everything, parts, mine)
    hidden = finish_hidden(*ring_sum(blocks))
    down = down_product(c, hidden, other_core(hidden), down_weights)
    down = lax.all_to_all(down, KV, 0, 0, tiled=True)
    down = down.astype(F32).sum(axis=0).astype(BF16)
    routes = [
        (((2 * o + b) * 8 + s) * 2 + k, ((2 * s + b) * 8 + (s + o) % 8) * 2 + k)
        for o in range(8) for b in range(2) for s in range(8) for k in range(2)
    ]
    down = lax.ppermute(down, EVERYWHERE, routes)
    mixed = (resid + down.astype(F32)).astype(BF16)
    return (mixed, new_state)


def solution(mesh):
    split = Mesh(mesh.devices.reshape(4, 4, 8, 2), EVERYWHERE)
    placed = (
        P(KV, TP),
        P(KV, TP, None),
        P(None, TP),
        P(None, TP),
        P(None, TP),
        P(None, TP),
        P(),
        P(),
        P(TP),
        P(TP),
        P(),
        P(),
        P(TP, None),
        P(),
        P(TP, KV),
        P(KV, TP),
    )
    return jax.shard_map(
        layer,
        mesh=split,
        in_specs=placed,
        out_specs=(P(KV, TP), P(KV, TP, None)),
        check_vma=False,
    )
```

time: 244 us -> 181 us (0.74)
  the two profiles are of different devices: /device:TPU:1 before, /device:TPU:56 now
where the time goes in v2:
time: 181 us; the launch traced here: 180 us
  waiting for transfers between devices  74.7 us (41%)
  blocking collectives  56.3 us (31%)
  starting transfers between devices  28.8 us (16%)
  Pallas kernels  14.2 us (8%)
  other arithmetic  3.49 us (2%)
  local copies, waits for them, and re-layouts  1.87 us (1%)
    ppermute x15, waiting for transfers between devices, shifted(): lax.ppermute(array, axis, [(i, (i + by) % length) for i in range(length)])  51.8 us
    all_gather x1, blocking collectives, layer(): everything = lax.all_gather(tokens, TP, axis=0, tiled=False)  21.6 us
    all_to_all x1, blocking collectives, layer(): mine = lax.all_to_all(send, KV, 0, 0, tiled=True)  18.3 us
    all_to_all x1, blocking collectives, layer(): down = lax.all_to_all(down, KV, 0, 0, tiled=True)  16.4 us
    ppermute x15, starting transfers between devices, shifted(): lax.ppermute(array, axis, [(i, (i + by) % length) for i in range(length)])  16.3 us
    all_to_all x1, waiting for transfers between devices, layer(): parts = lax.all_to_all(add(keep, took), 'z', 0, 0, tiled=True)  13 us
    pallas_call x1, Pallas kernels, attn(): pl.pallas_call(attn_kernel, out_shape=(jax.ShapeDtypeStruct((rows * 64, 1...  11.9 us
    ppermute x1, waiting for transfers between devices, layer(): down = lax.ppermute(down, EVERYWHERE, routes)  8.26 us
  transfers between devices with their start and end apart: 21, of which 14 were waited for; matrix products, arithmetic and copies ran while one was open for 1% of the time, Pallas kernels for 1%

profile of v2, /device:TPU:56, one launch (start us, length us, event | category | flops | bytes accessed | tf_op | source)
XLA Modules:
  0.0 180.2 jit_solution(15886118740657946741)
XLA Ops:
  0.6 1.1 constant_dynamic-slice_fusion
  1.8 0.7 pad_add_fusion.h0_ref
  2.5 21.6 %all-gather = bf16[1536,256]{1,0:T(8,128)(2,1)} all-gather(bf16[96,256]{1,0:T(8,128)(2,1)} %tok_ref.1), channel_id=2, replica_groups=mesh['y'=4,'x'=4,'z'=8,'c'=2] {'z','c'}, dimensions={0}, use_global_device_ids=true | all-gather | bytes 835584 | tf_op jit(solution)/shard_map/all_gather | solution.py:378
  24.1 11.9 %attn.1 = (f32[6144,128]{1,0:T(8,128)}, bf16[8,96,256]{2,1,0:T(8,128)(2,1)}, bf16[8,96,256]{2,1,0:T(8,128)(2,1)}) custom-call(s32[2]{0:T(128)} %pad_add_fusion.h0_ref, f32[2]{0:T(128)} %rate_ref.1, f32[2]{0:T(128)} %bias_ref.1, bf16[16,96,256]{2,1,0:T(8,128)(2,1)} %bitcast.21, f32[16,1,256]{2,1,0:T(1,128)} %bitcast.24, bf16[4096,128]{1,0:T(8,128)(2,1)} %wq_hbm.1, ...), custom_call_target="tpu_custom_call" | custom-call | flops 471859200 | bytes 12000000 | tf_op jit(solution)/shard_map/attn/pallas_call | solution.py:164
  36.5 1.6 collective-permute-done.1
  38.1 1.8 %add_convert_fusion = bf16[8,96,256]{2,1,0:T(8,128)(2,1)} fusion(bf16[8,96,256]{2,1,0:T(8,128)(2,1)S(1)} %collective-permute-done.1, bf16[8,96,256]{2,1,0:T(8,128)(2,1)} %get-tuple-element.24), kind=kLoop, calls=%fused_computation | loop fusion | flops 786432 | bytes 1179648 | tf_op jit(solution)/shard_map/convert_element_type | solution.py:290
  39.9 5.9 %all-to-all-start = ((bf16[8,96,256]{2,1,0:T(8,128)(2,1)}), bf16[8,96,256]{2,1,0:T(8,128)(2,1)S(1)}, u32[]{:S(2)}, u32[]{:S(2)}) async-start(bf16[8,96,256]{2,1,0:T(8,128)(2,1)} %add_convert_fusion), calls=%async_computation | async-start | bytes 786432 | tf_op jit(solution)/shard_map/all_to_all | solution.py:388
  45.8 0.8 dynamic_slice.9
  46.6 13.0 %all-to-all-done.parts_ref = bf16[8,96,256]{2,1,0:T(8,128)(2,1)S(1)} async-done(((bf16[8,96,256]{2,1,0:T(8,128)(2,1)}), bf16[8,96,256]{2,1,0:T(8,128)(2,1)S(1)}, u32[]{:S(2)}, u32[]{:S(2)}) %all-to-all-start) | async-done | bytes 393248 | tf_op jit(solution)/shard_map/all_to_all | solution.py:388
  59.8 18.3 %all_to_all.15.mine_ref = bf16[16,104,256]{2,1,0:T(8,128)(2,1)S(1)} all-to-all(bf16[16,104,256]{2,1,0:T(8,128)(2,1)S(1)} %get-tuple-element.27), channel_id=1, replica_groups=mesh['y'=4,'x'=4,'z'=8,'c'=2] {'y','x'}, dimensions={0} | all-to-all | bytes 1703936 | tf_op jit(solution)/shard_map/all_to_all | solution.py:390
  78.0 3.1 %collective-permute-start.11 = (bf16[1024,256]{1,0:T(8,128)(2,1)S(1)}, bf16[1024,256]{1,0:T(8,128)(2,1)S(1)}, u32[]{:S(2)}, u32[]{:S(2)}) collective-permute-start(bf16[1024,256]{1,0:T(8,128)(2,1)S(1)} %copy-done), channel_id=1, source_target_pairs={{0,14},{2,0},{4,2},{6,4},{8,6},{10,8},{12,10},{14,12},{1,15},{3,1}... | collective-permute-start | bytes 1572872 | tf_op jit(solution)/shard_map/ppermute | solution.py:197
  81.1 11.9 %collective-permute-done.11.refs_1_ = bf16[1024,256]{1,0:T(8,128)(2,1)S(1)} collective-permute-done((bf16[1024,256]{1,0:T(8,128)(2,1)S(1)}, bf16[1024,256]{1,0:T(8,128)(2,1)S(1)}, u32[]{:S(2)}, u32[]{:S(2)}) %collective-permute-start.11) | collective-permute-done | bytes 524320 | tf_op jit(solution)/shard_map/ppermute | solution.py:197
  93.0 2.2 %collective-permute-done.12.refs_8_ = bf16[1024,256]{1,0:T(8,128)(2,1)S(1)} collective-permute-done((bf16[1024,256]{1,0:T(8,128)(2,1)S(1)}, bf16[1024,256]{1,0:T(8,128)(2,1)S(1)}, u32[]{:S(2)}, u32[]{:S(2)}) %collective-permute-start.12) | collective-permute-done | bytes 524320 | tf_op jit(solution)/shard_map/ppermute | solution.py:197
  95.2 1.5 collective-permute-start.13
  97.2 1.0 up.1
  98.6 9.8 %collective-permute-done.13.refs_2_ = bf16[1024,256]{1,0:T(8,128)(2,1)S(1)} collective-permute-done((bf16[1024,256]{1,0:T(8,128)(2,1)S(1)}, bf16[1024,256]{1,0:T(8,128)(2,1)S(1)}, u32[]{:S(2)}, u32[]{:S(2)}) %collective-permute-start.13) | collective-permute-done | bytes 524320 | tf_op jit(solution)/shard_map/ppermute | solution.py:197
  108.4 3.1 %collective-permute-done.14.refs_7_ = bf16[1024,256]{1,0:T(8,128)(2,1)S(1)} collective-permute-done((bf16[1024,256]{1,0:T(8,128)(2,1)S(1)}, bf16[1024,256]{1,0:T(8,128)(2,1)S(1)}, u32[]{:S(2)}, u32[]{:S(2)}) %collective-permute-start.14) | collective-permute-done | bytes 524320 | tf_op jit(solution)/shard_map/ppermute | solution.py:197
  111.5 1.5 collective-permute-start.15
  113.5 1.5 collective-permute-start.7
  116.1 11.2 %collective-permute-done.7 = bf16[200,512]{1,0:T(8,128)(2,1)S(1)} collective-permute-done((bf16[200,512]{1,0:T(8,128)(2,1)S(1)}, bf16[200,512]{1,0:T(8,128)(2,1)S(1)}, u32[]{:S(2)}, u32[]{:S(2)}) %collective-permute-start.7) | collective-permute-done | bytes 204832 | tf_op jit(solution)/shard_map/ppermute | solution.py:197
  127.4 2.0 %collective-permute-start.8 = (bf16[200,512]{1,0:T(8,128)(2,1)S(1)}, bf16[200,512]{1,0:T(8,128)(2,1)S(1)}, u32[]{:S(2)}, u32[]{:S(2)}) collective-permute-start(bf16[200,512]{1,0:T(8,128)(2,1)S(1)} %add_convert_fusion.2), channel_id=1, source_target_pairs={{0,14},{2,0},{4,2},{6,4},{8,6},{10,8},{12,10},{14,12},{1,15},{3,1}... | collective-permute-start | bytes 614408 | tf_op jit(solution)/shard_map/ppermute | solution.py:197
  130.3 4.7 %collective-permute-done.8 = bf16[200,512]{1,0:T(8,128)(2,1)S(1)} collective-permute-done((bf16[200,512]{1,0:T(8,128)(2,1)S(1)}, bf16[200,512]{1,0:T(8,128)(2,1)S(1)}, u32[]{:S(2)}, u32[]{:S(2)}) %collective-permute-start.8) | collective-permute-done | bytes 204832 | tf_op jit(solution)/shard_map/ppermute | solution.py:197
  135.1 1.8 collective-permute-start.9
  137.3 1.8 collective-permute-start.17
  139.5 1.9 %collective-permute-done.9.c_ref = bf16[200,512]{1,0:T(8,128)(2,1)S(1)} collective-permute-done((bf16[200,512]{1,0:T(8,128)(2,1)S(1)}, bf16[200,512]{1,0:T(8,128)(2,1)S(1)}, u32[]{:S(2)}, u32[]{:S(2)}) %collective-permute-start.9) | collective-permute-done | bytes 204832 | tf_op jit(solution)/shard_map/ppermute | solution.py:197
  141.4 3.5 %collective-permute-done.6.b_ref = bf16[200,512]{1,0:T(8,128)(2,1)S(1)} collective-permute-done((bf16[200,512]{1,0:T(8,128)(2,1)S(1)}, bf16[200,512]{1,0:T(8,128)(2,1)S(1)}, u32[]{:S(2)}, u32[]{:S(2)}) %collective-permute-start.6) | collective-permute-done | bytes 204832 | tf_op jit(solution)/shard_map/ppermute | solution.py:197
  145.2 2.6 %collective-permute-done.18.refs_5_ = bf16[512,256]{1,0:T(8,128)(2,1)S(1)} collective-permute-done((bf16[512,256]{1,0:T(8,128)(2,1)S(1)}, bf16[512,256]{1,0:T(8,128)(2,1)S(1)}, u32[]{:S(2)}, u32[]{:S(2)}) %collective-permute-start.18) | collective-permute-done | bytes 262176 | tf_op jit(solution)/shard_map/ppermute | solution.py:197
  147.7 1.0 down.1
  148.7 16.4 %all_to_all.16 = bf16[16,96,256]{2,1,0:T(8,128)(2,1)S(1)} all-to-all(bf16[16,96,256]{2,1,0:T(8,128)(2,1)S(1)} %down.1), channel_id=1, replica_groups=mesh['y'=4,'x'=4,'z'=8,'c'=2] {'y','x'}, dimensions={0} | all-to-all | bytes 1572864 | tf_op jit(solution)/shard_map/all_to_all | solution.py:396
  165.2 6.0 %collective-permute-start.19 = (bf16[96,256]{1,0:T(8,128)(2,1)S(1)}, bf16[96,256]{1,0:T(8,128)(2,1)S(1)}, u32[]{:S(2)}, u32[]{:S(2)}) collective-permute-start(bf16[96,256]{1,0:T(8,128)(2,1)S(1)} %reduce_sum.12), channel_id=1, source_target_pairs={{0,0},{1,1},{2,34},{3,35},{4,68},{5,69},{6,102},{7,103},{8,136},{9... | collective-permute-start | bytes 147464 | tf_op jit(solution)/shard_map/ppermute | solution.py:402
  171.3 8.3 %collective-permute-done.19 = bf16[96,256]{1,0:T(8,128)(2,1)S(1)} collective-permute-done((bf16[96,256]{1,0:T(8,128)(2,1)S(1)}, bf16[96,256]{1,0:T(8,128)(2,1)S(1)}, u32[]{:S(2)}, u32[]{:S(2)}) %collective-permute-start.19) | collective-permute-done | bytes 49184 | tf_op jit(solution)/shard_map/ppermute | solution.py:402
  179.5 0.6 add_convert_fusion.6
  (35 shorter events, 5.5 us)
Async XLA Ops:
  1.7 22.4 %collective-permute-start = (bf16[256,512]{1,0:T(8,128)(2,1)S(1)}, bf16[256,512]{1,0:T(8,128)(2,1)S(1)}, u32[]{:S(2)}, u32[]{:S(2)}) collective-permute-start(bf16[256,512]{1,0:T(8,128)(2,1)S(1)} %get-tuple-element.45), channel_id=1, source_target_pairs={{0,1},{1,0},{2,3},{3,2},{4,5},{5,4},{6,7},{7,6},{8,9},{9,8},{10,11... | collective-permute-start | bytes 786440 | tf_op jit(solution)/shard_map/ppermute | solution.py:201
  24.1 35.5 %copy-start.1 = (bf16[96,256]{1,0:T(8,128)(2,1)S(1)}, bf16[96,256]{1,0:T(8,128)(2,1)}, u32[]{:S(2)}) copy-start(bf16[96,256]{1,0:T(8,128)(2,1)} %tok_ref.1) | copy-start | bytes 147460
  36.1 42.0 %copy-start = (bf16[1024,256]{1,0:T(8,128)(2,1)S(1)}, bf16[1024,256]{1,0:T(8,128)(2,1)}, u32[]{:S(2)}) copy-start(bf16[1024,256]{1,0:T(8,128)(2,1)} %refs_0_.1) | copy-start | bytes 1572868
  36.1 2.0 %collective-permute-start.1 = (bf16[8,96,256]{2,1,0:T(8,128)(2,1)}, bf16[8,96,256]{2,1,0:T(8,128)(2,1)S(1)}, u32[]{:S(2)}, u32[]{:S(2)}) collective-permute-start(bf16[8,96,256]{2,1,0:T(8,128)(2,1)} %get-tuple-element.25), channel_id=1, source_target_pairs={{0,1},{1,0},{2,3},{3,2},{4,5},{5,4},{6,7},{7,6},{8,9},{9,8},{10,11... | collective-permute-start | bytes 1179656 | tf_op jit(solution)/shard_map/ppermute | solution.py:201
  39.9 19.7 %all-to-all-start = ((bf16[8,96,256]{2,1,0:T(8,128)(2,1)}), bf16[8,96,256]{2,1,0:T(8,128)(2,1)S(1)}, u32[]{:S(2)}, u32[]{:S(2)}) async-start(bf16[8,96,256]{2,1,0:T(8,128)(2,1)} %add_convert_fusion), calls=%async_computation | async-start | bytes 786432 | tf_op jit(solution)/shard_map/all_to_all | solution.py:388
  78.0 19.2 %collective-permute-start.2 = (bf16[16,104,256]{2,1,0:T(8,128)(2,1)S(1)}, bf16[16,104,256]{2,1,0:T(8,128)(2,1)S(1)}, u32[]{:S(2)}, u32[]{:S(2)}) collective-permute-start(bf16[16,104,256]{2,1,0:T(8,128)(2,1)S(1)} %all_to_all.15.mine_ref), channel_id=1, source_target_pairs={{0,1},{1,0},{2,3},{3,2},{4,5},{5,4},{6,7},{7,6},{8,9},{9,8},{10,11... | collective-permute-start | bytes 2555912 | tf_op jit(solution)/shard_map/ppermute | solution.py:201
  78.0 14.9 %collective-permute-start.11 = (bf16[1024,256]{1,0:T(8,128)(2,1)S(1)}, bf16[1024,256]{1,0:T(8,128)(2,1)S(1)}, u32[]{:S(2)}, u32[]{:S(2)}) collective-permute-start(bf16[1024,256]{1,0:T(8,128)(2,1)S(1)} %copy-done), channel_id=1, source_target_pairs={{0,14},{2,0},{4,2},{6,4},{8,6},{10,8},{12,10},{14,12},{1,15},{3,1}... | collective-permute-start | bytes 1572872 | tf_op jit(solution)/shard_map/ppermute | solution.py:197
  81.1 14.1 %collective-permute-start.12 = (bf16[1024,256]{1,0:T(8,128)(2,1)S(1)}, bf16[1024,256]{1,0:T(8,128)(2,1)S(1)}, u32[]{:S(2)}, u32[]{:S(2)}) collective-permute-start(bf16[1024,256]{1,0:T(8,128)(2,1)S(1)} %copy-done), channel_id=1, source_target_pairs={{0,2},{2,4},{4,6},{6,8},{8,10},{10,12},{12,14},{14,0},{1,3},{3,5},... | collective-permute-start | bytes 1572872 | tf_op jit(solution)/shard_map/ppermute | solution.py:197
  95.2 13.2 %collective-permute-start.13 = (bf16[1024,256]{1,0:T(8,128)(2,1)S(1)}, bf16[1024,256]{1,0:T(8,128)(2,1)S(1)}, u32[]{:S(2)}, u32[]{:S(2)}) collective-permute-start(bf16[1024,256]{1,0:T(8,128)(2,1)S(1)} %collective-permute-done.11.refs_1_), channel_id=1, source_target_pairs={{0,14},{2,0},{4,2},{6,4},{8,6},{10,8},{12,10},{14,12},{1,15},{3,1}... | collective-permute-start | bytes 1572872 | tf_op jit(solution)/shard_map/ppermute | solution.py:197
  96.7 14.8 %collective-permute-start.14 = (bf16[1024,256]{1,0:T(8,128)(2,1)S(1)}, bf16[1024,256]{1,0:T(8,128)(2,1)S(1)}, u32[]{:S(2)}, u32[]{:S(2)}) collective-permute-start(bf16[1024,256]{1,0:T(8,128)(2,1)S(1)} %collective-permute-done.12.refs_8_), channel_id=1, source_target_pairs={{0,2},{2,4},{4,6},{6,8},{8,10},{10,12},{12,14},{14,0},{1,3},{3,5},... | collective-permute-start | bytes 1572872 | tf_op jit(solution)/shard_map/ppermute | solution.py:197
  98.2 17.4 %collective-permute-start.3 = (bf16[200,512]{1,0:T(8,128)(2,1)S(1)}, bf16[200,512]{1,0:T(8,128)(2,1)S(1)}, u32[]{:S(2)}, u32[]{:S(2)}) collective-permute-start(bf16[200,512]{1,0:T(8,128)(2,1)S(1)} %get-tuple-element.33), channel_id=1, source_target_pairs={{0,2},{2,4},{4,6},{6,8},{8,10},{10,12},{12,14},{14,0},{1,3},{3,5},... | collective-permute-start | bytes 614408 | tf_op jit(solution)/shard_map/ppermute | solution.py:197
  111.5 25.8 %collective-permute-start.15 = (bf16[1024,256]{1,0:T(8,128)(2,1)S(1)}, bf16[1024,256]{1,0:T(8,128)(2,1)S(1)}, u32[]{:S(2)}, u32[]{:S(2)}) collective-permute-start(bf16[1024,256]{1,0:T(8,128)(2,1)S(1)} %collective-permute-done.13.refs_2_), channel_id=1, source_target_pairs={{0,14},{2,0},{4,2},{6,4},{8,6},{10,8},{12,10},{14,12},{1,15},{3,1}... | collective-permute-start | bytes 1572872 | tf_op jit(solution)/shard_map/ppermute | solution.py:197
  113.0 24.3 %collective-permute-start.16 = (bf16[1024,256]{1,0:T(8,128)(2,1)S(1)}, bf16[1024,256]{1,0:T(8,128)(2,1)S(1)}, u32[]{:S(2)}, u32[]{:S(2)}) collective-permute-start(bf16[1024,256]{1,0:T(8,128)(2,1)S(1)} %collective-permute-done.14.refs_7_), channel_id=1, source_target_pairs={{0,2},{2,4},{4,6},{6,8},{8,10},{10,12},{12,14},{14,0},{1,3},{3,5},... | collective-permute-start | bytes 1572872 | tf_op jit(solution)/shard_map/ppermute | solution.py:197
  113.5 13.9 %collective-permute-start.7 = (bf16[200,512]{1,0:T(8,128)(2,1)S(1)}, bf16[200,512]{1,0:T(8,128)(2,1)S(1)}, u32[]{:S(2)}, u32[]{:S(2)}) collective-permute-start(bf16[200,512]{1,0:T(8,128)(2,1)S(1)} %get-tuple-element.36), channel_id=1, source_target_pairs={{0,14},{2,0},{4,2},{6,4},{8,6},{10,8},{12,10},{14,12},{1,15},{3,1}... | collective-permute-start | bytes 614408 | tf_op jit(solution)/shard_map/ppermute | solution.py:197
  115.7 14.1 %collective-permute-start.4 = (bf16[200,512]{1,0:T(8,128)(2,1)S(1)}, bf16[200,512]{1,0:T(8,128)(2,1)S(1)}, u32[]{:S(2)}, u32[]{:S(2)}) collective-permute-start(bf16[200,512]{1,0:T(8,128)(2,1)S(1)} %add_convert_fusion.5), channel_id=1, source_target_pairs={{0,2},{2,4},{4,6},{6,8},{8,10},{10,12},{12,14},{14,0},{1,3},{3,5},... | collective-permute-start | bytes 614408 | tf_op jit(solution)/shard_map/ppermute | solution.py:197
  127.4 7.6 %collective-permute-start.8 = (bf16[200,512]{1,0:T(8,128)(2,1)S(1)}, bf16[200,512]{1,0:T(8,128)(2,1)S(1)}, u32[]{:S(2)}, u32[]{:S(2)}) collective-permute-start(bf16[200,512]{1,0:T(8,128)(2,1)S(1)} %add_convert_fusion.2), channel_id=1, source_target_pairs={{0,14},{2,0},{4,2},{6,4},{8,6},{10,8},{12,10},{14,12},{1,15},{3,1}... | collective-permute-start | bytes 614408 | tf_op jit(solution)/shard_map/ppermute | solution.py:197
  129.9 7.0 %collective-permute-start.5 = (bf16[200,512]{1,0:T(8,128)(2,1)S(1)}, bf16[200,512]{1,0:T(8,128)(2,1)S(1)}, u32[]{:S(2)}, u32[]{:S(2)}) collective-permute-start(bf16[200,512]{1,0:T(8,128)(2,1)S(1)} %add_convert_fusion.4), channel_id=1, source_target_pairs={{0,2},{2,4},{4,6},{6,8},{8,10},{10,12},{12,14},{14,0},{1,3},{3,5},... | collective-permute-start | bytes 614408 | tf_op jit(solution)/shard_map/ppermute | solution.py:197
  135.1 6.3 %collective-permute-start.9 = (bf16[200,512]{1,0:T(8,128)(2,1)S(1)}, bf16[200,512]{1,0:T(8,128)(2,1)S(1)}, u32[]{:S(2)}, u32[]{:S(2)}) collective-permute-start(bf16[200,512]{1,0:T(8,128)(2,1)S(1)} %add_convert_fusion.1), channel_id=1, source_target_pairs={{0,14},{2,0},{4,2},{6,4},{8,6},{10,8},{12,10},{14,12},{1,15},{3,1}... | collective-permute-start | bytes 614408 | tf_op jit(solution)/shard_map/ppermute | solution.py:197
  136.9 8.0 %collective-permute-start.6 = (bf16[200,512]{1,0:T(8,128)(2,1)S(1)}, bf16[200,512]{1,0:T(8,128)(2,1)S(1)}, u32[]{:S(2)}, u32[]{:S(2)}) collective-permute-start(bf16[200,512]{1,0:T(8,128)(2,1)S(1)} %add_convert_fusion.3), channel_id=1, source_target_pairs={{0,2},{2,4},{4,6},{6,8},{8,10},{10,12},{12,14},{14,0},{1,3},{3,5},... | collective-permute-start | bytes 614408 | tf_op jit(solution)/shard_map/ppermute | solution.py:197
  137.3 7.8 %collective-permute-start.17 = (bf16[512,256]{1,0:T(8,128)(2,1)S(1)}, bf16[512,256]{1,0:T(8,128)(2,1)S(1)}, u32[]{:S(2)}, u32[]{:S(2)}) collective-permute-start(bf16[512,256]{1,0:T(8,128)(2,1)S(1)} %slice.6), channel_id=1, source_target_pairs={{0,14},{2,0},{4,2},{6,4},{8,6},{10,8},{12,10},{14,12},{1,15},{3,1}... | collective-permute-start | bytes 786440 | tf_op jit(solution)/shard_map/ppermute | solution.py:197
  139.1 8.6 %collective-permute-start.18 = (bf16[512,256]{1,0:T(8,128)(2,1)S(1)}, bf16[512,256]{1,0:T(8,128)(2,1)S(1)}, u32[]{:S(2)}, u32[]{:S(2)}) collective-permute-start(bf16[512,256]{1,0:T(8,128)(2,1)S(1)} %slice.7), channel_id=1, source_target_pairs={{0,2},{2,4},{4,6},{6,8},{8,10},{10,12},{12,14},{14,0},{1,3},{3,5},... | collective-permute-start | bytes 786440 | tf_op jit(solution)/shard_map/ppermute | solution.py:197
  145.0 2.7 %collective-permute-start.10 = (bf16[192,512]{1,0:T(8,128)(2,1)S(1)}, bf16[192,512]{1,0:T(8,128)(2,1)S(1)}, u32[]{:S(2)}, u32[]{:S(2)}) collective-permute-start(bf16[192,512]{1,0:T(8,128)(2,1)S(1)} %hidden.1.mine_ref), channel_id=1, source_target_pairs={{0,1},{1,0},{2,3},{3,2},{4,5},{5,4},{6,7},{7,6},{8,9},{9,8},{10,11... | collective-permute-start | bytes 589832 | tf_op jit(solution)/shard_map/ppermute | solution.py:201
  165.2 14.3 %collective-permute-start.19 = (bf16[96,256]{1,0:T(8,128)(2,1)S(1)}, bf16[96,256]{1,0:T(8,128)(2,1)S(1)}, u32[]{:S(2)}, u32[]{:S(2)}) collective-permute-start(bf16[96,256]{1,0:T(8,128)(2,1)S(1)} %reduce_sum.12), channel_id=1, source_target_pairs={{0,0},{1,1},{2,34},{3,35},{4,68},{5,69},{6,102},{7,103},{8,136},{9... | collective-permute-start | bytes 147464 | tf_op jit(solution)/shard_map/ppermute | solution.py:402

commit v3 on v2

--- a/solution.py
+++ b/solution.py
@@ -1,3 +1,5 @@
+import functools
+
 import jax
 import jax.numpy as jnp
 from jax import lax
@@ -16,7 +18,7 @@
 PAD = 8
 
 
-def attn_kernel(h0_ref, rate_ref, bias_ref, tok_ref, mg_ref, wq_hbm, wk_hbm, wv_hbm, wg_hbm, wd_hbm, wb_hbm, wo_hbm, og_ref, st_hbm,
+def attn_kernel(h0_ref, core_ref, rate_ref, bias_ref, tok_ref, mg_ref, wq_hbm, wk_hbm, wv_hbm, wg_hbm, wd_hbm, wb_hbm, wo_hbm, og_ref, st_hbm,
                 ns_hbm, keep_ref, give_ref, wo, w4, w2, st, xn, vv, od, ex, e2, sem_w, sem_in, sem_out):
     rows = tok_ref.shape[1]
     width = tok_ref.shape[2]
@@ -139,7 +141,7 @@
     ho = o * lax.rsqrt(ms + EPS) * gain * (g / (1.0 + jnp.exp(-g)))
     head_out = ho.astype(BF16)
     loads[6].wait()
-    core = h0_ref[1]
+    core = core_ref[0]
     for i in range(keep_ref.shape[0]):
         for ref, side in ((give_ref, 1 - core), (keep_ref, core)):
             cols = wo[:, pl.ds(pl.multiple_of((2 * i + side) * width, width), width)]
@@ -153,7 +155,7 @@
     lax.fori_loop(0, nt, finish, 0)
 
 
-def attn(tok, h0, wq, wk, wv, wg, wd, wb, wo, rate, bias, mix_gain, out_gain, state):
+def attn(tok, h0, core, wq, wk, wv, wg, wd, wb, wo, rate, bias, mix_gain, out_gain, state):
     parts, rows, width = tok.shape
     mg = mix_gain.reshape(parts, 1, width)
     heads = state.shape[1]
@@ -164,7 +166,7 @@
     ns, keep, give = pl.pallas_call(
         attn_kernel,
         out_shape=(jax.ShapeDtypeStruct((rows * 64, 128), F32), jax.ShapeDtypeStruct((8, rows, width), BF16), jax.ShapeDtypeStruct((8, rows, width), BF16)),
-        in_specs=[sm, sm, sm, vm, vm] + [an] * 7 + [vm, an],
+        in_specs=[sm, sm, sm, sm, vm, vm] + [an] * 7 + [vm, an],
         out_specs=(an, vm, vm),
         scratch_shapes=[
             pltpu.VMEM(wo.shape, BF16),
@@ -183,7 +185,7 @@
         compiler_params=pltpu.CompilerParams(vmem_limit_bytes=56 * 1024 * 1024),
         cost_estimate=pl.CostEstimate(flops=2 * 96 * 4096 * 600, bytes_accessed=12_000_000, transcendentals=50000),
         name="attn",
-    )(h0, rate, bias, tok, mg, wq, wk, wv, wg, wd.T, wb.T, wo, out_gain.reshape(1, 64), st)
+    )(h0, core, rate, bias, tok, mg, wq, wk, wv, wg, wd.T, wb.T, wo, out_gain.reshape(1, 64), st)
     ns = ns.reshape(rows, 32, heads, 128).transpose(0, 2, 1, 3).reshape(rows, heads, 4096)
     return ns, keep, give
 
@@ -239,23 +241,32 @@
         at = (z_ref[0] + o) & 7
         own = mine_ref[pl.ds(2 * at, 2)]
         his = other_ref[pl.ds(2 * at, 2)]
-        outs[o][: 2 * rows, :] = (
+        product = (
             jnp.dot(own[:, :rows].reshape(2 * rows, width), wm_ref[...], preferred_element_type=F32)
             + jnp.dot(his[:, :rows].reshape(2 * rows, width), wo_ref[...], preferred_element_type=F32)
         ).astype(BF16)
         squares = own[:, rows:, :128].astype(F32) + his[:, rows:, :128].astype(F32)
-        outs[o][2 * rows :, :128] = squares[0].astype(BF16)
-        outs[o][2 * rows :, 128:256] = squares[1].astype(BF16)
-        outs[o][2 * rows :, 256:] = jnp.zeros((PAD, outs[o].shape[1] - 256), BF16)
+        side = product.shape[1] // 2
+        left, right = outs[o], outs[o]
+        shift = side
+        if o == 4:
+            right, shift = outs[8], 0
+        left[: 2 * rows, :side] = product[:, :side]
+        left[2 * rows :, :128] = squares[0].astype(BF16)
+        left[2 * rows :, 128:256] = squares[1].astype(BF16)
+        right[: 2 * rows, shift : shift + side] = product[:, side:]
+        right[2 * rows :, shift : shift + side] = jnp.zeros((PAD, side), BF16)
 
 
 def up_product(z, mine, other, w_mine, w_other):
     rows = mine.shape[1] - PAD
     return pl.pallas_call(
         up_kernel,
-        out_shape=tuple(jax.ShapeDtypeStruct((2 * rows + PAD, w_mine.shape[1]), BF16) for _ in range(8)),
+        out_shape=tuple(
+            jax.ShapeDtypeStruct((2 * rows + PAD, w_mine.shape[1] // (2 if o in (4, 8) else 1)), BF16) for o in range(9)
+        ),
         in_specs=[SM] + [VM] * 4,
-        out_specs=tuple([VM] * 8),
+        out_specs=tuple([VM] * 9),
         compiler_params=pltpu.CompilerParams(vmem_limit_bytes=24 * 1024 * 1024),
         cost_estimate=pl.CostEstimate(flops=2 * 1536 * 512 * 512, bytes_accessed=4_000_000, transcendentals=0),
         name="up",
@@ -286,18 +297,61 @@
     )(first, second, third)
 
 
+def pair_kernel(one_ref, two_ref, out_ref):
+    out_ref[...] = (one_ref[...].astype(F32) + two_ref[...].astype(F32)).astype(BF16)
+
+
+def pair_sum(one, two):
+    return pl.pallas_call(
+        pair_kernel,
+        out_shape=jax.ShapeDtypeStruct(one.shape, BF16),
+        in_specs=[VM] * 2,
+        out_specs=VM,
+        compiler_params=pltpu.CompilerParams(vmem_limit_bytes=16 * 1024 * 1024),
+        cost_estimate=pl.CostEstimate(flops=1_000_000, bytes_accessed=1_000_000, transcendentals=0),
+        name="pair",
+    )(one, two)
+
+
 def add(one, two):
     return (one.astype(F32) + two.astype(F32)).astype(BF16)
 
 
+def half_kernel(start, full_ref, part_ref, out_ref):
+    out_ref[...] = full_ref[...]
+    cols = slice(start, start + part_ref.shape[1])
+    out_ref[:, cols] = (full_ref[:, cols].astype(F32) + part_ref[...].astype(F32)).astype(BF16)
+
+
+def half_sum(full, part, start):
+    return pl.pallas_call(
+        functools.partial(half_kernel, start),
+        out_shape=jax.ShapeDtypeStruct(full.shape, BF16),
+        in_specs=[VM] * 2,
+        out_specs=VM,
+        compiler_params=pltpu.CompilerParams(vmem_limit_bytes=8 * 1024 * 1024),
+        cost_estimate=pl.CostEstimate(flops=100_000, bytes_accessed=500_000, transcendentals=0),
+        name="half",
+    )(full, part)
+
+
 def ring_sum(blocks):
-    ahead = blocks[4]
-    back = blocks[5]
-    ahead = add(blocks[3], shifted(ahead, 1))
+    ahead = shifted(blocks[4], 1)
+    back = shifted(blocks[8], -1)
+    ahead = half_sum(blocks[3], ahead, 0)
+    ahead = shifted(ahead, 1)
+    back = half_sum(blocks[5], back, blocks[4].shape[1])
+    back = shifted(back, -1)
     for step in (2, 1):
-        ahead = add(blocks[step], shifted(ahead, 1))
-        back = add(blocks[8 - step], shifted(back, -1))
-    return blocks[0], shifted(ahead, 1), shifted(back, -1)
+        ahead = add(blocks[step], ahead)
+        ahead = shifted(ahead, 1)
+        back = add(blocks[8 - step], back)
+        back = shifted(back, -1)
+    return blocks[0], ahead, back
+
+
+def tied(array, *others):
+    return lax.optimization_barrier((array,) + others)[0]
 
 
 def ring_gather(block, *after):
@@ -319,7 +373,7 @@
     return parts
 
 
-def down_kernel(c_ref, mine_ref, other_ref, *refs):
+def down_kernel(z_ref, c_ref, mine_ref, other_ref, *refs):
     weights, out_ref = refs[:-1], refs[-1]
     rows = out_ref.shape[1]
     half = mine_ref.shape[1]
@@ -335,22 +389,23 @@
             ref = weights[o] if o < 4 else weights[o + 1]
             top, bottom = ref[:half, :], ref[half:, :]
         out = jnp.dot(low, top, preferred_element_type=F32) + jnp.dot(high, bottom, preferred_element_type=F32)
-        out_ref[2 * o] = out[:rows].astype(BF16)
-        out_ref[2 * o + 1] = out[rows:].astype(BF16)
-
-
-def down_product(c, mine, other, weights):
+        at = (o + 2 * z_ref[0]) & 7
+        out_ref[2 * at] = out[:rows].astype(BF16)
+        out_ref[2 * at + 1] = out[rows:].astype(BF16)
+
+
+def down_product(z, c, mine, other, weights):
     rows = mine.shape[0] // 2
     width = weights[0].shape[1]
     return pl.pallas_call(
         down_kernel,
         out_shape=jax.ShapeDtypeStruct((16, rows, width), BF16),
-        in_specs=[SM] + [VM] * 11,
+        in_specs=[SM, SM] + [VM] * 11,
         out_specs=VM,
         compiler_params=pltpu.CompilerParams(vmem_limit_bytes=24 * 1024 * 1024),
         cost_estimate=pl.CostEstimate(flops=2 * 192 * 1024 * 2048, bytes_accessed=6_000_000, transcendentals=0),
         name="down",
-    )(c.reshape(1), mine, other, *weights)
+    )(z.reshape(1), c.reshape(1), mine, other, *weights)
 
 
 def layer(
@@ -376,28 +431,28 @@
     tp = z * 2 + c
     half = w_up.shape[1] // 2
     everything = lax.all_gather(tokens, TP, axis=0, tiled=False)
+    new_state, keep, give = attn(
+        everything, (tp * 2).reshape(1), c.reshape(1), w_query, w_key, w_value, w_gate, w_decay, w_beta, w_out,
+        decay_rate, decay_bias, mix_gain, out_gain, state,
+    )
+    took = other_core(give)
+    parts = lax.all_to_all(pair_sum(keep, took), "z", 0, 0, tiled=True)
+    w_up = tied(w_up, give)
     up_mine = lax.dynamic_slice_in_dim(w_up, c * half, half, 1)
     up_other = other_core(lax.dynamic_slice_in_dim(w_up, (1 - c) * half, half, 1))
     gain = lax.dynamic_slice_in_dim(ffn_gain, tp * width, width, 0).reshape(1, width)
-    everything, up_other = lax.optimization_barrier((everything, up_other))
-    new_state, keep, give = attn(
-        everything, jnp.stack([tp * 2, c]), w_query, w_key, w_value, w_gate, w_decay, w_beta, w_out,
-        decay_rate, decay_bias, mix_gain, out_gain, state,
-    )
-    took = other_core(give)
-    parts = lax.all_to_all(add(keep, took), "z", 0, 0, tiled=True)
     resid, send = residual(tokens, gain, parts)
     mine = lax.all_to_all(send, KV, 0, 0, tiled=True)
     theirs = other_core(mine)
     blocks = up_product(z, mine, theirs, up_mine, up_other)
-    down_weights = ring_gather(w_down, None, everything, parts, mine)
+    down_weights = ring_gather(w_down, everything, None, send, mine)
     hidden = finish_hidden(*ring_sum(blocks))
-    down = down_product(c, hidden, other_core(hidden), down_weights)
+    down = down_product(z, c, hidden, other_core(hidden), down_weights)
     down = lax.all_to_all(down, KV, 0, 0, tiled=True)
     down = down.astype(F32).sum(axis=0).astype(BF16)
     routes = [
-        (((2 * o + b) * 8 + s) * 2 + k, ((2 * s + b) * 8 + (s + o) % 8) * 2 + k)
-        for o in range(8) for b in range(2) for s in range(8) for k in range(2)
+        (((2 * a + b) * 8 + s) * 2 + k, ((2 * s + b) * 8 + (a - s) % 8) * 2 + k)
+        for a in range(8) for b in range(2) for s in range(8) for k in range(2)
     ]
     down = lax.ppermute(down, EVERYWHERE, routes)
     mixed = (resid + down.astype(F32)).astype(BF16)

time: 181 us -> 179 us (0.989)
  the two profiles are of different devices: /device:TPU:56 before, /device:TPU:224 now
where the time goes in v3:
time: 179 us
  waiting for transfers between devices  66.8 us (37%)
  blocking collectives  54.1 us (30%)
  starting transfers between devices  38.4 us (21%)
  Pallas kernels  15.1 us (8%)
  local copies, waits for them, and re-layouts  2.87 us (2%)
    ppermute x16, waiting for transfers between devices, shifted(): lax.ppermute(array, axis, [(i, (i + by) % length) for i in range(length)])  46.3 us
    ppermute x16, starting transfers between devices, shifted(): lax.ppermute(array, axis, [(i, (i + by) % length) for i in range(length)])  28.6 us
    all_to_all x1, blocking collectives, layer(): mine = lax.all_to_all(send, KV, 0, 0, tiled=True)  20.1 us
    all_gather x1, blocking collectives, layer(): everything = lax.all_gather(tokens, TP, axis=0, tiled=False)  17.7 us
    all_to_all x1, blocking collectives, layer(): down = lax.all_to_all(down, KV, 0, 0, tiled=True)  16.4 us
    pallas_call x1, Pallas kernels, attn(): pl.pallas_call(attn_kernel, out_shape=(jax.ShapeDtypeStruct((rows * 64, 1...  11.9 us
    ppermute x1, waiting for transfers between devices, layer(): down = lax.ppermute(down, EVERYWHERE, routes)  9.78 us
    all_to_all x1, waiting for transfers between devices, layer(): parts = lax.all_to_all(pair_sum(keep, took), 'z', 0, 0, tiled=True)  9.1 us
  transfers between devices with their start and end apart: 22, of which 10 were waited for; matrix products, arithmetic and copies ran while one was open for 1% of the time, Pallas kernels for 1%

profile of v3, /device:TPU:224, one launch (start us, length us, event | category | flops | bytes accessed | tf_op | source)
XLA Modules:
  0.0 179.1 jit_solution(6226377650841720910)
XLA Ops:
  0.6 17.7 %all-gather = bf16[1536,256]{1,0:T(8,128)(2,1)} all-gather(bf16[96,256]{1,0:T(8,128)(2,1)} %tok_ref.1), channel_id=2, replica_groups=mesh['y'=4,'x'=4,'z'=8,'c'=2] {'z','c'}, dimensions={0}, use_global_device_ids=true | all-gather | bytes 835584 | tf_op jit(solution)/shard_map/all_gather | solution.py:433
  18.3 11.9 %attn.1 = (f32[6144,128]{1,0:T(8,128)}, bf16[8,96,256]{2,1,0:T(8,128)(2,1)}, bf16[8,96,256]{2,1,0:T(8,128)(2,1)}) custom-call(s32[1]{0:T(128)} %bitcast.1.h0_ref, s32[1]{0:T(128)} %bitcast.2.core_ref.c_ref, f32[2]{0:T(128)} %rate_ref.1, f32[2]{0:T(128)} %bias_ref.1, bf16[16,96,256]{2,1,0:T(8,128)(2,1)} %bitcast.21, f32[16,1,256]{2,1,0:T(1,128)} %bitcast.24, ...), custom_call_target="tpu_custom_call" | custom-call | flops 471859200 | bytes 12000000 | tf_op jit(solution)/shard_map/attn/pallas_call | solution.py:166
  30.7 1.6 collective-permute-done.two_ref
  32.3 1.0 copy-done.1
  33.3 0.8 pair.1
  34.1 7.1 %all-to-all-start = ((bf16[8,96,256]{2,1,0:T(8,128)(2,1)}), bf16[8,96,256]{2,1,0:T(8,128)(2,1)S(1)}, u32[]{:S(2)}, u32[]{:S(2)}) async-start(bf16[8,96,256]{2,1,0:T(8,128)(2,1)} %pair.1), calls=%async_computation | async-start | bytes 786432 | tf_op jit(solution)/shard_map/all_to_all | solution.py:439
  41.2 0.8 dynamic_slice.9
  42.0 9.1 %all-to-all-done.parts_ref = bf16[8,96,256]{2,1,0:T(8,128)(2,1)S(1)} async-done(((bf16[8,96,256]{2,1,0:T(8,128)(2,1)}), bf16[8,96,256]{2,1,0:T(8,128)(2,1)S(1)}, u32[]{:S(2)}, u32[]{:S(2)}) %all-to-all-start) | async-done | bytes 393248 | tf_op jit(solution)/shard_map/all_to_all | solution.py:439
  51.3 20.1 %all_to_all.15.mine_ref = bf16[16,104,256]{2,1,0:T(8,128)(2,1)S(1)} all-to-all(bf16[16,104,256]{2,1,0:T(8,128)(2,1)S(1)} %get-tuple-element.26), channel_id=1, replica_groups=mesh['y'=4,'x'=4,'z'=8,'c'=2] {'y','x'}, dimensions={0} | all-to-all | bytes 1703936 | tf_op jit(solution)/shard_map/all_to_all | solution.py:445
  71.3 4.8 %collective-permute-start.12 = (bf16[1024,256]{1,0:T(8,128)(2,1)S(1)}, bf16[1024,256]{1,0:T(8,128)(2,1)S(1)}, u32[]{:S(2)}, u32[]{:S(2)}) collective-permute-start(bf16[1024,256]{1,0:T(8,128)(2,1)S(1)} %copy-done), channel_id=1, source_target_pairs={{0,14},{2,0},{4,2},{6,4},{8,6},{10,8},{12,10},{14,12},{1,15},{3,1}... | collective-permute-start | bytes 1572872 | tf_op jit(solution)/shard_map/ppermute | solution.py:199
  76.2 2.6 %collective-permute-start.14 = (bf16[1024,256]{1,0:T(8,128)(2,1)S(1)}, bf16[1024,256]{1,0:T(8,128)(2,1)S(1)}, u32[]{:S(2)}, u32[]{:S(2)}) collective-permute-start(bf16[1024,256]{1,0:T(8,128)(2,1)S(1)} %copy-done), channel_id=1, source_target_pairs={{0,2},{2,4},{4,6},{6,8},{8,10},{10,12},{12,14},{14,0},{1,3},{3,5},... | collective-permute-start | bytes 1572872 | tf_op jit(solution)/shard_map/ppermute | solution.py:199
  78.8 1.1 constant_dynamic-slice_fusion
  80.1 11.2 %collective-permute-done.12.refs_1_ = bf16[1024,256]{1,0:T(8,128)(2,1)S(1)} collective-permute-done((bf16[1024,256]{1,0:T(8,128)(2,1)S(1)}, bf16[1024,256]{1,0:T(8,128)(2,1)S(1)}, u32[]{:S(2)}, u32[]{:S(2)}) %collective-permute-start.12) | collective-permute-done | bytes 524320 | tf_op jit(solution)/shard_map/ppermute | solution.py:199
  91.3 3.2 %collective-permute-start.15 = (bf16[1024,256]{1,0:T(8,128)(2,1)S(1)}, bf16[1024,256]{1,0:T(8,128)(2,1)S(1)}, u32[]{:S(2)}, u32[]{:S(2)}) collective-permute-start(bf16[1024,256]{1,0:T(8,128)(2,1)S(1)} %collective-permute-done.14.refs_8_), channel_id=1, source_target_pairs={{0,2},{2,4},{4,6},{6,8},{8,10},{10,12},{12,14},{14,0},{1,3},{3,5},... | collective-permute-start | bytes 1572872 | tf_op jit(solution)/shard_map/ppermute | solution.py:199
  94.5 1.0 up.1
  95.5 0.6 collective-permute-start.3
  96.1 11.6 %collective-permute-done.3.part_ref = bf16[200,256]{1,0:T(8,128)(2,1)S(1)} collective-permute-done((bf16[200,256]{1,0:T(8,128)(2,1)S(1)}, bf16[200,256]{1,0:T(8,128)(2,1)S(1)}, u32[]{:S(2)}, u32[]{:S(2)}) %collective-permute-start.3) | collective-permute-done | bytes 102432 | tf_op jit(solution)/shard_map/ppermute | solution.py:199
  107.8 3.8 %collective-permute-start.4 = (bf16[200,512]{1,0:T(8,128)(2,1)S(1)}, bf16[200,512]{1,0:T(8,128)(2,1)S(1)}, u32[]{:S(2)}, u32[]{:S(2)}) collective-permute-start(bf16[200,512]{1,0:T(8,128)(2,1)S(1)} %half.2), channel_id=1, source_target_pairs={{0,2},{2,4},{4,6},{6,8},{8,10},{10,12},{12,14},{14,0},{1,3},{3,5},... | collective-permute-start | bytes 614408 | tf_op jit(solution)/shard_map/ppermute | solution.py:199
  111.6 3.2 %collective-permute-start.17 = (bf16[1024,256]{1,0:T(8,128)(2,1)S(1)}, bf16[1024,256]{1,0:T(8,128)(2,1)S(1)}, u32[]{:S(2)}, u32[]{:S(2)}) collective-permute-start(bf16[1024,256]{1,0:T(8,128)(2,1)S(1)} %collective-permute-done.15.refs_7_), channel_id=1, source_target_pairs={{0,2},{2,4},{4,6},{6,8},{8,10},{10,12},{12,14},{14,0},{1,3},{3,5},... | collective-permute-start | bytes 1572872 | tf_op jit(solution)/shard_map/ppermute | solution.py:199
  114.9 3.6 %collective-permute-done.7.part_ref = bf16[200,256]{1,0:T(8,128)(2,1)S(1)} collective-permute-done((bf16[200,256]{1,0:T(8,128)(2,1)S(1)}, bf16[200,256]{1,0:T(8,128)(2,1)S(1)}, u32[]{:S(2)}, u32[]{:S(2)}) %collective-permute-start.7) | collective-permute-done | bytes 102432 | tf_op jit(solution)/shard_map/ppermute | solution.py:199
  118.7 3.3 %collective-permute-start.5 = (bf16[200,512]{1,0:T(8,128)(2,1)S(1)}, bf16[200,512]{1,0:T(8,128)(2,1)S(1)}, u32[]{:S(2)}, u32[]{:S(2)}) collective-permute-start(bf16[200,512]{1,0:T(8,128)(2,1)S(1)} %add_convert_fusion.3), channel_id=1, source_target_pairs={{0,2},{2,4},{4,6},{6,8},{8,10},{10,12},{12,14},{14,0},{1,3},{3,5},... | collective-permute-start | bytes 614408 | tf_op jit(solution)/shard_map/ppermute | solution.py:199
  122.0 9.7 %collective-permute-done.8 = bf16[200,512]{1,0:T(8,128)(2,1)S(1)} collective-permute-done((bf16[200,512]{1,0:T(8,128)(2,1)S(1)}, bf16[200,512]{1,0:T(8,128)(2,1)S(1)}, u32[]{:S(2)}, u32[]{:S(2)}) %collective-permute-start.8) | collective-permute-done | bytes 204832 | tf_op jit(solution)/shard_map/ppermute | solution.py:199
  131.9 3.3 %collective-permute-start.6 = (bf16[200,512]{1,0:T(8,128)(2,1)S(1)}, bf16[200,512]{1,0:T(8,128)(2,1)S(1)}, u32[]{:S(2)}, u32[]{:S(2)}) collective-permute-start(bf16[200,512]{1,0:T(8,128)(2,1)S(1)} %add_convert_fusion.2), channel_id=1, source_target_pairs={{0,2},{2,4},{4,6},{6,8},{8,10},{10,12},{12,14},{14,0},{1,3},{3,5},... | collective-permute-start | bytes 614408 | tf_op jit(solution)/shard_map/ppermute | solution.py:199
  135.2 3.6 %collective-permute-done.9 = bf16[200,512]{1,0:T(8,128)(2,1)S(1)} collective-permute-done((bf16[200,512]{1,0:T(8,128)(2,1)S(1)}, bf16[200,512]{1,0:T(8,128)(2,1)S(1)}, u32[]{:S(2)}, u32[]{:S(2)}) %collective-permute-start.9) | collective-permute-done | bytes 204832 | tf_op jit(solution)/shard_map/ppermute | solution.py:199
  139.1 3.3 %collective-permute-start.19 = (bf16[512,256]{1,0:T(8,128)(2,1)S(1)}, bf16[512,256]{1,0:T(8,128)(2,1)S(1)}, u32[]{:S(2)}, u32[]{:S(2)}) collective-permute-start(bf16[512,256]{1,0:T(8,128)(2,1)S(1)} %slice.7), channel_id=1, source_target_pairs={{0,2},{2,4},{4,6},{6,8},{8,10},{10,12},{12,14},{14,0},{1,3},{3,5},... | collective-permute-start | bytes 786440 | tf_op jit(solution)/shard_map/ppermute | solution.py:199
  142.4 4.0 %collective-permute-done.10.c_ref = bf16[200,512]{1,0:T(8,128)(2,1)S(1)} collective-permute-done((bf16[200,512]{1,0:T(8,128)(2,1)S(1)}, bf16[200,512]{1,0:T(8,128)(2,1)S(1)}, u32[]{:S(2)}, u32[]{:S(2)}) %collective-permute-start.10) | collective-permute-done | bytes 204832 | tf_op jit(solution)/shard_map/ppermute | solution.py:199
  146.7 2.6 %collective-permute-done.18.refs_4_ = bf16[512,256]{1,0:T(8,128)(2,1)S(1)} collective-permute-done((bf16[512,256]{1,0:T(8,128)(2,1)S(1)}, bf16[512,256]{1,0:T(8,128)(2,1)S(1)}, u32[]{:S(2)}, u32[]{:S(2)}) %collective-permute-start.18) | collective-permute-done | bytes 262176 | tf_op jit(solution)/shard_map/ppermute | solution.py:199
  149.2 1.0 down.1
  150.2 16.4 %all_to_all.16 = bf16[16,96,256]{2,1,0:T(8,128)(2,1)S(1)} all-to-all(bf16[16,96,256]{2,1,0:T(8,128)(2,1)S(1)} %down.1), channel_id=1, replica_groups=mesh['y'=4,'x'=4,'z'=8,'c'=2] {'y','x'}, dimensions={0} | all-to-all | bytes 1572864 | tf_op jit(solution)/shard_map/all_to_all | solution.py:451
  166.7 1.9 %collective-permute-start.20 = (bf16[96,256]{1,0:T(8,128)(2,1)S(1)}, bf16[96,256]{1,0:T(8,128)(2,1)S(1)}, u32[]{:S(2)}, u32[]{:S(2)}) collective-permute-start(bf16[96,256]{1,0:T(8,128)(2,1)S(1)} %reduce_sum.12), channel_id=1, source_target_pairs={{0,0},{1,1},{2,46},{3,47},{4,76},{5,77},{6,106},{7,107},{8,136},{9... | collective-permute-start | bytes 147464 | tf_op jit(solution)/shard_map/ppermute | solution.py:457
  168.7 9.8 %collective-permute-done.20 = bf16[96,256]{1,0:T(8,128)(2,1)S(1)} collective-permute-done((bf16[96,256]{1,0:T(8,128)(2,1)S(1)}, bf16[96,256]{1,0:T(8,128)(2,1)S(1)}, u32[]{:S(2)}, u32[]{:S(2)}) %collective-permute-start.20) | collective-permute-done | bytes 49184 | tf_op jit(solution)/shard_map/ppermute | solution.py:457
  178.4 0.6 add_convert_fusion.4
  (39 shorter events, 1.9 us)
Async XLA Ops:
  18.3 32.8 %copy-start.2 = (bf16[96,256]{1,0:T(8,128)(2,1)S(1)}, bf16[96,256]{1,0:T(8,128)(2,1)}, u32[]{:S(2)}) copy-start(bf16[96,256]{1,0:T(8,128)(2,1)} %tok_ref.1) | copy-start | bytes 147460
  30.3 41.1 %copy-start = (bf16[1024,256]{1,0:T(8,128)(2,1)S(1)}, bf16[1024,256]{1,0:T(8,128)(2,1)}, u32[]{:S(2)}) copy-start(bf16[1024,256]{1,0:T(8,128)(2,1)} %refs_0_.1) | copy-start | bytes 1572868
  30.3 2.0 %collective-permute-start = (bf16[8,96,256]{2,1,0:T(8,128)(2,1)}, bf16[8,96,256]{2,1,0:T(8,128)(2,1)S(1)}, u32[]{:S(2)}, u32[]{:S(2)}) collective-permute-start(bf16[8,96,256]{2,1,0:T(8,128)(2,1)} %get-tuple-element.24), channel_id=1, source_target_pairs={{0,1},{1,0},{2,3},{3,2},{4,5},{5,4},{6,7},{7,6},{8,9},{9,8},{10,11... | collective-permute-start | bytes 1179656 | tf_op jit(solution)/shard_map/ppermute | solution.py:203
  32.3 1.0 copy-start.1
  34.1 17.0 %all-to-all-start = ((bf16[8,96,256]{2,1,0:T(8,128)(2,1)}), bf16[8,96,256]{2,1,0:T(8,128)(2,1)S(1)}, u32[]{:S(2)}, u32[]{:S(2)}) async-start(bf16[8,96,256]{2,1,0:T(8,128)(2,1)} %pair.1), calls=%async_computation | async-start | bytes 786432 | tf_op jit(solution)/shard_map/all_to_all | solution.py:439
  71.3 23.2 %collective-permute-start.1 = (bf16[16,104,256]{2,1,0:T(8,128)(2,1)S(1)}, bf16[16,104,256]{2,1,0:T(8,128)(2,1)S(1)}, u32[]{:S(2)}, u32[]{:S(2)}) collective-permute-start(bf16[16,104,256]{2,1,0:T(8,128)(2,1)S(1)} %all_to_all.15.mine_ref), channel_id=1, source_target_pairs={{0,1},{1,0},{2,3},{3,2},{4,5},{5,4},{6,7},{7,6},{8,9},{9,8},{10,11... | collective-permute-start | bytes 2555912 | tf_op jit(solution)/shard_map/ppermute | solution.py:203
  71.3 20.0 %collective-permute-start.12 = (bf16[1024,256]{1,0:T(8,128)(2,1)S(1)}, bf16[1024,256]{1,0:T(8,128)(2,1)S(1)}, u32[]{:S(2)}, u32[]{:S(2)}) collective-permute-start(bf16[1024,256]{1,0:T(8,128)(2,1)S(1)} %copy-done), channel_id=1, source_target_pairs={{0,14},{2,0},{4,2},{6,4},{8,6},{10,8},{12,10},{14,12},{1,15},{3,1}... | collective-permute-start | bytes 1572872 | tf_op jit(solution)/shard_map/ppermute | solution.py:199
  76.2 15.1 %collective-permute-start.14 = (bf16[1024,256]{1,0:T(8,128)(2,1)S(1)}, bf16[1024,256]{1,0:T(8,128)(2,1)S(1)}, u32[]{:S(2)}, u32[]{:S(2)}) collective-permute-start(bf16[1024,256]{1,0:T(8,128)(2,1)S(1)} %copy-done), channel_id=1, source_target_pairs={{0,2},{2,4},{4,6},{6,8},{8,10},{10,12},{12,14},{14,0},{1,3},{3,5},... | collective-permute-start | bytes 1572872 | tf_op jit(solution)/shard_map/ppermute | solution.py:199
  79.9 14.7 %collective-permute-start.2 = (bf16[256,512]{1,0:T(8,128)(2,1)S(1)}, bf16[256,512]{1,0:T(8,128)(2,1)S(1)}, u32[]{:S(2)}, u32[]{:S(2)}) collective-permute-start(bf16[256,512]{1,0:T(8,128)(2,1)S(1)} %get-tuple-element.44), channel_id=1, source_target_pairs={{0,1},{1,0},{2,3},{3,2},{4,5},{5,4},{6,7},{7,6},{8,9},{9,8},{10,11... | collective-permute-start | bytes 786440 | tf_op jit(solution)/shard_map/ppermute | solution.py:203
  91.3 20.2 %collective-permute-start.13 = (bf16[1024,256]{1,0:T(8,128)(2,1)S(1)}, bf16[1024,256]{1,0:T(8,128)(2,1)S(1)}, u32[]{:S(2)}, u32[]{:S(2)}) collective-permute-start(bf16[1024,256]{1,0:T(8,128)(2,1)S(1)} %collective-permute-done.12.refs_1_), channel_id=1, source_target_pairs={{0,14},{2,0},{4,2},{6,4},{8,6},{10,8},{12,10},{14,12},{1,15},{3,1}... | collective-permute-start | bytes 1572872 | tf_op jit(solution)/shard_map/ppermute | solution.py:199
  91.3 20.2 %collective-permute-start.15 = (bf16[1024,256]{1,0:T(8,128)(2,1)S(1)}, bf16[1024,256]{1,0:T(8,128)(2,1)S(1)}, u32[]{:S(2)}, u32[]{:S(2)}) collective-permute-start(bf16[1024,256]{1,0:T(8,128)(2,1)S(1)} %collective-permute-done.14.refs_8_), channel_id=1, source_target_pairs={{0,2},{2,4},{4,6},{6,8},{8,10},{10,12},{12,14},{14,0},{1,3},{3,5},... | collective-permute-start | bytes 1572872 | tf_op jit(solution)/shard_map/ppermute | solution.py:199
  95.5 12.2 %collective-permute-start.3 = (bf16[200,256]{1,0:T(8,128)(2,1)S(1)}, bf16[200,256]{1,0:T(8,128)(2,1)S(1)}, u32[]{:S(2)}, u32[]{:S(2)}) collective-permute-start(bf16[200,256]{1,0:T(8,128)(2,1)S(1)} %get-tuple-element.32), channel_id=1, source_target_pairs={{0,2},{2,4},{4,6},{6,8},{8,10},{10,12},{12,14},{14,0},{1,3},{3,5},... | collective-permute-start | bytes 307208 | tf_op jit(solution)/shard_map/ppermute | solution.py:199
  107.8 10.9 %collective-permute-start.4 = (bf16[200,512]{1,0:T(8,128)(2,1)S(1)}, bf16[200,512]{1,0:T(8,128)(2,1)S(1)}, u32[]{:S(2)}, u32[]{:S(2)}) collective-permute-start(bf16[200,512]{1,0:T(8,128)(2,1)S(1)} %half.2), channel_id=1, source_target_pairs={{0,2},{2,4},{4,6},{6,8},{8,10},{10,12},{12,14},{14,0},{1,3},{3,5},... | collective-permute-start | bytes 614408 | tf_op jit(solution)/shard_map/ppermute | solution.py:199
  111.5 7.0 %collective-permute-start.7 = (bf16[200,256]{1,0:T(8,128)(2,1)S(1)}, bf16[200,256]{1,0:T(8,128)(2,1)S(1)}, u32[]{:S(2)}, u32[]{:S(2)}) collective-permute-start(bf16[200,256]{1,0:T(8,128)(2,1)S(1)} %get-tuple-element.36), channel_id=1, source_target_pairs={{0,14},{2,0},{4,2},{6,4},{8,6},{10,8},{12,10},{14,12},{1,15},{3,1}... | collective-permute-start | bytes 307208 | tf_op jit(solution)/shard_map/ppermute | solution.py:199
  111.5 27.4 %collective-permute-start.16 = (bf16[1024,256]{1,0:T(8,128)(2,1)S(1)}, bf16[1024,256]{1,0:T(8,128)(2,1)S(1)}, u32[]{:S(2)}, u32[]{:S(2)}) collective-permute-start(bf16[1024,256]{1,0:T(8,128)(2,1)S(1)} %collective-permute-done.13.refs_2_), channel_id=1, source_target_pairs={{0,14},{2,0},{4,2},{6,4},{8,6},{10,8},{12,10},{14,12},{1,15},{3,1}... | collective-permute-start | bytes 1572872 | tf_op jit(solution)/shard_map/ppermute | solution.py:199
  111.6 27.3 %collective-permute-start.17 = (bf16[1024,256]{1,0:T(8,128)(2,1)S(1)}, bf16[1024,256]{1,0:T(8,128)(2,1)S(1)}, u32[]{:S(2)}, u32[]{:S(2)}) collective-permute-start(bf16[1024,256]{1,0:T(8,128)(2,1)S(1)} %collective-permute-done.15.refs_7_), channel_id=1, source_target_pairs={{0,2},{2,4},{4,6},{6,8},{8,10},{10,12},{12,14},{14,0},{1,3},{3,5},... | collective-permute-start | bytes 1572872 | tf_op jit(solution)/shard_map/ppermute | solution.py:199
  118.5 13.1 %collective-permute-start.8 = (bf16[200,512]{1,0:T(8,128)(2,1)S(1)}, bf16[200,512]{1,0:T(8,128)(2,1)S(1)}, u32[]{:S(2)}, u32[]{:S(2)}) collective-permute-start(bf16[200,512]{1,0:T(8,128)(2,1)S(1)} %half.3), channel_id=1, source_target_pairs={{0,14},{2,0},{4,2},{6,4},{8,6},{10,8},{12,10},{14,12},{1,15},{3,1}... | collective-permute-start | bytes 614408 | tf_op jit(solution)/shard_map/ppermute | solution.py:199
  118.7 13.1 %collective-permute-start.5 = (bf16[200,512]{1,0:T(8,128)(2,1)S(1)}, bf16[200,512]{1,0:T(8,128)(2,1)S(1)}, u32[]{:S(2)}, u32[]{:S(2)}) collective-permute-start(bf16[200,512]{1,0:T(8,128)(2,1)S(1)} %add_convert_fusion.3), channel_id=1, source_target_pairs={{0,2},{2,4},{4,6},{6,8},{8,10},{10,12},{12,14},{14,0},{1,3},{3,5},... | collective-permute-start | bytes 614408 | tf_op jit(solution)/shard_map/ppermute | solution.py:199
  131.7 7.0 %collective-permute-start.9 = (bf16[200,512]{1,0:T(8,128)(2,1)S(1)}, bf16[200,512]{1,0:T(8,128)(2,1)S(1)}, u32[]{:S(2)}, u32[]{:S(2)}) collective-permute-start(bf16[200,512]{1,0:T(8,128)(2,1)S(1)} %add_convert_fusion.1), channel_id=1, source_target_pairs={{0,14},{2,0},{4,2},{6,4},{8,6},{10,8},{12,10},{14,12},{1,15},{3,1}... | collective-permute-start | bytes 614408 | tf_op jit(solution)/shard_map/ppermute | solution.py:199
  131.9 10.5 %collective-permute-start.6 = (bf16[200,512]{1,0:T(8,128)(2,1)S(1)}, bf16[200,512]{1,0:T(8,128)(2,1)S(1)}, u32[]{:S(2)}, u32[]{:S(2)}) collective-permute-start(bf16[200,512]{1,0:T(8,128)(2,1)S(1)} %add_convert_fusion.2), channel_id=1, source_target_pairs={{0,2},{2,4},{4,6},{6,8},{8,10},{10,12},{12,14},{14,0},{1,3},{3,5},... | collective-permute-start | bytes 614408 | tf_op jit(solution)/shard_map/ppermute | solution.py:199
  138.8 7.6 %collective-permute-start.10 = (bf16[200,512]{1,0:T(8,128)(2,1)S(1)}, bf16[200,512]{1,0:T(8,128)(2,1)S(1)}, u32[]{:S(2)}, u32[]{:S(2)}) collective-permute-start(bf16[200,512]{1,0:T(8,128)(2,1)S(1)} %add_convert_fusion), channel_id=1, source_target_pairs={{0,14},{2,0},{4,2},{6,4},{8,6},{10,8},{12,10},{14,12},{1,15},{3,1}... | collective-permute-start | bytes 614408 | tf_op jit(solution)/shard_map/ppermute | solution.py:199
  139.0 10.3 %collective-permute-start.18 = (bf16[512,256]{1,0:T(8,128)(2,1)S(1)}, bf16[512,256]{1,0:T(8,128)(2,1)S(1)}, u32[]{:S(2)}, u32[]{:S(2)}) collective-permute-start(bf16[512,256]{1,0:T(8,128)(2,1)S(1)} %slice.6), channel_id=1, source_target_pairs={{0,14},{2,0},{4,2},{6,4},{8,6},{10,8},{12,10},{14,12},{1,15},{3,1}... | collective-permute-start | bytes 786440 | tf_op jit(solution)/shard_map/ppermute | solution.py:199
  139.1 10.1 %collective-permute-start.19 = (bf16[512,256]{1,0:T(8,128)(2,1)S(1)}, bf16[512,256]{1,0:T(8,128)(2,1)S(1)}, u32[]{:S(2)}, u32[]{:S(2)}) collective-permute-start(bf16[512,256]{1,0:T(8,128)(2,1)S(1)} %slice.7), channel_id=1, source_target_pairs={{0,2},{2,4},{4,6},{6,8},{8,10},{10,12},{12,14},{14,0},{1,3},{3,5},... | collective-permute-start | bytes 786440 | tf_op jit(solution)/shard_map/ppermute | solution.py:199
  146.6 2.7 %collective-permute-start.11 = (bf16[192,512]{1,0:T(8,128)(2,1)S(1)}, bf16[192,512]{1,0:T(8,128)(2,1)S(1)}, u32[]{:S(2)}, u32[]{:S(2)}) collective-permute-start(bf16[192,512]{1,0:T(8,128)(2,1)S(1)} %hidden.1.mine_ref), channel_id=1, source_target_pairs={{0,1},{1,0},{2,3},{3,2},{4,5},{5,4},{6,7},{7,6},{8,9},{9,8},{10,11... | collective-permute-start | bytes 589832 | tf_op jit(solution)/shard_map/ppermute | solution.py:203
  166.7 11.7 %collective-permute-start.20 = (bf16[96,256]{1,0:T(8,128)(2,1)S(1)}, bf16[96,256]{1,0:T(8,128)(2,1)S(1)}, u32[]{:S(2)}, u32[]{:S(2)}) collective-permute-start(bf16[96,256]{1,0:T(8,128)(2,1)S(1)} %reduce_sum.12), channel_id=1, source_target_pairs={{0,0},{1,1},{2,46},{3,47},{4,76},{5,77},{6,106},{7,107},{8,136},{9... | collective-permute-start | bytes 147464 | tf_op jit(solution)/shard_map/ppermute | solution.py:457

commit v4 on v3

--- a/solution.py
+++ b/solution.py
@@ -19,7 +19,7 @@
 
 
 def attn_kernel(h0_ref, core_ref, rate_ref, bias_ref, tok_ref, mg_ref, wq_hbm, wk_hbm, wv_hbm, wg_hbm, wd_hbm, wb_hbm, wo_hbm, og_ref, st_hbm,
-                ns_hbm, keep_ref, give_ref, wo, w4, w2, st, xn, vv, od, ex, e2, sem_w, sem_in, sem_out):
+                kept_ref, keep_ref, give_ref, wo, w4, w2, st, xn, vv, od, ex, e2, sem_w, sem_in):
     rows = tok_ref.shape[1]
     width = tok_ref.shape[2]
     parts = tok_ref.shape[0]
@@ -28,11 +28,8 @@
     loads += [pltpu.make_async_copy(src, w2.at[i], sem_w.at[4 + i]) for i, src in enumerate((wd_hbm, wb_hbm))]
     loads += [pltpu.make_async_copy(wo_hbm, wo, sem_w.at[6])]
     cin = pltpu.make_async_copy(st_hbm, st, sem_in)
-    for i in (1, 0, 4, 5, 2):
-        loads[i].start()
-    cin.start()
-    loads[3].start()
-    loads[6].start()
+    loads[1].start()
+    loads[0].start()
     ei = lax.broadcasted_iota(jnp.int32, e2.shape, 0)
     ec = lax.broadcasted_iota(jnp.int32, e2.shape, 1)
     e2[...] = jnp.where((ei & 63) == (ec >> 6), 1.0, 0.0).astype(BF16)
@@ -40,6 +37,9 @@
     for t in range(parts):
         x = tok_ref[t].astype(F32)
         ss = ss + x * x
+    for i in (4, 5, 2):
+        loads[i].start()
+    cin.start()
     r = lax.rsqrt(jnp.sum(ss, axis=-1, keepdims=True) / (parts * width) + EPS)
     for t in range(parts):
         xn[:, t * width:(t + 1) * width] = (tok_ref[t].astype(F32) * r * mg_ref[t]).astype(BF16)
@@ -73,6 +73,9 @@
     k = proj(1)
     ks = k * lax.rsqrt(spread(halves(k * k)) + EPS)
     expand(ks, 0)
+    kept_ref[0] = ks
+    loads[3].start()
+    loads[6].start()
     q = proj(0)
     qs = q * lax.rsqrt(spread(halves(q * q)) + EPS) * (64 ** -0.5)
     expand(qs, 2)
@@ -96,26 +99,22 @@
         b = jnp.sum(jnp.where(sel, pb, 0.0), axis=-1, keepdims=True)
         stren = 1.0 / (1.0 + jnp.exp(-b))
         od[h, 0] = jnp.broadcast_to(dec, (rows, 128))
+        kept_ref[3 + h] = jnp.broadcast_to(dec, (rows, 128))
         od[h, 1] = jnp.broadcast_to(stren, (rows, 128))
         od[h, 2] = jnp.broadcast_to(kq[h], (rows, 128))
     cin.wait()
-
-    def out_copy(bt):
-        return pltpu.make_async_copy(st.at[pl.ds(bt * 512, 512), :], ns_hbm.at[pl.ds(bt * 512, 512), :], sem_out)
 
     def body(bt, _):
         r0 = pl.multiple_of(bt * 8, 8)
         for h in range(2):
             rec = jnp.zeros((8, 128), F32)
             out = jnp.zeros((8, 128), F32)
-            terms = []
             for j in range(32):
                 s = st[pl.ds(bt * 512 + 2 * j + h, 8, stride=64), :]
                 ke = ex[h, pl.ds(r0, 8), j * 128:(j + 1) * 128]
                 qe = ex[2 + h, pl.ds(r0, 8), j * 128:(j + 1) * 128]
                 rec = rec + s * ke
                 out = out + s * qe
-                terms.append(s)
             rec = rec + pltpu.roll(rec, 64, 1)
             out = out + pltpu.roll(out, 64, 1)
             dec = od[h, 0, pl.ds(r0, 8), :]
@@ -123,14 +122,7 @@
             kq8 = od[h, 2, pl.ds(r0, 8), :]
             delta = stren * (vv[h, pl.ds(r0, 8), :] - dec * rec)
             od[h, 3, pl.ds(r0, 8), :] = dec * out + kq8 * delta
-            for j in range(32):
-                ke = ex[h, pl.ds(r0, 8), j * 128:(j + 1) * 128]
-                st[pl.ds(bt * 512 + 2 * j + h, 8, stride=64), :] = dec * terms[j] + ke * delta
-
-        @pl.when(bt > 0)
-        def _():
-            out_copy(bt - 1).start()
-
+            kept_ref[1 + h, pl.ds(r0, 8), :] = delta
         return 0
 
     lax.fori_loop(0, nt, body, 0)
@@ -146,13 +138,6 @@
         for ref, side in ((give_ref, 1 - core), (keep_ref, core)):
             cols = wo[:, pl.ds(pl.multiple_of((2 * i + side) * width, width), width)]
             ref[i] = jnp.dot(head_out, cols, preferred_element_type=F32).astype(BF16)
-    out_copy(nt - 1).start()
-
-    def finish(bt, _):
-        out_copy(bt).wait()
-        return 0
-
-    lax.fori_loop(0, nt, finish, 0)
 
 
 def attn(tok, h0, core, wq, wk, wv, wg, wd, wb, wo, rate, bias, mix_gain, out_gain, state):
@@ -163,11 +148,11 @@
     vm = pl.BlockSpec(memory_space=pltpu.VMEM)
     sm = pl.BlockSpec(memory_space=pltpu.SMEM)
     an = pl.BlockSpec(memory_space=pl.ANY)
-    ns, keep, give = pl.pallas_call(
+    kept, keep, give = pl.pallas_call(
         attn_kernel,
-        out_shape=(jax.ShapeDtypeStruct((rows * 64, 128), F32), jax.ShapeDtypeStruct((8, rows, width), BF16), jax.ShapeDtypeStruct((8, rows, width), BF16)),
+        out_shape=(jax.ShapeDtypeStruct((5, rows, 128), F32), jax.ShapeDtypeStruct((8, rows, width), BF16), jax.ShapeDtypeStruct((8, rows, width), BF16)),
         in_specs=[sm, sm, sm, sm, vm, vm] + [an] * 7 + [vm, an],
-        out_specs=(an, vm, vm),
+        out_specs=(vm, vm, vm),
         scratch_shapes=[
             pltpu.VMEM(wo.shape, BF16),
             pltpu.VMEM((4,) + wq.shape, BF16),
@@ -180,14 +165,45 @@
             pltpu.VMEM((128, 4096), BF16),
             pltpu.SemaphoreType.DMA((7,)),
             pltpu.SemaphoreType.DMA,
-            pltpu.SemaphoreType.DMA,
         ],
         compiler_params=pltpu.CompilerParams(vmem_limit_bytes=56 * 1024 * 1024),
         cost_estimate=pl.CostEstimate(flops=2 * 96 * 4096 * 600, bytes_accessed=12_000_000, transcendentals=50000),
         name="attn",
     )(h0, core, rate, bias, tok, mg, wq, wk, wv, wg, wd.T, wb.T, wo, out_gain.reshape(1, 64), st)
-    ns = ns.reshape(rows, 32, heads, 128).transpose(0, 2, 1, 3).reshape(rows, heads, 4096)
-    return ns, keep, give
+    return kept, keep, give
+
+
+def state_kernel(kept_ref, st_ref, *refs):
+    out_ref = refs[-1]
+    lane = lax.broadcasted_iota(jnp.int32, (8, 128), 1)
+    upper = lane >> 6
+    for h in range(2):
+        key = kept_ref[0]
+        delta = kept_ref[1 + h]
+        decay = kept_ref[3 + h]
+        for j in range(32):
+            at = pl.ds(2 * j + h, 8, stride=64)
+            spread = jnp.take_along_axis(key, upper + (64 * h + 2 * j), axis=1)
+            out_ref[at, :] = decay * st_ref[at, :] + spread * delta
+
+
+def next_state(kept, state, base, steps, partial=None):
+    rows, heads, _ = state.shape
+    st = state.reshape(rows, heads, 32, 128).transpose(0, 2, 1, 3).reshape(rows * 64, 128)
+    block = pl.BlockSpec((512, 128), lambda i: (i + base, 0))
+    operands = (kept, st) if partial is None else (kept, st, partial)
+    return pl.pallas_call(
+        state_kernel,
+        grid=(steps,),
+        out_shape=jax.ShapeDtypeStruct((rows * 64, 128), F32),
+        in_specs=[pl.BlockSpec((5, 8, 128), lambda i: (0, i + base, 0)), block]
+        + [pl.BlockSpec(memory_space=pl.ANY)] * (len(operands) - 2),
+        out_specs=block,
+        input_output_aliases={} if partial is None else {2: 0},
+        compiler_params=pltpu.CompilerParams(vmem_limit_bytes=56 * 1024 * 1024),
+        cost_estimate=pl.CostEstimate(flops=10_000_000, bytes_accessed=3_200_000, transcendentals=0),
+        name="next",
+    )(*operands)
 
 
 VM = pl.BlockSpec(memory_space=pltpu.VMEM)
@@ -203,7 +219,7 @@
     return lax.ppermute(array, "c", [(0, 1), (1, 0)])
 
 
-def out_kernel(tok_ref, gain_ref, parts_ref, resid_ref, send_ref):
+def out_kernel(tp_ref, tok_ref, gain_ref, parts_ref, resid_ref, send_ref):
     rows, width = tok_ref.shape
     acc = tok_ref[...].astype(F32)
     for i in range(parts_ref.shape[0]):
@@ -212,7 +228,7 @@
     squares = jnp.sum(acc * acc, axis=-1, keepdims=True)
     eye = lax.broadcasted_iota(jnp.int32, (rows, 128), 0) == lax.broadcasted_iota(jnp.int32, (rows, 128), 1)
     flat = jnp.sum(jnp.where(eye, squares, 0.0), axis=0, keepdims=True)
-    scaled = (acc * gain_ref[...]).astype(BF16)
+    scaled = (acc * gain_ref[tp_ref[0]]).astype(BF16)
     extra = jnp.broadcast_to(flat, (PAD, 128)).astype(BF16)
     blank = jnp.zeros((PAD, width - 128), BF16)
     for i in range(send_ref.shape[0]):
@@ -221,28 +237,30 @@
         send_ref[i, rows:, 128:] = blank
 
 
-def residual(tokens, gain, parts):
+def residual(tp, tokens, gain, parts):
     rows, width = tokens.shape
     return pl.pallas_call(
         out_kernel,
         out_shape=(jax.ShapeDtypeStruct((rows, width), F32), jax.ShapeDtypeStruct((16, rows + PAD, width), BF16)),
-        in_specs=[VM] * 3,
+        in_specs=[SM] + [VM] * 3,
         out_specs=(VM, VM),
         compiler_params=pltpu.CompilerParams(vmem_limit_bytes=16 * 1024 * 1024),
         cost_estimate=pl.CostEstimate(flops=1_000_000, bytes_accessed=2_000_000, transcendentals=0),
         name="out",
-    )(tokens, gain, parts)
-
-
-def up_kernel(z_ref, mine_ref, other_ref, wm_ref, wo_ref, *outs):
+    )(tp.reshape(1), tokens, gain, parts)
+
+
+def up_kernel(z_ref, c_ref, mine_ref, other_ref, wu_ref, wo_ref, *outs):
     rows = mine_ref.shape[1] - PAD
     width = mine_ref.shape[2]
+    wide = wo_ref.shape[1]
+    w_mine = wu_ref[:, pl.ds(pl.multiple_of(c_ref[0] * wide, wide), wide)]
     for o in (4, 3, 5, 2, 6, 1, 7, 0):
         at = (z_ref[0] + o) & 7
         own = mine_ref[pl.ds(2 * at, 2)]
         his = other_ref[pl.ds(2 * at, 2)]
         product = (
-            jnp.dot(own[:, :rows].reshape(2 * rows, width), wm_ref[...], preferred_element_type=F32)
+            jnp.dot(own[:, :rows].reshape(2 * rows, width), w_mine, preferred_element_type=F32)
             + jnp.dot(his[:, :rows].reshape(2 * rows, width), wo_ref[...], preferred_element_type=F32)
         ).astype(BF16)
         squares = own[:, rows:, :128].astype(F32) + his[:, rows:, :128].astype(F32)
@@ -258,19 +276,19 @@
         right[2 * rows :, shift : shift + side] = jnp.zeros((PAD, side), BF16)
 
 
-def up_product(z, mine, other, w_mine, w_other):
+def up_product(z, c, mine, other, w_up, w_other):
     rows = mine.shape[1] - PAD
     return pl.pallas_call(
         up_kernel,
         out_shape=tuple(
-            jax.ShapeDtypeStruct((2 * rows + PAD, w_mine.shape[1] // (2 if o in (4, 8) else 1)), BF16) for o in range(9)
+            jax.ShapeDtypeStruct((2 * rows + PAD, w_other.shape[1] // (2 if o in (4, 8) else 1)), BF16) for o in range(9)
         ),
-        in_specs=[SM] + [VM] * 4,
+        in_specs=[SM, SM] + [VM] * 4,
         out_specs=tuple([VM] * 9),
         compiler_params=pltpu.CompilerParams(vmem_limit_bytes=24 * 1024 * 1024),
         cost_estimate=pl.CostEstimate(flops=2 * 1536 * 512 * 512, bytes_accessed=4_000_000, transcendentals=0),
         name="up",
-    )(z.reshape(1), mine, other, w_mine, w_other)
+    )(z.reshape(1), c.reshape(1), mine, other, w_up, w_other)
 
 
 def hidden_kernel(a_ref, b_ref, c_ref, out_ref):
@@ -313,8 +331,40 @@
     )(one, two)
 
 
-def add(one, two):
-    return (one.astype(F32) + two.astype(F32)).astype(BF16)
+def total_kernel(parts_ref, out_ref):
+    total = parts_ref[0].astype(F32)
+    for i in range(1, parts_ref.shape[0]):
+        total = total + parts_ref[i].astype(F32)
+    out_ref[...] = total.astype(BF16)
+
+
+def total_of(parts):
+    return pl.pallas_call(
+        total_kernel,
+        out_shape=jax.ShapeDtypeStruct(parts.shape[1:], BF16),
+        in_specs=[VM],
+        out_specs=VM,
+        compiler_params=pltpu.CompilerParams(vmem_limit_bytes=4 * 1024 * 1024),
+        cost_estimate=pl.CostEstimate(flops=500_000, bytes_accessed=900_000, transcendentals=0),
+        name="total",
+    )(parts)
+
+
+def other_half_kernel(c_ref, w_ref, out_ref):
+    half = out_ref.shape[1]
+    out_ref[...] = w_ref[:, pl.ds(pl.multiple_of((1 - c_ref[0]) * half, half), half)]
+
+
+def other_half(c, w):
+    return pl.pallas_call(
+        other_half_kernel,
+        out_shape=jax.ShapeDtypeStruct((w.shape[0], w.shape[1] // 2), BF16),
+        in_specs=[SM, VM],
+        out_specs=VM,
+        compiler_params=pltpu.CompilerParams(vmem_limit_bytes=4 * 1024 * 1024),
+        cost_estimate=pl.CostEstimate(flops=100_000, bytes_accessed=800_000, transcendentals=0),
+        name="other",
+    )(c.reshape(1), w)
 
 
 def half_kernel(start, full_ref, part_ref, out_ref):
@@ -343,9 +393,9 @@
     back = half_sum(blocks[5], back, blocks[4].shape[1])
     back = shifted(back, -1)
     for step in (2, 1):
-        ahead = add(blocks[step], ahead)
+        ahead = pair_sum(blocks[step], ahead)
         ahead = shifted(ahead, 1)
-        back = add(blocks[8 - step], back)
+        back = pair_sum(blocks[8 - step], back)
         back = shifted(back, -1)
     return blocks[0], ahead, back
 
@@ -426,30 +476,32 @@
     w_up,
     w_down,
 ):
-    _, width = tokens.shape
+    rows, width = tokens.shape
     _, _, z, c = (lax.axis_index(axis).astype(jnp.int32) for axis in EVERYWHERE)
     tp = z * 2 + c
-    half = w_up.shape[1] // 2
     everything = lax.all_gather(tokens, TP, axis=0, tiled=False)
-    new_state, keep, give = attn(
+    kept, keep, give = attn(
         everything, (tp * 2).reshape(1), c.reshape(1), w_query, w_key, w_value, w_gate, w_decay, w_beta, w_out,
         decay_rate, decay_bias, mix_gain, out_gain, state,
     )
     took = other_core(give)
     parts = lax.all_to_all(pair_sum(keep, took), "z", 0, 0, tiled=True)
     w_up = tied(w_up, give)
-    up_mine = lax.dynamic_slice_in_dim(w_up, c * half, half, 1)
-    up_other = other_core(lax.dynamic_slice_in_dim(w_up, (1 - c) * half, half, 1))
-    gain = lax.dynamic_slice_in_dim(ffn_gain, tp * width, width, 0).reshape(1, width)
-    resid, send = residual(tokens, gain, parts)
+    up_send = other_half(c, w_up)
+    up_other = other_core(up_send)
+    half_state = next_state(kept, state, 0, 6)
+    resid, send = residual(tp, tokens, ffn_gain.reshape(16, 1, width), parts)
     mine = lax.all_to_all(send, KV, 0, 0, tiled=True)
     theirs = other_core(mine)
-    blocks = up_product(z, mine, theirs, up_mine, up_other)
+    blocks = up_product(z, c, mine, theirs, w_up, up_other)
     down_weights = ring_gather(w_down, everything, None, send, mine)
     hidden = finish_hidden(*ring_sum(blocks))
     down = down_product(z, c, hidden, other_core(hidden), down_weights)
+    half_state = next_state(kept, state, 6, 3, half_state)
+    new_state = next_state(kept, state, 9, 3, half_state)
+    new_state = new_state.reshape(rows, 32, 2, 128).transpose(0, 2, 1, 3).reshape(state.shape)
     down = lax.all_to_all(down, KV, 0, 0, tiled=True)
-    down = down.astype(F32).sum(axis=0).astype(BF16)
+    down = total_of(down)
     routes = [
         (((2 * a + b) * 8 + s) * 2 + k, ((2 * s + b) * 8 + (a - s) % 8) * 2 + k)
         for a in range(8) for b in range(2) for s in range(8) for k in range(2)

time: 179 us -> 182 us (1.017)
  the two profiles are of different devices: /device:TPU:224 before, /device:TPU:32 now
where the time goes in v4:
time: 182 us
  blocking collectives  77 us (42%)
  waiting for transfers between devices  44.3 us (24%)
  starting transfers between devices  32.3 us (18%)
  Pallas kernels  25.5 us (14%)
    ppermute x16, waiting for transfers between devices, shifted(): lax.ppermute(array, axis, [(i, (i + by) % length) for i in range(length)])  41.2 us
    ppermute x16, starting transfers between devices, shifted(): lax.ppermute(array, axis, [(i, (i + by) % length) for i in range(length)])  23 us
    all_gather x1, blocking collectives, layer(): everything = lax.all_gather(tokens, TP, axis=0, tiled=False)  21.6 us
    all_to_all x1, blocking collectives, layer(): mine = lax.all_to_all(send, KV, 0, 0, tiled=True)  21.1 us
    all_to_all x1, blocking collectives, layer(): parts = lax.all_to_all(pair_sum(keep, took), 'z', 0, 0, tiled=True)  19.4 us
    all_to_all x1, blocking collectives, layer(): down = lax.all_to_all(down, KV, 0, 0, tiled=True)  14.8 us
    pallas_call x3, Pallas kernels, next_state(): pl.pallas_call(state_kernel, grid=(steps,), out_shape=jax.ShapeDtypeStruc...  12.4 us
    pallas_call x1, Pallas kernels, attn(): pl.pallas_call(attn_kernel, out_shape=(jax.ShapeDtypeStruct((5, rows, 128...  10.3 us
  transfers between devices with their start and end apart: 21, of which 11 were waited for; matrix products, arithmetic and copies ran while one was open for 0% of the time, Pallas kernels for 8%

profile of v4, /device:TPU:32, one launch (start us, length us, event | category | flops | bytes accessed | tf_op | source)
XLA Modules:
  0.0 181.6 jit_solution(7488806009843929570)
XLA Ops:
  0.6 21.6 %all-gather = bf16[1536,256]{1,0:T(8,128)(2,1)} all-gather(bf16[96,256]{1,0:T(8,128)(2,1)} %tok_ref.1), channel_id=2, replica_groups=mesh['y'=4,'x'=4,'z'=8,'c'=2] {'z','c'}, dimensions={0}, use_global_device_ids=true | all-gather | bytes 835584 | tf_op jit(solution)/shard_map/all_gather | solution.py:482
  22.3 10.3 %attn.1 = (f32[5,96,128]{2,1,0:T(8,128)}, bf16[8,96,256]{2,1,0:T(8,128)(2,1)}, bf16[8,96,256]{2,1,0:T(8,128)(2,1)}) custom-call(s32[1]{0:T(128)} %bitcast.2.h0_ref, s32[1]{0:T(128)} %bitcast.3.core_ref.c_ref, f32[2]{0:T(128)} %rate_ref.1, f32[2]{0:T(128)} %bias_ref.1, bf16[16,96,256]{2,1,0:T(8,128)(2,1)} %bitcast.26, f32[16,1,256]{2,1,0:T(1,128)} %bitcast.29, ...), custom_call_target="tpu_custom_call" | custom-call | flops 471859200 | bytes 12000000 | tf_op jit(solution)/shard_map/attn/pallas_call | solution.py:151
  33.1 1.6 collective-permute-done.two_ref
  34.7 1.0 copy-done.2
  35.7 19.4 %all_to_all.15.parts_ref = bf16[8,96,256]{2,1,0:T(8,128)(2,1)S(1)} all-to-all(bf16[8,96,256]{2,1,0:T(8,128)(2,1)S(1)} %pair.5), channel_id=1, replica_groups=mesh['y'=4,'x'=4,'z'=8,'c'=2] {'z'}, dimensions={0} | all-to-all | bytes 786432 | tf_op jit(solution)/shard_map/all_to_all | solution.py:488
  55.3 21.1 %all_to_all.16.mine_ref = bf16[16,104,256]{2,1,0:T(8,128)(2,1)S(1)} all-to-all(bf16[16,104,256]{2,1,0:T(8,128)(2,1)S(1)} %get-tuple-element.26), channel_id=1, replica_groups=mesh['y'=4,'x'=4,'z'=8,'c'=2] {'y','x'}, dimensions={0} | all-to-all | bytes 1703936 | tf_op jit(solution)/shard_map/all_to_all | solution.py:494
  76.4 1.8 collective-permute-start.12
  78.4 12.3 %collective-permute-done.12.refs_1_ = bf16[1024,256]{1,0:T(8,128)(2,1)S(1)} collective-permute-done((bf16[1024,256]{1,0:T(8,128)(2,1)S(1)}, bf16[1024,256]{1,0:T(8,128)(2,1)S(1)}, u32[]{:S(2)}, u32[]{:S(2)}) %collective-permute-start.12) | collective-permute-done | bytes 524320 | tf_op jit(solution)/shard_map/ppermute | solution.py:215
  90.8 1.8 collective-permute-start.13
  92.9 1.5 collective-permute-done.2.wo_ref
  94.4 1.0 up.1
  95.5 2.0 %collective-permute-start.7 = (bf16[200,256]{1,0:T(8,128)(2,1)S(1)}, bf16[200,256]{1,0:T(8,128)(2,1)S(1)}, u32[]{:S(2)}, u32[]{:S(2)}) collective-permute-start(bf16[200,256]{1,0:T(8,128)(2,1)S(1)} %get-tuple-element.36), channel_id=1, source_target_pairs={{0,14},{2,0},{4,2},{6,4},{8,6},{10,8},{12,10},{14,12},{1,15},{3,1}... | collective-permute-start | bytes 307208 | tf_op jit(solution)/shard_map/ppermute | solution.py:215
  97.5 10.4 %collective-permute-done.3.part_ref = bf16[200,256]{1,0:T(8,128)(2,1)S(1)} collective-permute-done((bf16[200,256]{1,0:T(8,128)(2,1)S(1)}, bf16[200,256]{1,0:T(8,128)(2,1)S(1)}, u32[]{:S(2)}, u32[]{:S(2)}) %collective-permute-start.3) | collective-permute-done | bytes 102432 | tf_op jit(solution)/shard_map/ppermute | solution.py:215
  108.0 0.5 collective-permute-start.4
  108.5 2.8 %collective-permute-start.8 = (bf16[200,512]{1,0:T(8,128)(2,1)S(1)}, bf16[200,512]{1,0:T(8,128)(2,1)S(1)}, u32[]{:S(2)}, u32[]{:S(2)}) collective-permute-start(bf16[200,512]{1,0:T(8,128)(2,1)S(1)} %half.3), channel_id=1, source_target_pairs={{0,14},{2,0},{4,2},{6,4},{8,6},{10,8},{12,10},{14,12},{1,15},{3,1}... | collective-permute-start | bytes 614408 | tf_op jit(solution)/shard_map/ppermute | solution.py:215
  111.4 3.2 %collective-permute-start.16 = (bf16[1024,256]{1,0:T(8,128)(2,1)S(1)}, bf16[1024,256]{1,0:T(8,128)(2,1)S(1)}, u32[]{:S(2)}, u32[]{:S(2)}) collective-permute-start(bf16[1024,256]{1,0:T(8,128)(2,1)S(1)} %collective-permute-done.13.refs_2_), channel_id=1, source_target_pairs={{0,14},{2,0},{4,2},{6,4},{8,6},{10,8},{12,10},{14,12},{1,15},{3,1}... | collective-permute-start | bytes 1572872 | tf_op jit(solution)/shard_map/ppermute | solution.py:215
  114.6 0.8 collective-permute-done.4.two_ref
  115.5 0.9 collective-permute-done.8.two_ref
  116.4 3.7 %collective-permute-start.9 = (bf16[200,512]{1,0:T(8,128)(2,1)S(1)}, bf16[200,512]{1,0:T(8,128)(2,1)S(1)}, u32[]{:S(2)}, u32[]{:S(2)}) collective-permute-start(bf16[200,512]{1,0:T(8,128)(2,1)S(1)} %pair.8), channel_id=1, source_target_pairs={{0,14},{2,0},{4,2},{6,4},{8,6},{10,8},{12,10},{14,12},{1,15},{3,1}... | collective-permute-start | bytes 614408 | tf_op jit(solution)/shard_map/ppermute | solution.py:215
  120.2 10.7 %collective-permute-done.5.two_ref = bf16[200,512]{1,0:T(8,128)(2,1)S(1)} collective-permute-done((bf16[200,512]{1,0:T(8,128)(2,1)S(1)}, bf16[200,512]{1,0:T(8,128)(2,1)S(1)}, u32[]{:S(2)}, u32[]{:S(2)}) %collective-permute-start.5) | collective-permute-done | bytes 204832 | tf_op jit(solution)/shard_map/ppermute | solution.py:215
  131.2 2.9 %collective-permute-start.10 = (bf16[200,512]{1,0:T(8,128)(2,1)S(1)}, bf16[200,512]{1,0:T(8,128)(2,1)S(1)}, u32[]{:S(2)}, u32[]{:S(2)}) collective-permute-start(bf16[200,512]{1,0:T(8,128)(2,1)S(1)} %pair.9), channel_id=1, source_target_pairs={{0,14},{2,0},{4,2},{6,4},{8,6},{10,8},{12,10},{14,12},{1,15},{3,1}... | collective-permute-start | bytes 614408 | tf_op jit(solution)/shard_map/ppermute | solution.py:215
  134.1 3.3 %collective-permute-start.18 = (bf16[512,256]{1,0:T(8,128)(2,1)S(1)}, bf16[512,256]{1,0:T(8,128)(2,1)S(1)}, u32[]{:S(2)}, u32[]{:S(2)}) collective-permute-start(bf16[512,256]{1,0:T(8,128)(2,1)S(1)} %slice.6), channel_id=1, source_target_pairs={{0,14},{2,0},{4,2},{6,4},{8,6},{10,8},{12,10},{14,12},{1,15},{3,1}... | collective-permute-start | bytes 786440 | tf_op jit(solution)/shard_map/ppermute | solution.py:215
  137.8 1.3 collective-permute-done.10.c_ref
  139.4 3.6 %collective-permute-done.18.refs_4_ = bf16[512,256]{1,0:T(8,128)(2,1)S(1)} collective-permute-done((bf16[512,256]{1,0:T(8,128)(2,1)S(1)}, bf16[512,256]{1,0:T(8,128)(2,1)S(1)}, u32[]{:S(2)}, u32[]{:S(2)}) %collective-permute-start.18) | collective-permute-done | bytes 262176 | tf_op jit(solution)/shard_map/ppermute | solution.py:215
  143.0 0.9 collective-permute-done.19.refs_5_
  143.9 1.0 down.1
  144.9 14.8 %all_to_all.17.parts_ref = bf16[16,96,256]{2,1,0:T(8,128)(2,1)S(1)} all-to-all(bf16[16,96,256]{2,1,0:T(8,128)(2,1)S(1)} %down.1), channel_id=1, replica_groups=mesh['y'=4,'x'=4,'z'=8,'c'=2] {'y','x'}, dimensions={0} | all-to-all | bytes 1572864 | tf_op jit(solution)/shard_map/all_to_all | solution.py:503
  159.9 8.7 %collective-permute-start.20 = (bf16[96,256]{1,0:T(8,128)(2,1)S(1)}, bf16[96,256]{1,0:T(8,128)(2,1)S(1)}, u32[]{:S(2)}, u32[]{:S(2)}) collective-permute-start(bf16[96,256]{1,0:T(8,128)(2,1)S(1)} %total.1), channel_id=1, source_target_pairs={{0,0},{1,1},{2,46},{3,47},{4,76},{5,77},{6,106},{7,107},{8,136},{9... | collective-permute-start | bytes 147464 | tf_op jit(solution)/shard_map/ppermute | solution.py:509
  168.5 5.5 %next.3.refs_0_ = f32[6144,128]{1,0:T(8,128)} custom-call(f32[5,96,128]{2,1,0:T(8,128)} %get-tuple-element.43.kept_ref, f32[6144,128]{1,0:T(8,128)} %bitcast.22), custom_call_target="tpu_custom_call" | custom-call | flops 10000000 | bytes 3200000 | tf_op jit(solution)/shard_map/next/pallas_call | solution.py:195
  174.1 3.4 %next.4.refs_0_ = f32[6144,128]{1,0:T(8,128)} custom-call(f32[5,96,128]{2,1,0:T(8,128)} %get-tuple-element.43.kept_ref, f32[6144,128]{1,0:T(8,128)} %bitcast.23, f32[6144,128]{1,0:T(8,128)} %next.3.refs_0_), custom_call_target="tpu_custom_call", output_to_operand_aliasing={{}: (2, {})} | custom-call | flops 10000000 | bytes 3200000 | tf_op jit(solution)/shard_map/next/pallas_call | solution.py:195
  177.5 3.4 %next.5 = f32[6144,128]{1,0:T(8,128)} custom-call(f32[5,96,128]{2,1,0:T(8,128)} %get-tuple-element.43.kept_ref, f32[6144,128]{1,0:T(8,128)} %bitcast.24, f32[6144,128]{1,0:T(8,128)} %next.4.refs_0_), custom_call_target="tpu_custom_call", output_to_operand_aliasing={{}: (2, {})} | custom-call | flops 10000000 | bytes 3200000 | tf_op jit(solution)/shard_map/next/pallas_call | solution.py:195
  180.9 0.6 add_convert_fusion
  (44 shorter events, 2.8 us)
Async XLA Ops:
  22.3 32.9 %copy-start.3 = (bf16[96,256]{1,0:T(8,128)(2,1)S(1)}, bf16[96,256]{1,0:T(8,128)(2,1)}, u32[]{:S(2)}) copy-start(bf16[96,256]{1,0:T(8,128)(2,1)} %tok_ref.1) | copy-start | bytes 147460
  22.3 32.9 %copy-start.4 = (f32[4096]{0:T(1024)S(1)}, f32[4096]{0:T(1024)}, u32[]{:S(2)}) copy-start(f32[4096]{0:T(1024)} %param.29) | copy-start | bytes 49156
  32.6 43.8 %copy-start = (bf16[1024,256]{1,0:T(8,128)(2,1)S(1)}, bf16[1024,256]{1,0:T(8,128)(2,1)}, u32[]{:S(2)}) copy-start(bf16[1024,256]{1,0:T(8,128)(2,1)} %refs_0_.1) | copy-start | bytes 1572868
  32.6 60.2 %copy-start.1 = (bf16[256,1024]{1,0:T(8,128)(2,1)S(1)}, bf16[256,1024]{1,0:T(8,128)(2,1)}, u32[]{:S(2)}) copy-start(bf16[256,1024]{1,0:T(8,128)(2,1)} %wu_ref) | copy-start | bytes 1572868
  32.6 2.0 %collective-permute-start = (bf16[8,96,256]{2,1,0:T(8,128)(2,1)}, bf16[8,96,256]{2,1,0:T(8,128)(2,1)S(1)}, u32[]{:S(2)}, u32[]{:S(2)}) collective-permute-start(bf16[8,96,256]{2,1,0:T(8,128)(2,1)} %get-tuple-element.24), channel_id=1, source_target_pairs={{0,1},{1,0},{2,3},{3,2},{4,5},{5,4},{6,7},{7,6},{8,9},{9,8},{10,11... | collective-permute-start | bytes 1179656 | tf_op jit(solution)/shard_map/ppermute | solution.py:219
  34.6 1.0 copy-start.2
  76.4 18.0 %collective-permute-start.1 = (bf16[16,104,256]{2,1,0:T(8,128)(2,1)S(1)}, bf16[16,104,256]{2,1,0:T(8,128)(2,1)S(1)}, u32[]{:S(2)}, u32[]{:S(2)}) collective-permute-start(bf16[16,104,256]{2,1,0:T(8,128)(2,1)S(1)} %all_to_all.16.mine_ref), channel_id=1, source_target_pairs={{0,1},{1,0},{2,3},{3,2},{4,5},{5,4},{6,7},{7,6},{8,9},{9,8},{10,11... | collective-permute-start | bytes 2555912 | tf_op jit(solution)/shard_map/ppermute | solution.py:219
  76.4 14.3 %collective-permute-start.12 = (bf16[1024,256]{1,0:T(8,128)(2,1)S(1)}, bf16[1024,256]{1,0:T(8,128)(2,1)S(1)}, u32[]{:S(2)}, u32[]{:S(2)}) collective-permute-start(bf16[1024,256]{1,0:T(8,128)(2,1)S(1)} %copy-done), channel_id=1, source_target_pairs={{0,14},{2,0},{4,2},{6,4},{8,6},{10,8},{12,10},{14,12},{1,15},{3,1}... | collective-permute-start | bytes 1572872 | tf_op jit(solution)/shard_map/ppermute | solution.py:215
  78.2 14.3 %collective-permute-start.14 = (bf16[1024,256]{1,0:T(8,128)(2,1)S(1)}, bf16[1024,256]{1,0:T(8,128)(2,1)S(1)}, u32[]{:S(2)}, u32[]{:S(2)}) collective-permute-start(bf16[1024,256]{1,0:T(8,128)(2,1)S(1)} %copy-done), channel_id=1, source_target_pairs={{0,2},{2,4},{4,6},{6,8},{8,10},{10,12},{12,14},{14,0},{1,3},{3,5},... | collective-permute-start | bytes 1572872 | tf_op jit(solution)/shard_map/ppermute | solution.py:215
  90.8 20.6 %collective-permute-start.13 = (bf16[1024,256]{1,0:T(8,128)(2,1)S(1)}, bf16[1024,256]{1,0:T(8,128)(2,1)S(1)}, u32[]{:S(2)}, u32[]{:S(2)}) collective-permute-start(bf16[1024,256]{1,0:T(8,128)(2,1)S(1)} %collective-permute-done.12.refs_1_), channel_id=1, source_target_pairs={{0,14},{2,0},{4,2},{6,4},{8,6},{10,8},{12,10},{14,12},{1,15},{3,1}... | collective-permute-start | bytes 1572872 | tf_op jit(solution)/shard_map/ppermute | solution.py:215
  92.5 18.8 %collective-permute-start.15 = (bf16[1024,256]{1,0:T(8,128)(2,1)S(1)}, bf16[1024,256]{1,0:T(8,128)(2,1)S(1)}, u32[]{:S(2)}, u32[]{:S(2)}) collective-permute-start(bf16[1024,256]{1,0:T(8,128)(2,1)S(1)} %collective-permute-done.14.refs_8_), channel_id=1, source_target_pairs={{0,2},{2,4},{4,6},{6,8},{8,10},{10,12},{12,14},{14,0},{1,3},{3,5},... | collective-permute-start | bytes 1572872 | tf_op jit(solution)/shard_map/ppermute | solution.py:215
  92.8 1.6 collective-permute-start.2
  95.4 12.5 %collective-permute-start.3 = (bf16[200,256]{1,0:T(8,128)(2,1)S(1)}, bf16[200,256]{1,0:T(8,128)(2,1)S(1)}, u32[]{:S(2)}, u32[]{:S(2)}) collective-permute-start(bf16[200,256]{1,0:T(8,128)(2,1)S(1)} %get-tuple-element.32), channel_id=1, source_target_pairs={{0,2},{2,4},{4,6},{6,8},{8,10},{10,12},{12,14},{14,0},{1,3},{3,5},... | collective-permute-start | bytes 307208 | tf_op jit(solution)/shard_map/ppermute | solution.py:215
  95.5 13.0 %collective-permute-start.7 = (bf16[200,256]{1,0:T(8,128)(2,1)S(1)}, bf16[200,256]{1,0:T(8,128)(2,1)S(1)}, u32[]{:S(2)}, u32[]{:S(2)}) collective-permute-start(bf16[200,256]{1,0:T(8,128)(2,1)S(1)} %get-tuple-element.36), channel_id=1, source_target_pairs={{0,14},{2,0},{4,2},{6,4},{8,6},{10,8},{12,10},{14,12},{1,15},{3,1}... | collective-permute-start | bytes 307208 | tf_op jit(solution)/shard_map/ppermute | solution.py:215
  108.0 7.4 %collective-permute-start.4 = (bf16[200,512]{1,0:T(8,128)(2,1)S(1)}, bf16[200,512]{1,0:T(8,128)(2,1)S(1)}, u32[]{:S(2)}, u32[]{:S(2)}) collective-permute-start(bf16[200,512]{1,0:T(8,128)(2,1)S(1)} %half.2), channel_id=1, source_target_pairs={{0,2},{2,4},{4,6},{6,8},{8,10},{10,12},{12,14},{14,0},{1,3},{3,5},... | collective-permute-start | bytes 614408 | tf_op jit(solution)/shard_map/ppermute | solution.py:215
  108.5 7.8 %collective-permute-start.8 = (bf16[200,512]{1,0:T(8,128)(2,1)S(1)}, bf16[200,512]{1,0:T(8,128)(2,1)S(1)}, u32[]{:S(2)}, u32[]{:S(2)}) collective-permute-start(bf16[200,512]{1,0:T(8,128)(2,1)S(1)} %half.3), channel_id=1, source_target_pairs={{0,14},{2,0},{4,2},{6,4},{8,6},{10,8},{12,10},{14,12},{1,15},{3,1}... | collective-permute-start | bytes 614408 | tf_op jit(solution)/shard_map/ppermute | solution.py:215
  111.4 22.8 %collective-permute-start.16 = (bf16[1024,256]{1,0:T(8,128)(2,1)S(1)}, bf16[1024,256]{1,0:T(8,128)(2,1)S(1)}, u32[]{:S(2)}, u32[]{:S(2)}) collective-permute-start(bf16[1024,256]{1,0:T(8,128)(2,1)S(1)} %collective-permute-done.13.refs_2_), channel_id=1, source_target_pairs={{0,14},{2,0},{4,2},{6,4},{8,6},{10,8},{12,10},{14,12},{1,15},{3,1}... | collective-permute-start | bytes 1572872 | tf_op jit(solution)/shard_map/ppermute | solution.py:215
  114.6 19.5 %collective-permute-start.17 = (bf16[1024,256]{1,0:T(8,128)(2,1)S(1)}, bf16[1024,256]{1,0:T(8,128)(2,1)S(1)}, u32[]{:S(2)}, u32[]{:S(2)}) collective-permute-start(bf16[1024,256]{1,0:T(8,128)(2,1)S(1)} %collective-permute-done.15.refs_7_), channel_id=1, source_target_pairs={{0,2},{2,4},{4,6},{6,8},{8,10},{10,12},{12,14},{14,0},{1,3},{3,5},... | collective-permute-start | bytes 1572872 | tf_op jit(solution)/shard_map/ppermute | solution.py:215
  115.4 15.4 %collective-permute-start.5 = (bf16[200,512]{1,0:T(8,128)(2,1)S(1)}, bf16[200,512]{1,0:T(8,128)(2,1)S(1)}, u32[]{:S(2)}, u32[]{:S(2)}) collective-permute-start(bf16[200,512]{1,0:T(8,128)(2,1)S(1)} %pair.6), channel_id=1, source_target_pairs={{0,2},{2,4},{4,6},{6,8},{8,10},{10,12},{12,14},{14,0},{1,3},{3,5},... | collective-permute-start | bytes 614408 | tf_op jit(solution)/shard_map/ppermute | solution.py:215
  116.4 14.7 %collective-permute-start.9 = (bf16[200,512]{1,0:T(8,128)(2,1)S(1)}, bf16[200,512]{1,0:T(8,128)(2,1)S(1)}, u32[]{:S(2)}, u32[]{:S(2)}) collective-permute-start(bf16[200,512]{1,0:T(8,128)(2,1)S(1)} %pair.8), channel_id=1, source_target_pairs={{0,14},{2,0},{4,2},{6,4},{8,6},{10,8},{12,10},{14,12},{1,15},{3,1}... | collective-permute-start | bytes 614408 | tf_op jit(solution)/shard_map/ppermute | solution.py:215
  130.9 6.9 %collective-permute-start.6 = (bf16[200,512]{1,0:T(8,128)(2,1)S(1)}, bf16[200,512]{1,0:T(8,128)(2,1)S(1)}, u32[]{:S(2)}, u32[]{:S(2)}) collective-permute-start(bf16[200,512]{1,0:T(8,128)(2,1)S(1)} %pair.7), channel_id=1, source_target_pairs={{0,2},{2,4},{4,6},{6,8},{8,10},{10,12},{12,14},{14,0},{1,3},{3,5},... | collective-permute-start | bytes 614408 | tf_op jit(solution)/shard_map/ppermute | solution.py:215
  131.2 8.0 %collective-permute-start.10 = (bf16[200,512]{1,0:T(8,128)(2,1)S(1)}, bf16[200,512]{1,0:T(8,128)(2,1)S(1)}, u32[]{:S(2)}, u32[]{:S(2)}) collective-permute-start(bf16[200,512]{1,0:T(8,128)(2,1)S(1)} %pair.9), channel_id=1, source_target_pairs={{0,14},{2,0},{4,2},{6,4},{8,6},{10,8},{12,10},{14,12},{1,15},{3,1}... | collective-permute-start | bytes 614408 | tf_op jit(solution)/shard_map/ppermute | solution.py:215
  134.1 8.9 %collective-permute-start.18 = (bf16[512,256]{1,0:T(8,128)(2,1)S(1)}, bf16[512,256]{1,0:T(8,128)(2,1)S(1)}, u32[]{:S(2)}, u32[]{:S(2)}) collective-permute-start(bf16[512,256]{1,0:T(8,128)(2,1)S(1)} %slice.6), channel_id=1, source_target_pairs={{0,14},{2,0},{4,2},{6,4},{8,6},{10,8},{12,10},{14,12},{1,15},{3,1}... | collective-permute-start | bytes 786440 | tf_op jit(solution)/shard_map/ppermute | solution.py:215
  137.4 6.4 %collective-permute-start.19 = (bf16[512,256]{1,0:T(8,128)(2,1)S(1)}, bf16[512,256]{1,0:T(8,128)(2,1)S(1)}, u32[]{:S(2)}, u32[]{:S(2)}) collective-permute-start(bf16[512,256]{1,0:T(8,128)(2,1)S(1)} %slice.7), channel_id=1, source_target_pairs={{0,2},{2,4},{4,6},{6,8},{8,10},{10,12},{12,14},{14,0},{1,3},{3,5},... | collective-permute-start | bytes 786440 | tf_op jit(solution)/shard_map/ppermute | solution.py:215
  139.3 4.6 %collective-permute-start.11 = (bf16[192,512]{1,0:T(8,128)(2,1)S(1)}, bf16[192,512]{1,0:T(8,128)(2,1)S(1)}, u32[]{:S(2)}, u32[]{:S(2)}) collective-permute-start(bf16[192,512]{1,0:T(8,128)(2,1)S(1)} %hidden.1.mine_ref), channel_id=1, source_target_pairs={{0,1},{1,0},{2,3},{3,2},{4,5},{5,4},{6,7},{7,6},{8,9},{9,8},{10,11... | collective-permute-start | bytes 589832 | tf_op jit(solution)/shard_map/ppermute | solution.py:219
  159.9 21.1 %collective-permute-start.20 = (bf16[96,256]{1,0:T(8,128)(2,1)S(1)}, bf16[96,256]{1,0:T(8,128)(2,1)S(1)}, u32[]{:S(2)}, u32[]{:S(2)}) collective-permute-start(bf16[96,256]{1,0:T(8,128)(2,1)S(1)} %total.1), channel_id=1, source_target_pairs={{0,0},{1,1},{2,46},{3,47},{4,76},{5,77},{6,106},{7,107},{8,136},{9... | collective-permute-start | bytes 147464 | tf_op jit(solution)/shard_map/ppermute | solution.py:509
